TPU v7x, 512 devices: a whole 4x8x8 slice. The times are simulated.
512 devices in a mesh: kv: 32 (over z, x), tp: 16 (over y, core).
Axes of the slice: x: 4, y: 8, z: 8, core: 2. Of those that a mesh axis runs over, the one named last changes fastest.
Arguments:
- tokens: bfloat16 [16, 4096], P(None, ('kv', 'tp')), may hold values from -24 to 24
- live_lengths: int32 [16], replicated, may hold values from 256 to 16384, as said below
- kv_cache: bfloat16 [16, 16384, 2048], P(None, 'kv', 'tp'), may hold values from -128 to 128
- gate_sums: float32 [16, 16, 16384], P(None, 'tp', 'kv'), may hold values from -16384 to 0, as said below
- w_query: bfloat16 [4096, 4096], P('kv', 'tp'), may hold values from -0.09375 to 0.09375
- w_key: bfloat16 [4096, 1024], P('kv', 'tp'), may hold values from -0.09375 to 0.09375
- w_value: bfloat16 [4096, 1024], P('kv', 'tp'), may hold values from -0.09375 to 0.09375
- w_forget: bfloat16 [4096, 16], replicated, may hold values from -0.09375 to 0.09375
- forget_bias: float32 [16], replicated, may hold values from -1 to 2
- w_out: bfloat16 [4096, 4096], P('tp', 'kv'), may hold values from -0.75 to 0.75
- first_gain: float32 [4096], P(('kv', 'tp')), may hold values from 0 to 4
- w_gate: bfloat16 [4096, 11264], P('kv', 'tp'), may hold values from -0.09375 to 0.09375
- w_up: bfloat16 [4096, 11264], P('kv', 'tp'), may hold values from -0.09375 to 0.09375
- w_down: bfloat16 [11264, 4096], P('tp', 'kv'), may hold values from -0.109375 to 0.109375
- second_gain: float32 [4096], P(('kv', 'tp')), may hold values from 0 to 4
Outputs:
- layer_out: bfloat16 [16, 4096], P(None, ('kv', 'tp'))
Inputs may be any that keep to these rules, and one draw needn't show every extreme that they name: `live_lengths`: at least one sequence has length exactly 16384. `gate_sums`: entries at positions at or beyond the sequence's length are 0.
All inputs are finite; a program needn't handle non-finite values.
Results may differ from a plain program's by a relative error of at most 0.019.
Values may be sent and summed in bfloat16 or wider, within the bound.
No kernel may reach another device: no remote copies, remote signals or barrier semaphores. Data moves between devices by JAX's collectives and lax.ppermute only.
A program may use at most 64 MiB of HBM per device.

v0:
```python
import jax
import jax.numpy as jnp
from jax import lax
from jax.sharding import Mesh
from jax.sharding import PartitionSpec as P

D = 4096
DH = 64
GROUP = 4
KV = ("kv_0", "kv_1")
KV_TP = ("kv_0", "kv_1", "tp")


EPSILON = 1e-05
EMPTY_SCORE = -1e30


def sent_to_all(shard, axis):
    devices = lax.axis_size(axis)
    return lax.all_to_all(
        jnp.broadcast_to(shard[None], (devices, *shard.shape)), axis, 0, 0, tiled=True
    )


def over_copies(shard, axis):
    everything = sent_to_all(shard, axis)
    return jnp.sum(everything, axis=0)


def packed_total(arrays, axis):
    ends = [0]
    for a in arrays:
        ends.append(ends[-1] + a.size)
    running = over_copies(jnp.concatenate([a.ravel() for a in arrays]), axis)
    return tuple((running[b:e].reshape(a.shape) for a, b, e in zip(arrays, ends, ends[1:])))


def gather_turned(arrays, axis, dims):
    turned = [jnp.moveaxis(a, dim, 0) for a, dim in zip(arrays, dims)]
    widths = [t[0].size for t in turned]
    both = jnp.concatenate([t.reshape(-1, w) for t, w in zip(turned, widths)], axis=1)
    result = lax.all_gather(both, axis, axis=0, tiled=True)
    tiles = jnp.split(result, [sum(widths[:k]) for k in range(1, len(widths))], axis=1)
    return tuple(
        (
            jnp.moveaxis(b.reshape(-1, *t.shape[1:]), 0, dim)
            for b, t, dim in zip(tiles, turned, dims)
        )
    )


def collected_together(shard, axis):
    leaves = jax.tree.leaves(shard)
    turns = sorted(range(len(leaves)), key=lambda k: -leaves[k].size)
    width = (1, *leaves[turns[0]].shape)[-1]
    lines = [
        jnp.pad(leaves[k].reshape(-1), (0, -leaves[k].size % width)).reshape(-1, width)
        for k in turns
    ]
    both, at, found = (lax.all_gather(jnp.concatenate(lines), axis), 0, {})
    for k, line in zip(turns, lines):
        piece = both[:, at : at + len(line)].reshape(len(both), -1)
        found[k] = piece[:, : leaves[k].size].reshape(-1, *leaves[k].shape)
        at += len(line)
    numbers = iter(range(len(leaves)))
    return jax.tree.map(lambda _: found[next(numbers)], shard)


def combined_by_axis(shard, axes, combine):
    for axis in axes:
        pieces = collected_together(shard, axis)
        shard = jax.tree.map(lambda part: part[0], pieces)
        for k in range(1, lax.axis_size(axis)):
            shard = combine(shard, jax.tree.map(lambda part: part[k], pieces))
    return shard


def cut_along(shard, dim, devices):
    shape = shard.shape
    tiles = shard.reshape(*shape[:dim], devices, shape[dim] // devices, *shape[dim + 1 :])
    return jnp.moveaxis(tiles, dim, 0)


def sent_and_summed(shard, axis, dim):
    devices = lax.axis_size(axis)
    tiles = lax.all_to_all(cut_along(shard, dim, devices), axis, 0, 0, tiled=True)
    return jnp.sum(tiles.astype(jnp.float32), axis=0)


def side_by_side(arrays, axis, dim, along):
    widths = [a.shape[along] for a in arrays]
    both = jnp.concatenate(arrays, axis=along)
    result = sent_and_summed(both, axis, dim)
    return tuple(jnp.split(result, [sum(widths[:k]) for k in range(1, len(widths))], axis=along))


def in_order(tiles, dim):
    shape = list(tiles.shape[1:])
    shape[dim] *= tiles.shape[0]
    return jnp.moveaxis(tiles, 0, dim).reshape(shape)


def gather_directly(shard, axis, dim):
    return in_order(sent_to_all(shard, axis), dim)


def combine_parts(earlier, later):
    earlier_top, earlier_total, earlier_sum = earlier
    later_top, later_total, later_sum = later
    joint_top = jnp.maximum(earlier_top, later_top)
    earlier_scale = jnp.exp(earlier_top - joint_top)
    later_scale = jnp.exp(later_top - joint_top)
    joint_total = earlier_total * earlier_scale + later_total * later_scale
    joint_sum = earlier_sum * earlier_scale[..., None] + later_sum * later_scale[..., None]
    return (joint_top, joint_total, joint_sum)


def normalize_block(mixture, norm_gain):
    row_sum, row_square = packed_total(
        (jnp.sum(mixture, axis=1), jnp.sum(mixture * mixture, axis=1)), KV
    )
    centre = row_sum / D
    spread = row_square / D - centre * centre
    scaled = (mixture - centre[:, None]) * lax.rsqrt(spread[:, None] + EPSILON) * norm_gain
    return scaled.astype(jnp.bfloat16)


def on_device(
    tokens,
    live_lengths,
    kv_cache,
    gate_sums,
    w_query,
    w_key,
    w_value,
    w_forget,
    forget_bias,
    w_out,
    first_gain,
    w_gate,
    w_up,
    w_down,
    second_gain,
):
    sequences = tokens.shape[0]
    own_cols = tokens.shape[1]
    gains_pair = jnp.stack([first_gain, second_gain], axis=0)
    wide_rows, wide_gains = gather_turned((tokens.astype(jnp.float32), gains_pair), "tp", (1, 1))
    block_rows = wide_rows.astype(jnp.bfloat16)
    row_count = block_rows.shape[1]
    row_start = lax.axis_index(KV) * row_count
    local_heads = kv_cache.shape[2] // (2 * DH)
    head_start = lax.axis_index("tp") * local_heads
    forget_rows = lax.dynamic_slice(w_forget, (row_start, head_start), (row_count, local_heads))
    query_part = jnp.dot(block_rows, w_query, preferred_element_type=jnp.float32)
    key_part = jnp.dot(block_rows, w_key, preferred_element_type=jnp.float32)
    value_part = jnp.dot(block_rows, w_value, preferred_element_type=jnp.float32)
    forget_part = jnp.dot(block_rows, forget_rows, preferred_element_type=jnp.float32)
    query_sum, key_sum, value_sum, forget_sum = packed_total(
        (query_part, key_part, value_part, forget_part), KV
    )
    queries = query_sum.astype(jnp.bfloat16).reshape(sequences, local_heads, GROUP, DH)
    new_keys = key_sum.astype(jnp.bfloat16).reshape(sequences, local_heads, DH)
    new_values = value_sum.astype(jnp.bfloat16).reshape(sequences, local_heads, DH)
    bias_rows = lax.dynamic_slice_in_dim(forget_bias, head_start, local_heads)
    new_gate = jax.nn.log_sigmoid(forget_sum + bias_rows)
    positions = kv_cache.shape[1]
    cached = kv_cache.reshape(sequences, positions, local_heads, 2, DH)
    score_scale = DH ** (-0.5)
    scores = (
        jnp.einsum(
            "bgjd,bpgd->bgjp", queries, cached[:, :, :, 0], preferred_element_type=jnp.float32
        )
        * score_scale
    )
    scores = scores + gate_sums[:, :, None, :] + new_gate[:, :, None, None]
    position_selector = lax.axis_index(KV) * positions + jnp.arange(positions, dtype=jnp.int32)
    live_mask = (position_selector[None, :] < live_lengths[:, None])[:, None, None, :]
    local_top = jnp.max(jnp.where(live_mask, scores, EMPTY_SCORE), axis=-1)
    weights = jnp.where(live_mask, jnp.exp(scores - local_top[..., None]), 0.0)
    local_total = jnp.sum(weights, axis=-1)
    local_sum = jnp.einsum(
        "bgjp,bpgd->bgjd",
        weights.astype(jnp.bfloat16),
        cached[:, :, :, 1],
        preferred_element_type=jnp.float32,
    )
    row_top, weight_total, summed = combined_by_axis(
        (local_top, local_total, local_sum), KV, combine_parts
    )
    own_score = (
        jnp.einsum("bgjd,bgd->bgj", queries, new_keys, preferred_element_type=jnp.float32)
        * score_scale
    )
    final_top = jnp.maximum(row_top, own_score)
    carry_scale = jnp.exp(row_top - final_top)
    own_weight = jnp.exp(own_score - final_top)
    own_rounded = lax.optimization_barrier(own_weight.astype(jnp.bfloat16)).astype(jnp.float32)
    numerator = summed * carry_scale[..., None] + own_rounded[..., None] * new_values[
        :, :, None, :
    ].astype(jnp.float32)
    attended = (numerator / (weight_total * carry_scale + own_weight)[..., None]).astype(
        jnp.bfloat16
    )
    attended = attended.reshape(sequences, local_heads * GROUP * DH)
    attn_part = jnp.dot(attended, w_out, preferred_element_type=jnp.float32)
    attn_block = over_copies(attn_part, "tp")
    mid_rows = normalize_block(wide_rows + attn_block, wide_gains[0])
    gate_part = jnp.dot(mid_rows, w_gate, preferred_element_type=jnp.float32)
    up_part = jnp.dot(mid_rows, w_up, preferred_element_type=jnp.float32)
    gate_share, up_share = side_by_side(
        (gate_part.astype(jnp.bfloat16), up_part.astype(jnp.bfloat16)), KV, 1, 0
    )
    hidden_share = (jax.nn.silu(gate_share) * up_share).astype(jnp.bfloat16)
    hidden = gather_directly(hidden_share, KV, 1)
    ffn_part = jnp.dot(hidden, w_down, preferred_element_type=jnp.float32)
    ffn_block = over_copies(ffn_part, "tp")
    out_block = normalize_block(mid_rows.astype(jnp.float32) + ffn_block, wide_gains[1])
    return lax.dynamic_slice_in_dim(out_block, lax.axis_index("tp") * own_cols, own_cols, 1)


def solution(mesh):
    split = Mesh(mesh.devices.reshape(8, 4, mesh.shape["tp"]), ("kv_0", "kv_1", "tp"))
    placed = (
        P(None, KV_TP),
        P(),
        P(None, KV, "tp"),
        P(None, "tp", KV),
        P(KV, "tp"),
        P(KV, "tp"),
        P(KV, "tp"),
        P(),
        P(),
        P("tp", KV),
        P(KV_TP),
        P(KV, "tp"),
        P(KV, "tp"),
        P("tp", KV),
        P(KV_TP),
    )
    return jax.shard_map(
        on_device, mesh=split, in_specs=placed, out_specs=P(None, KV_TP), check_vma=False
    )
```

profile of v0, /device:TPU:1, one launch (start us, length us, event | category | flops | bytes accessed | tf_op | source)
XLA Modules:
  0.0 193.3 jit_solution(11887656849411303763)
XLA Ops:
  0.0 0.8 maximum_bitcast_fusion.2
  0.9 0.7 convert_bitcast_fusion
  1.7 21.0 %all_gather.15 = f32[128,18]{1,0:T(8,128)S(1)} all-gather(f32[8,18]{1,0:T(8,128)S(1)} %pad_maximum_fusion.2), channel_id=1, replica_groups=mesh['kv_0'=8,'kv_1'=4,'tp'=16] {'tp'}, dimensions={0}, use_global_device_ids=true | all-gather | bytes 9792 | tf_op jit(solution)/shard_map/all_gather | solution.py:42
  22.7 0.9 fusion.70
  23.7 0.8 fusion.69
  24.6 1.0 convolution_bitcast_fusion
  25.6 0.9 convolution_bitcast_fusion.1
  26.5 1.3 broadcast_in_dim.31
  27.8 11.0 %all-to-all-start = ((f32[32,1,6160]{2,1,0:T(1,128)}), f32[32,1,6160]{2,1,0:T(1,128)S(1)}, u32[]{:S(2)}, u32[]{:S(2)}) async-start(f32[32,1,6160]{2,1,0:T(1,128)} %broadcast_in_dim.31), calls=%async_computation | async-start | bytes 1605632 | tf_op jit(solution)/shard_map/all_to_all | solution.py:20
  38.8 0.6 dynamic_slice.10
  39.4 2.6 %copy.118 = bf16[16,512,128]{1,2,0:T(8,128)(2,1)} copy(bf16[16,512,128]{2,1,0:T(8,128)(2,1)S(1)} %copy-done.1) | data formatting | bytes 4194304 | tf_op args[2]
  42.1 18.6 %all-to-all-done = f32[32,1,6160]{2,1,0:T(1,128)S(1)} async-done(((f32[32,1,6160]{2,1,0:T(1,128)}), f32[32,1,6160]{2,1,0:T(1,128)S(1)}, u32[]{:S(2)}, u32[]{:S(2)}) %all-to-all-start) | async-done | bytes 788512 | tf_op jit(solution)/shard_map/all_to_all | solution.py:20
  60.7 0.5 reduce_sum.99
  61.2 0.7 fusion.38
  61.9 1.6 select_reduce_fusion
  64.5 18.6 %all-gather.2 = f32[8,66,64]{1,2,0:T(8,128)S(1)} all-gather(f32[1,66,64]{1,2,0:T(8,128)S(1)} %maximum_bitcast_fusion), channel_id=2, replica_groups=mesh['kv_0'=8,'kv_1'=4,'tp'=16] {'kv_0'}, dimensions={0}, use_global_device_ids=true | all-gather | bytes 152064 | tf_op jit(solution)/shard_map/all_gather | solution.py:60
  83.1 0.5 slice_reduce_fusion.25
  84.1 10.5 %all-gather.3 = f32[4,66,64]{1,2,0:T(8,128)S(1)} all-gather(f32[1,66,64]{1,2,0:T(8,128)S(1)} %maximum_bitcast_fusion.1), channel_id=3, replica_groups=mesh['kv_0'=8,'kv_1'=4,'tp'=16] {'kv_1'}, dimensions={0}, use_global_device_ids=true | all-gather | bytes 84480 | tf_op jit(solution)/shard_map/all_gather | solution.py:60
  98.6 0.7 broadcast_in_dim.34
  99.2 14.6 %all-to-all-start.1 = ((f32[16,16,128]{2,1,0:T(8,128)}), f32[16,16,128]{2,1,0:T(8,128)S(1)}, u32[]{:S(2)}, u32[]{:S(2)}) async-start(f32[16,16,128]{2,1,0:T(8,128)} %broadcast_in_dim.34), calls=%async_computation.1 | async-start | bytes 262144 | tf_op jit(solution)/shard_map/all_to_all | solution.py:20
  113.9 8.8 %all-to-all-done.1 = f32[16,16,128]{2,1,0:T(8,128)S(1)} async-done(((f32[16,16,128]{2,1,0:T(8,128)}), f32[16,16,128]{2,1,0:T(8,128)S(1)}, u32[]{:S(2)}, u32[]{:S(2)}) %all-to-all-start.1) | async-done | bytes 131104 | tf_op jit(solution)/shard_map/all_to_all | solution.py:20
  122.9 0.6 broadcast_in_dim.35
  123.5 5.3 %all-to-all-start.2 = ((f32[32,1,32]{2,1,0:T(1,128)}), f32[32,1,32]{2,1,0:T(1,128)S(1)}, u32[]{:S(2)}, u32[]{:S(2)}) async-start(f32[32,1,32]{2,1,0:T(1,128)} %broadcast_in_dim.35), calls=%async_computation.2 | async-start | bytes 32768 | tf_op jit(solution)/shard_map/all_to_all | solution.py:20
  129.1 8.4 %all-to-all-done.2 = f32[32,1,32]{2,1,0:T(1,128)S(1)} async-done(((f32[32,1,32]{2,1,0:T(1,128)}), f32[32,1,32]{2,1,0:T(1,128)S(1)}, u32[]{:S(2)}, u32[]{:S(2)}) %all-to-all-start.2) | async-done | bytes 4128 | tf_op jit(solution)/shard_map/all_to_all | solution.py:20
  138.1 0.6 reshape.1443
  139.3 11.7 %all_to_all.38 = bf16[32,2,352]{2,1,0:T(2,128)(2,1)S(1)} all-to-all(bf16[32,2,352]{2,1,0:T(2,128)(2,1)S(1)} %reshape.1497), channel_id=1, replica_groups=mesh['kv_0'=8,'kv_1'=4,'tp'=16] {'kv_0','kv_1'}, dimensions={0} | all-to-all | bytes 90112 | tf_op jit(solution)/shard_map/all_to_all | solution.py:86
  151.8 11.7 %all_to_all.39 = bf16[32,2,176]{2,1,0:T(2,128)(2,1)S(1)} all-to-all(bf16[32,2,176]{2,1,0:T(2,128)(2,1)S(1)} %reshape.1499), channel_id=1, replica_groups=mesh['kv_0'=8,'kv_1'=4,'tp'=16] {'kv_0','kv_1'}, dimensions={0} | all-to-all | bytes 45056 | tf_op jit(solution)/shard_map/all_to_all | solution.py:20
  164.0 15.1 %all_to_all.40 = f32[16,16,128]{2,1,0:T(8,128)S(1)} all-to-all(f32[16,16,128]{2,1,0:T(8,128)S(1)} %broadcast_in_dim.37), channel_id=1, replica_groups=mesh['kv_0'=8,'kv_1'=4,'tp'=16] {'tp'}, dimensions={0} | all-to-all | bytes 262144 | tf_op jit(solution)/shard_map/all_to_all | solution.py:20
  179.3 0.6 broadcast_in_dim.38
  179.9 3.9 %all-to-all-start.6 = ((f32[32,1,32]{2,1,0:T(1,128)}), f32[32,1,32]{2,1,0:T(1,128)S(1)}, u32[]{:S(2)}, u32[]{:S(2)}) async-start(f32[32,1,32]{2,1,0:T(1,128)} %broadcast_in_dim.38), calls=%async_computation.6 | async-start | bytes 32768 | tf_op jit(solution)/shard_map/all_to_all | solution.py:20
  183.9 8.5 %all-to-all-done.6 = f32[32,1,32]{2,1,0:T(1,128)S(1)} async-done(((f32[32,1,32]{2,1,0:T(1,128)}), f32[32,1,32]{2,1,0:T(1,128)S(1)}, u32[]{:S(2)}, u32[]{:S(2)}) %all-to-all-start.6) | async-done | bytes 4128 | tf_op jit(solution)/shard_map/all_to_all | solution.py:20
  192.6 0.7 copy.138
  (126 shorter events, 9.1 us)
Async XLA Ops:
  0.0 137.7 %copy-start = (bf16[128,704]{0,1:T(8,128)(2,1)S(1)}, bf16[128,704]{0,1:T(8,128)(2,1)}, u32[]{:S(2)}) copy-start(bf16[128,704]{0,1:T(8,128)(2,1)} %param.27) | copy-start | bytes 540676
  0.0 38.8 %copy-start.8 = (f32[16]{0:T(128)S(1)}, f32[16]{0:T(128)}, u32[]{:S(2)}) copy-start(f32[16]{0:T(128)} %param.23) | copy-start | bytes 196
  0.0 39.4 %copy-start.6 = (f32[16,1,512]{2,1,0:T(1,128)S(1)}, f32[16,1,512]{2,1,0:T(1,128)}, u32[]{:S(2)}) copy-start(f32[16,1,512]{2,1,0:T(1,128)} %param.18) | copy-start | bytes 98308
  0.0 39.4 %copy-start.1 = (bf16[16,512,128]{2,1,0:T(8,128)(2,1)S(1)}, bf16[16,512,128]{2,1,0:T(8,128)(2,1)}, u32[]{:S(2)}) copy-start(bf16[16,512,128]{2,1,0:T(8,128)(2,1)} %param.17) | copy-start | bytes 6291460
  27.8 32.9 %all-to-all-start = ((f32[32,1,6160]{2,1,0:T(1,128)}), f32[32,1,6160]{2,1,0:T(1,128)S(1)}, u32[]{:S(2)}, u32[]{:S(2)}) async-start(f32[32,1,6160]{2,1,0:T(1,128)} %broadcast_in_dim.31), calls=%async_computation | async-start | bytes 1605632 | tf_op jit(solution)/shard_map/all_to_all | solution.py:20
  39.4 2.6 %copy-start.7 = (s32[16]{0:T(128)S(1)}, s32[16]{0:T(128)}, u32[]{:S(2)}) copy-start(s32[16]{0:T(128)} %param.16) | copy-start | bytes 196
  42.0 21.5 %copy-start.2 = (bf16[16,512,128]{1,2,0:T(8,128)(2,1)S(1)}, bf16[16,512,128]{1,2,0:T(8,128)(2,1)}, u32[]{:S(2)}) copy-start(bf16[16,512,128]{1,2,0:T(8,128)(2,1)} %copy.118) | copy-start | bytes 6291460
  63.9 34.5 %copy-start.5 = (bf16[256,128]{1,0:T(8,128)(2,1)S(1)}, bf16[256,128]{1,0:T(8,128)(2,1)}, u32[]{:S(2)}) copy-start(bf16[256,128]{1,0:T(8,128)(2,1)} %param.24) | copy-start | bytes 196612
  84.0 53.9 %copy-start.3 = (bf16[128,704]{0,1:T(8,128)(2,1)S(1)}, bf16[128,704]{0,1:T(8,128)(2,1)}, u32[]{:S(2)}) copy-start(bf16[128,704]{0,1:T(8,128)(2,1)} %param.26) | copy-start | bytes 540676
  98.6 65.3 %copy-start.4 = (bf16[704,128]{1,0:T(8,128)(2,1)S(1)}, bf16[704,128]{1,0:T(8,128)(2,1)}, u32[]{:S(2)}) copy-start(bf16[704,128]{1,0:T(8,128)(2,1)} %param.28) | copy-start | bytes 540676
  99.2 23.5 %all-to-all-start.1 = ((f32[16,16,128]{2,1,0:T(8,128)}), f32[16,16,128]{2,1,0:T(8,128)S(1)}, u32[]{:S(2)}, u32[]{:S(2)}) async-start(f32[16,16,128]{2,1,0:T(8,128)} %broadcast_in_dim.34), calls=%async_computation.1 | async-start | bytes 262144 | tf_op jit(solution)/shard_map/all_to_all | solution.py:20
  123.5 14.0 %all-to-all-start.2 = ((f32[32,1,32]{2,1,0:T(1,128)}), f32[32,1,32]{2,1,0:T(1,128)S(1)}, u32[]{:S(2)}, u32[]{:S(2)}) async-start(f32[32,1,32]{2,1,0:T(1,128)} %broadcast_in_dim.35), calls=%async_computation.2 | async-start | bytes 32768 | tf_op jit(solution)/shard_map/all_to_all | solution.py:20
  179.9 12.5 %all-to-all-start.6 = ((f32[32,1,32]{2,1,0:T(1,128)}), f32[32,1,32]{2,1,0:T(1,128)S(1)}, u32[]{:S(2)}, u32[]{:S(2)}) async-start(f32[32,1,32]{2,1,0:T(1,128)} %broadcast_in_dim.38), calls=%async_computation.6 | async-start | bytes 32768 | tf_op jit(solution)/shard_map/all_to_all | solution.py:20
where the time goes:
time: 194 us; the launch traced here: 193 us
  blocking collectives  88.6 us (46%)
  waiting for transfers between devices  44.4 us (23%)
  starting transfers between devices  34.8 us (18%)
  local copies, waits for them, and re-layouts  14.5 us (7%)
  matrix products  6.3 us (3%)
  other arithmetic  4.36 us (2%)
    all_to_all x4, waiting for transfers between devices, sent_to_all(): lax.all_to_all(jnp.broadcast_to(shard[None], (devices, *shard.shape)), ax...  44.4 us
    all_to_all x4, starting transfers between devices, sent_to_all(): lax.all_to_all(jnp.broadcast_to(shard[None], (devices, *shard.shape)), ax...  34.8 us
    all_gather x2, blocking collectives, collected_together(): both, at, found = (lax.all_gather(jnp.concatenate(lines), axis), 0, {})  29.2 us
    all_to_all x2, blocking collectives, sent_to_all(): lax.all_to_all(jnp.broadcast_to(shard[None], (devices, *shard.shape)), ax...  26.8 us
    all_gather x1, blocking collectives, gather_turned(): result = lax.all_gather(both, axis, axis=0, tiled=True)  21 us
    all_to_all x1, blocking collectives, sent_and_summed(): lax.all_to_all(cut_along(shard, dim, devices), axis, 0, 0, tiled=True)  11.7 us
  transfers between devices with their start and end apart: 4, of which 4 were waited for; matrix products, arithmetic and copies ran while one was open for 2% of the time, Pallas kernels for 0%

commit v1 on v0

v1 whole, which is shorter than its diff:
```python
import jax
import jax.numpy as jnp
from jax import lax
from jax.sharding import Mesh
from jax.sharding import PartitionSpec as P

D = 4096
DH = 64
GROUP = 4
HALF = 384
KV = ("kv_0", "kv_1")
KV_TP = ("kv_0", "kv_1", "tp")
EPSILON = 1e-05
EMPTY_SCORE = -1e30
F32 = jnp.float32
BF16 = jnp.bfloat16


def exchanged(pieces, axis):
    return lax.all_to_all(pieces, axis, 0, 0, tiled=True)


def sent_to_all(shard, axis):
    devices = lax.axis_size(axis)
    return exchanged(jnp.broadcast_to(shard[None], (devices, *shard.shape)), axis)


def in_pieces(value, count):
    pieces = []
    for _ in range(count):
        piece = lax.reduce_precision(value, 8, 7)
        pieces.append(piece.astype(BF16))
        value = value - piece
    return pieces


def on_device(
    tokens,
    live_lengths,
    kv_cache,
    gate_sums,
    w_query,
    w_key,
    w_value,
    w_forget,
    forget_bias,
    w_out,
    first_gain,
    w_gate,
    w_up,
    w_down,
    second_gain,
):
    sequences, own_cols = tokens.shape
    kv_index = lax.axis_index(KV)
    tp_index = lax.axis_index("tp")
    kv_size = lax.axis_size(KV)
    positions = kv_cache.shape[1]
    hidden_cols = w_gate.shape[1]

    turned = jnp.concatenate(
        [tokens.astype(F32).T, first_gain[:, None], second_gain[:, None]], axis=1
    )
    block = sent_to_all(turned, "tp").reshape(-1, sequences + 2)
    rows = block[:, :sequences].T
    gains = block[:, sequences:].T
    width = rows.shape[1]

    rows_bf = rows.astype(BF16)
    forget_rows = lax.dynamic_slice(w_forget, (kv_index * width, tp_index), (width, 1))
    query_part = jnp.dot(rows_bf, w_query, preferred_element_type=F32)
    key_part = jnp.dot(rows_bf, w_key, preferred_element_type=F32)
    value_part = jnp.dot(rows_bf, w_value, preferred_element_type=F32)
    forget_part = jnp.dot(rows_bf, forget_rows, preferred_element_type=F32)[:, 0]
    token_part = jnp.sum(rows, axis=1)
    out_part = jnp.sum(w_out.astype(F32), axis=1)
    new_rows = jnp.concatenate([key_part, value_part], axis=1).astype(BF16)
    new_rows = jnp.concatenate([new_rows] * (kv_size // sequences), axis=0)
    small = jnp.concatenate([*in_pieces(forget_part, 2), *in_pieces(token_part, 2)])
    small = jnp.pad(small, (0, 2 * DH - small.size))
    mixed = jnp.concatenate(
        [new_rows, jnp.broadcast_to(small[None], (kv_size, small.size))], axis=1
    )
    common = jnp.concatenate([query_part.astype(BF16), *(p[None] for p in in_pieces(out_part, 2))])
    message = jnp.concatenate(
        [jnp.broadcast_to(common[None], (kv_size, *common.shape)), mixed[:, None]], axis=1
    )
    total = jnp.sum(exchanged(message, KV).astype(F32), axis=0)
    queries = total[:sequences].astype(BF16).reshape(sequences, GROUP, DH)
    out_row_sums = total[sequences] + total[sequences + 1]
    mixed = total[sequences + 2]
    new_key = mixed[:DH].astype(BF16)
    new_value = mixed[DH : 2 * DH].astype(BF16).astype(F32)
    small = mixed[2 * DH : 2 * DH + 4 * sequences].reshape(4, sequences)
    new_gate = jax.nn.log_sigmoid(
        small[0] + small[1] + lax.dynamic_slice_in_dim(forget_bias, tp_index, 1)
    )
    token_sums = small[2] + small[3]

    score_scale = DH**-0.5
    keys, values = kv_cache[:, :, :DH], kv_cache[:, :, DH:]
    scores = (
        jnp.einsum("bjd,bpd->bjp", queries, keys, preferred_element_type=F32) * score_scale
    )
    scores = scores + gate_sums[:, :, :] + new_gate[:, None, None]
    position = kv_index * positions + jnp.arange(positions, dtype=jnp.int32)
    live = (position[None, :] < live_lengths[:, None])[:, None, :]
    own_here = (jnp.arange(sequences) == kv_index)[:, None]
    own_score = jnp.einsum("bjd,d->bj", queries, new_key, preferred_element_type=F32) * score_scale
    own_score = jnp.where(own_here, own_score, EMPTY_SCORE)
    top = jnp.maximum(jnp.max(jnp.where(live, scores, EMPTY_SCORE), axis=-1), own_score)
    weights = jnp.where(live, jnp.exp(scores - top[..., None]), 0.0)
    own_weight = jnp.where(own_here, jnp.exp(own_score - top), 0.0)
    weight_total = jnp.sum(weights, axis=-1) + own_weight
    weighted = jnp.einsum(
        "bjp,bpd->bjd", weights.astype(BF16), values, preferred_element_type=F32
    )
    own_rounded = lax.reduce_precision(own_weight, 8, 7)
    weighted = weighted + own_rounded[..., None] * new_value
    stats = jnp.concatenate([*in_pieces(top, 3), *in_pieces(weight_total, 2)], axis=1)
    stats = jnp.pad(stats, ((0, 0), (0, 2 * DH - stats.shape[1])))
    message = jnp.concatenate([weighted.reshape(sequences, -1).astype(BF16), stats], axis=1)
    parts = sent_to_all(message, KV).astype(F32)
    heads = GROUP * DH
    stats = parts[:, :, heads : heads + 5 * GROUP].reshape(kv_size, sequences, 5, GROUP)
    tops = stats[:, :, 0] + stats[:, :, 1] + stats[:, :, 2]
    totals = stats[:, :, 3] + stats[:, :, 4]
    scales = jnp.exp(tops - jnp.max(tops, axis=0))
    joint_total = jnp.sum(totals * scales, axis=0)
    parts = parts[:, :, :heads].reshape(kv_size, sequences, GROUP, DH)
    joint = jnp.sum(parts * scales[..., None], axis=0)
    attended = (joint / joint_total[..., None]).astype(BF16).reshape(sequences, heads)

    attn_part = jnp.dot(attended, w_out, preferred_element_type=F32)
    mean_part = jnp.sum(attended.astype(F32) * out_row_sums, axis=1)
    means = jnp.concatenate(in_pieces(mean_part, 2))
    means = jnp.pad(means, (0, width - means.size))
    message = jnp.concatenate([attn_part.astype(BF16), means[None]])
    total = jnp.sum(sent_to_all(message, "tp").astype(F32), axis=0)
    mean_sums = total[sequences, :sequences] + total[sequences, sequences : 2 * sequences]
    centre = (token_sums + mean_sums) / D
    centred = rows + total[:sequences] - centre[:, None]
    scaled = centred * gains[0]

    squares = jnp.sum(centred * centred, axis=1)
    scaled_bf = scaled.astype(BF16)
    pad = ((0, 0), (0, 2 * HALF - hidden_cols))
    gate_part = jnp.dot(scaled_bf, w_gate, preferred_element_type=F32).astype(BF16)
    up_part = jnp.dot(scaled_bf, w_up, preferred_element_type=F32).astype(BF16)
    squares = jnp.concatenate(in_pieces(squares, 2))
    squares = jnp.pad(squares, (0, HALF - squares.size))
    message = jnp.stack(
        [
            jnp.pad(gate_part, pad).reshape(kv_size, HALF),
            jnp.pad(up_part, pad).reshape(kv_size, HALF),
            jnp.broadcast_to(squares[None], (kv_size, HALF)),
        ],
        axis=1,
    )
    total = jnp.sum(exchanged(message, KV).astype(F32), axis=0)
    spread = (total[2, :sequences] + total[2, sequences : 2 * sequences]) / D
    shrink = lax.rsqrt(spread + EPSILON)
    own_shrink = lax.dynamic_slice_in_dim(shrink, kv_index // 2, 1)
    hidden_share = jax.nn.silu(total[0] * own_shrink) * (total[1] * own_shrink)
    mid = lax.reduce_precision(scaled * shrink[:, None], 8, 7)

    hidden = sent_to_all(hidden_share.astype(BF16)[None], KV).reshape(sequences, 2 * HALF)

    ffn_part = jnp.dot(hidden[:, :hidden_cols], w_down, preferred_element_type=F32)
    ffn = jnp.sum(sent_to_all(ffn_part.astype(BF16), "tp").astype(F32), axis=0)
    mixture = mid + ffn

    block_sum = jnp.sum(mixture, axis=1)
    block_centre = block_sum / width
    block_square = jnp.sum((mixture - block_centre[:, None]) ** 2, axis=1)
    both = sent_to_all(jnp.concatenate([block_centre, block_square])[None], KV)
    centres, squares = both[:, 0, :sequences], both[:, 0, sequences:]
    centre = jnp.sum(centres, axis=0) / kv_size
    spread = jnp.sum(squares + width * (centres - centre) ** 2, axis=0) / D
    own = tp_index * own_cols
    mixture = lax.dynamic_slice_in_dim(mixture, own, own_cols, 1)
    gain = lax.dynamic_slice_in_dim(gains[1], own, own_cols)
    out = (mixture - centre[:, None]) * lax.rsqrt(spread[:, None] + EPSILON) * gain
    return out.astype(BF16)


def solution(mesh):
    split = Mesh(mesh.devices.reshape(8, 4, mesh.shape["tp"]), ("kv_0", "kv_1", "tp"))
    placed = (
        P(None, KV_TP),
        P(),
        P(None, KV, "tp"),
        P(None, "tp", KV),
        P(KV, "tp"),
        P(KV, "tp"),
        P(KV, "tp"),
        P(),
        P(),
        P("tp", KV),
        P(KV_TP),
        P(KV, "tp"),
        P(KV, "tp"),
        P("tp", KV),
        P(KV_TP),
    )
    return jax.shard_map(
        on_device, mesh=split, in_specs=placed, out_specs=P(None, KV_TP), check_vma=False
    )
```

time: 194 us -> 153 us (0.79)
  blocking collectives: 88.6 us -> 11.8 us
  waiting for transfers between devices: 44.4 us -> 66.3 us
  starting transfers between devices: 34.8 us -> 46.9 us
  other arithmetic: 4.36 us -> 9.97 us
  local copies, waits for them, and re-layouts: 14.5 us -> 10.1 us
    all_gather x3 -> x0, blocking collectives: 50.1 us -> none  [the longest x2 29.2 us: collected_together(): both, at, found = (lax.all_gather(jnp.concatenate(lines), axis), 0, {})]
    all_to_all x3 -> x1, blocking collectives: 38.5 us -> 11.8 us  [exchanged(): return lax.all_to_all(pieces, axis, 0, 0, tiled=True)]
    all_to_all x4 -> x7, waiting for transfers between devices: 44.4 us -> 66.3 us  [exchanged(): return lax.all_to_all(pieces, axis, 0, 0, tiled=True)]
    all_to_all x4 -> x7, starting transfers between devices: 34.8 us -> 46.9 us  [exchanged(): return lax.all_to_all(pieces, axis, 0, 0, tiled=True)]
    unnamed x28 -> x21, local copies, waits for them, and re-layouts: 3.53 us -> 1.08 us
  transfers between devices with their start and end apart: 4 -> 7, of which waited for: 4 -> 7; matrix products, arithmetic and copies ran while one was open for 2% -> 1% of each run, Pallas kernels for 0% -> 0%
where the time goes in v1:
time: 153 us; the launch traced here: 152 us
  waiting for transfers between devices  66.3 us (43%)
  starting transfers between devices  46.9 us (31%)
  blocking collectives  11.8 us (8%)
  local copies, waits for them, and re-layouts  10.1 us (7%)
  other arithmetic  9.97 us (7%)
  matrix products  6.14 us (4%)
    all_to_all x7, waiting for transfers between devices, exchanged(): return lax.all_to_all(pieces, axis, 0, 0, tiled=True)  66.3 us
    all_to_all x7, starting transfers between devices, exchanged(): return lax.all_to_all(pieces, axis, 0, 0, tiled=True)  46.9 us
    all_to_all x1, blocking collectives, exchanged(): return lax.all_to_all(pieces, axis, 0, 0, tiled=True)  11.8 us
    broadcast_in_dim x7, local copies, waits for them, and re-layouts, sent_to_all(): jnp.broadcast_to(shard[None], (devices, *shard.shape))  3.23 us
  transfers between devices with their start and end apart: 7, of which 7 were waited for; matrix products, arithmetic and copies ran while one was open for 1% of the time, Pallas kernels for 0%

profile of v1, /device:TPU:1, one launch (start us, length us, event | category | flops | bytes accessed | tf_op | source)
XLA Modules:
  0.0 151.7 jit_solution(15464000430800125499)
XLA Ops:
  0.0 0.8 convert_bitcast_fusion
  0.9 0.7 copy.84
  1.6 0.7 copy.85
  2.4 0.7 reshape.278
  3.1 10.1 %all-to-all-start = ((f32[16,1,144]{2,1,0:T(1,128)}), f32[16,1,144]{2,1,0:T(1,128)S(1)}, u32[]{:S(2)}, u32[]{:S(2)}) async-start(f32[16,1,144]{2,1,0:T(1,128)} %reshape.278), calls=%async_computation | async-start | bytes 32768 | tf_op jit(solution)/shard_map/all_to_all | solution.py:20
  13.2 0.9 convert_reduce_fusion.4
  14.2 6.4 %all-to-all-done = f32[16,1,144]{2,1,0:T(1,128)S(1)} async-done(((f32[16,1,144]{2,1,0:T(1,128)}), f32[16,1,144]{2,1,0:T(1,128)S(1)}, u32[]{:S(2)}, u32[]{:S(2)}) %all-to-all-start) | async-done | bytes 9248 | tf_op jit(solution)/shard_map/all_to_all | solution.py:20
  21.9 0.9 convolution_convert_fusion.5
  22.8 0.9 convolution_convert_fusion.6
  23.7 0.9 reduce-precision_convert_fusion.7
  24.8 1.0 convolution_convert_fusion.2
  25.9 0.8 pad_maximum_fusion
  26.7 11.3 %all-to-all-start.1 = ((bf16[32,19,256]{2,1,0:T(8,128)(2,1)}), bf16[32,19,256]{2,1,0:T(8,128)(2,1)S(1)}, u32[]{:S(2)}, u32[]{:S(2)}) async-start(bf16[32,19,256]{2,1,0:T(8,128)(2,1)} %pad_maximum_fusion), calls=%async_computation.1 | async-start | bytes 786432 | tf_op jit(solution)/shard_map/all_to_all | solution.py:20
  38.7 13.2 %all-to-all-done.1 = bf16[32,19,256]{2,1,0:T(8,128)(2,1)S(1)} async-done(((bf16[32,19,256]{2,1,0:T(8,128)(2,1)}), bf16[32,19,256]{2,1,0:T(8,128)(2,1)S(1)}, u32[]{:S(2)}, u32[]{:S(2)}) %all-to-all-start.1) | async-done | bytes 311328 | tf_op jit(solution)/shard_map/all_to_all | solution.py:20
  52.1 0.7 fusion.65
  53.1 0.8 select_reduce_fusion
  54.2 0.8 fusion.17
  55.2 0.8 broadcast_in_dim.128
  56.0 5.0 %all-to-all-start.2 = ((bf16[32,16,384]{2,1,0:T(8,128)(2,1)}), bf16[32,16,384]{2,1,0:T(8,128)(2,1)S(1)}, u32[]{:S(2)}, u32[]{:S(2)}) async-start(bf16[32,16,384]{2,1,0:T(8,128)(2,1)} %broadcast_in_dim.128), calls=%async_computation.2 | async-start | bytes 786432 | tf_op jit(solution)/shard_map/all_to_all | solution.py:20
  61.0 12.8 %all-to-all-done.2 = bf16[32,16,384]{2,1,0:T(8,128)(2,1)S(1)} async-done(((bf16[32,16,384]{2,1,0:T(8,128)(2,1)}), bf16[32,16,384]{2,1,0:T(8,128)(2,1)S(1)}, u32[]{:S(2)}, u32[]{:S(2)}) %all-to-all-start.2) | async-done | bytes 393248 | tf_op jit(solution)/shard_map/all_to_all | solution.py:20
  73.8 1.3 copy.90
  77.6 6.8 %all-to-all-start.3 = ((bf16[16,17,128]{2,1,0:T(8,128)(2,1)}), bf16[16,17,128]{2,1,0:T(8,128)(2,1)S(1)}, u32[]{:S(2)}, u32[]{:S(2)}) async-start(bf16[16,17,128]{2,1,0:T(8,128)(2,1)} %broadcast_in_dim.130), calls=%async_computation.3 | async-start | bytes 196608 | tf_op jit(solution)/shard_map/all_to_all | solution.py:20
  84.5 8.4 %all-to-all-done.3 = bf16[16,17,128]{2,1,0:T(8,128)(2,1)S(1)} async-done(((bf16[16,17,128]{2,1,0:T(8,128)(2,1)}), bf16[16,17,128]{2,1,0:T(8,128)(2,1)S(1)}, u32[]{:S(2)}, u32[]{:S(2)}) %all-to-all-start.3) | async-done | bytes 69664 | tf_op jit(solution)/shard_map/all_to_all | solution.py:20
  93.9 0.8 pad_maximum_fusion.1
  94.7 3.9 %all-to-all-start.4 = ((bf16[32,3,384]{2,1,0:T(4,128)(2,1)}), bf16[32,3,384]{2,1,0:T(4,128)(2,1)S(1)}, u32[]{:S(2)}, u32[]{:S(2)}) async-start(bf16[32,3,384]{2,1,0:T(4,128)(2,1)} %pad_maximum_fusion.1), calls=%async_computation.4 | async-start | bytes 196608 | tf_op jit(solution)/shard_map/all_to_all | solution.py:20
  98.6 9.4 %all-to-all-done.4 = bf16[32,3,384]{2,1,0:T(4,128)(2,1)S(1)} async-done(((bf16[32,3,384]{2,1,0:T(4,128)(2,1)}), bf16[32,3,384]{2,1,0:T(4,128)(2,1)S(1)}, u32[]{:S(2)}, u32[]{:S(2)}) %all-to-all-start.4) | async-done | bytes 73760 | tf_op jit(solution)/shard_map/all_to_all | solution.py:20
  110.0 0.8 reduce.18
  110.8 11.8 %all_to_all.40 = bf16[32,2,192]{2,1,0:T(2,128)(2,1)S(1)} all-to-all(bf16[32,2,192]{2,1,0:T(2,128)(2,1)S(1)} %reshape.280), channel_id=1, replica_groups=mesh['kv_0'=8,'kv_1'=4,'tp'=16] {'kv_0','kv_1'}, dimensions={0} | all-to-all | bytes 49152 | tf_op jit(solution)/shard_map/all_to_all | solution.py:20
  123.7 5.9 %all-to-all-start.6 = ((bf16[16,16,128]{2,1,0:T(8,128)(2,1)}), bf16[16,16,128]{2,1,0:T(8,128)(2,1)S(1)}, u32[]{:S(2)}, u32[]{:S(2)}) async-start(bf16[16,16,128]{2,1,0:T(8,128)(2,1)} %broadcast_in_dim.132), calls=%async_computation.6 | async-start | bytes 131072 | tf_op jit(solution)/shard_map/all_to_all | solution.py:20
  129.7 7.7 %all-to-all-done.6 = bf16[16,16,128]{2,1,0:T(8,128)(2,1)S(1)} async-done(((bf16[16,16,128]{2,1,0:T(8,128)(2,1)}), bf16[16,16,128]{2,1,0:T(8,128)(2,1)S(1)}, u32[]{:S(2)}, u32[]{:S(2)}) %all-to-all-start.6) | async-done | bytes 65568 | tf_op jit(solution)/shard_map/all_to_all | solution.py:20
  138.4 3.9 %all-to-all-start.7 = ((f32[32,1,32]{2,1,0:T(1,128)}), f32[32,1,32]{2,1,0:T(1,128)S(1)}, u32[]{:S(2)}, u32[]{:S(2)}) async-start(f32[32,1,32]{2,1,0:T(1,128)} %broadcast_in_dim.133), calls=%async_computation.7 | async-start | bytes 32768 | tf_op jit(solution)/shard_map/all_to_all | solution.py:20
  142.4 8.5 %all-to-all-done.7 = f32[32,1,32]{2,1,0:T(1,128)S(1)} async-done(((f32[32,1,32]{2,1,0:T(1,128)}), f32[32,1,32]{2,1,0:T(1,128)S(1)}, u32[]{:S(2)}, u32[]{:S(2)}) %all-to-all-start.7) | async-done | bytes 4128 | tf_op jit(solution)/shard_map/all_to_all | solution.py:20
  (105 shorter events, 11.9 us)
Async XLA Ops:
  0.0 93.2 %copy-start = (bf16[128,704]{0,1:T(8,128)(2,1)S(1)}, bf16[128,704]{0,1:T(8,128)(2,1)}, u32[]{:S(2)}) copy-start(bf16[128,704]{0,1:T(8,128)(2,1)} %param.26) | copy-start | bytes 540676
  0.0 38.0 %copy-start.7 = (f32[16]{0:T(128)S(1)}, f32[16]{0:T(128)}, u32[]{:S(2)}) copy-start(f32[16]{0:T(128)} %param.23) | copy-start | bytes 196
  0.0 38.6 %copy-start.4 = (f32[16,1,512]{2,1,0:T(1,128)S(1)}, f32[16,1,512]{2,1,0:T(1,128)}, u32[]{:S(2)}) copy-start(f32[16,1,512]{2,1,0:T(1,128)} %param.18) | copy-start | bytes 98308
  0.0 38.6 %copy-start.5 = (s32[16]{0:T(128)S(1)}, s32[16]{0:T(128)}, u32[]{:S(2)}) copy-start(s32[16]{0:T(128)} %param.16) | copy-start | bytes 196
  0.0 53.1 %copy-start.6 = (bf16[16,512,128]{2,1,0:T(8,128)(2,1)S(1)}, bf16[16,512,128]{2,1,0:T(8,128)(2,1)}, u32[]{:S(2)}) copy-start(bf16[16,512,128]{2,1,0:T(8,128)(2,1)} %param.17) | copy-start | bytes 6291460
  3.1 17.5 %all-to-all-start = ((f32[16,1,144]{2,1,0:T(1,128)}), f32[16,1,144]{2,1,0:T(1,128)S(1)}, u32[]{:S(2)}, u32[]{:S(2)}) async-start(f32[16,1,144]{2,1,0:T(1,128)} %reshape.278), calls=%async_computation | async-start | bytes 32768 | tf_op jit(solution)/shard_map/all_to_all | solution.py:20
  26.7 25.2 %all-to-all-start.1 = ((bf16[32,19,256]{2,1,0:T(8,128)(2,1)}), bf16[32,19,256]{2,1,0:T(8,128)(2,1)S(1)}, u32[]{:S(2)}, u32[]{:S(2)}) async-start(bf16[32,19,256]{2,1,0:T(8,128)(2,1)} %pad_maximum_fusion), calls=%async_computation.1 | async-start | bytes 786432 | tf_op jit(solution)/shard_map/all_to_all | solution.py:20
  56.0 17.8 %all-to-all-start.2 = ((bf16[32,16,384]{2,1,0:T(8,128)(2,1)}), bf16[32,16,384]{2,1,0:T(8,128)(2,1)S(1)}, u32[]{:S(2)}, u32[]{:S(2)}) async-start(bf16[32,16,384]{2,1,0:T(8,128)(2,1)} %broadcast_in_dim.128), calls=%async_computation.2 | async-start | bytes 786432 | tf_op jit(solution)/shard_map/all_to_all | solution.py:20
  75.8 0.8 copy-start.1
  75.8 17.6 %copy-start.2 = (bf16[128,704]{0,1:T(8,128)(2,1)S(1)}, bf16[128,704]{0,1:T(8,128)(2,1)}, u32[]{:S(2)}) copy-start(bf16[128,704]{0,1:T(8,128)(2,1)} %param.27) | copy-start | bytes 540676
  76.5 46.5 %copy-start.3 = (bf16[704,128]{1,0:T(8,128)(2,1)S(1)}, bf16[704,128]{1,0:T(8,128)(2,1)}, u32[]{:S(2)}) copy-start(bf16[704,128]{1,0:T(8,128)(2,1)} %param.28) | copy-start | bytes 540676
  77.6 15.3 %all-to-all-start.3 = ((bf16[16,17,128]{2,1,0:T(8,128)(2,1)}), bf16[16,17,128]{2,1,0:T(8,128)(2,1)S(1)}, u32[]{:S(2)}, u32[]{:S(2)}) async-start(bf16[16,17,128]{2,1,0:T(8,128)(2,1)} %broadcast_in_dim.130), calls=%async_computation.3 | async-start | bytes 196608 | tf_op jit(solution)/shard_map/all_to_all | solution.py:20
  94.7 13.3 %all-to-all-start.4 = ((bf16[32,3,384]{2,1,0:T(4,128)(2,1)}), bf16[32,3,384]{2,1,0:T(4,128)(2,1)S(1)}, u32[]{:S(2)}, u32[]{:S(2)}) async-start(bf16[32,3,384]{2,1,0:T(4,128)(2,1)} %pad_maximum_fusion.1), calls=%async_computation.4 | async-start | bytes 196608 | tf_op jit(solution)/shard_map/all_to_all | solution.py:20
  123.7 13.7 %all-to-all-start.6 = ((bf16[16,16,128]{2,1,0:T(8,128)(2,1)}), bf16[16,16,128]{2,1,0:T(8,128)(2,1)S(1)}, u32[]{:S(2)}, u32[]{:S(2)}) async-start(bf16[16,16,128]{2,1,0:T(8,128)(2,1)} %broadcast_in_dim.132), calls=%async_computation.6 | async-start | bytes 131072 | tf_op jit(solution)/shard_map/all_to_all | solution.py:20
  138.4 12.5 %all-to-all-start.7 = ((f32[32,1,32]{2,1,0:T(1,128)}), f32[32,1,32]{2,1,0:T(1,128)S(1)}, u32[]{:S(2)}, u32[]{:S(2)}) async-start(f32[32,1,32]{2,1,0:T(1,128)} %broadcast_in_dim.133), calls=%async_computation.7 | async-start | bytes 32768 | tf_op jit(solution)/shard_map/all_to_all | solution.py:20

commit v2 on v1

v2 whole, which is shorter than its diff:
```python
import jax
import jax.numpy as jnp
from jax import lax
from jax.experimental import pallas as pl
from jax.experimental.pallas import tpu as pltpu
from jax.sharding import Mesh
from jax.sharding import PartitionSpec as P

D = 4096
DH = 64
LANES = 128
KV = ("kv_0", "kv_1")
KV_TP = ("kv_0", "kv_1", "tp")
EPSILON = 1e-05
EMPTY_SCORE = -1e30
F32 = jnp.float32
BF16 = jnp.bfloat16

VMEM = pl.BlockSpec(memory_space=pltpu.VMEM)
SMEM = pl.BlockSpec(memory_space=pltpu.SMEM)
ANY = pl.BlockSpec(memory_space=pl.ANY)


def kernel(body, outs, specs, scratch=()):
    return pl.pallas_call(
        body,
        out_shape=[jax.ShapeDtypeStruct(shape, dtype) for shape, dtype in outs],
        in_specs=specs,
        out_specs=[VMEM] * len(outs),
        scratch_shapes=scratch,
    )


def exchanged(pieces, axis):
    return lax.all_to_all(pieces, axis, 0, 0, tiled=True)


def kv_index():
    return lax.axis_index("kv_0") * lax.axis_size("kv_1") + lax.axis_index("kv_1")


def iota(shape, dim):
    return lax.broadcasted_iota(jnp.int32, shape, dim)


def rounded(x):
    return x.astype(BF16).astype(F32)


def in_pieces(value, count):
    pieces = []
    for _ in range(count):
        piece = rounded(value)
        pieces.append(piece)
        value = value - piece
    return pieces


def diagonal(rows, turn):
    return iota((rows, LANES), 1) == iota((rows, LANES), 0) + rows * turn


def as_row(columns):
    rows = columns[0].shape[0]
    tile = jnp.zeros((rows, LANES), F32)
    for turn, column in enumerate(columns):
        tile = jnp.where(diagonal(rows, turn), column, tile)
    return jnp.sum(tile, axis=0, keepdims=True)


def as_column(row, rows, turns):
    mask = diagonal(rows, turns[0])
    for turn in turns[1:]:
        mask = mask | diagonal(rows, turn)
    return jnp.sum(jnp.where(mask, row, 0.0), axis=1, keepdims=True)


def summed(ref, start, size):
    total = ref[0, pl.ds(start, size)].astype(F32)
    for k in range(1, ref.shape[0]):
        total = total + ref[k, pl.ds(start, size)].astype(F32)
    return total


def k_tokens(tokens, out, tile):
    own = tokens.shape[1]
    tile[...] = jnp.zeros(tile.shape, F32)
    tile[:, :own] = tokens[...].astype(F32)
    placed = pltpu.roll(tile[...], lax.axis_index("tp") * own, 1).astype(BF16)
    for k in range(out.shape[0]):
        out[k] = placed


def k_project(recv, w_query, w_key, w_value, w_forget, w_out, out, x_out, new_rows, wf, sem):
    rows = recv.shape[1]
    width = wf.shape[0]
    start = pl.multiple_of(kv_index() * width, width)
    copy = pltpu.make_async_copy(w_forget.at[pl.ds(start, width)], wf, sem)
    copy.start()
    x = summed(recv, 0, rows)
    x_out[...] = x
    xb = x.astype(BF16)
    query = jnp.dot(xb, w_query[...], preferred_element_type=F32)
    key = jnp.dot(xb, w_key[...], preferred_element_type=F32)
    value = jnp.dot(xb, w_value[...], preferred_element_type=F32)
    new_rows[:, :DH] = key
    new_rows[:, DH:] = value
    out_sums = lax.dot_general(
        jnp.ones((8, LANES), BF16), w_out[...], (((1,), (1,)), ((), ())), preferred_element_type=F32
    )
    sums_hi, sums_lo = in_pieces(out_sums, 2)
    token_col = jnp.sum(x, axis=1, keepdims=True)
    copy.wait()
    forget = jnp.dot(xb, wf[...], preferred_element_type=F32)
    mine = iota(forget.shape, 1) == lax.axis_index("tp")
    forget_col = jnp.sum(jnp.where(mine, forget, 0.0), axis=1, keepdims=True)
    small = as_row([*in_pieces(forget_col, 2), *in_pieces(token_col, 2)])
    row = iota((8, LANES), 0)
    tail = jnp.where(row == 1, small, 0.0)
    tail = jnp.where(row == 2, sums_hi[:, :LANES], tail)
    tail = jnp.where(row == 3, sums_hi[:, LANES:], tail)
    tail = jnp.where(row == 4, sums_lo[:, :LANES], tail)
    tail = jnp.where(row == 5, sums_lo[:, LANES:], tail)
    left = query[:, :LANES].astype(BF16)
    right = query[:, LANES:].astype(BF16)
    for b in range(rows):
        own_tail = jnp.where(row == 0, new_rows[pl.ds(b, 1), :], tail).astype(BF16)
        for k in range(b, out.shape[0], rows):
            out[k, pl.ds(0, rows)] = left
            out[k, pl.ds(rows, rows)] = right
            out[k, pl.ds(2 * rows, 8)] = own_tail


def k_attend(recv, lengths, bias, cache, gate, out, tok_out, sums_out, qs, os):
    rows = cache.shape[0]
    positions = cache.shape[1]
    scale = DH**-0.5
    left = rounded(summed(recv, 0, rows))
    right = rounded(summed(recv, rows, rows))
    tail = summed(recv, 2 * rows, 8)
    new_row = rounded(tail[0:1])
    small = tail[1:2]
    sums_out[0:1, :] = tail[2:3] + tail[4:5]
    sums_out[1:2, :] = tail[3:4] + tail[5:6]
    tok_out[...] = jnp.broadcast_to(as_column(small, rows, (2, 3)), tok_out.shape)
    fetched = as_column(small, rows, (0, 1)) + bias[lax.axis_index("tp")]
    new_gate = jnp.minimum(fetched, 0.0) - jnp.log(1.0 + jnp.exp(-jnp.abs(fetched)))
    low = iota((rows, LANES), 1) < DH
    qs[pl.ds(0, rows)] = jnp.where(low, left, 0.0)
    qs[pl.ds(rows, rows)] = jnp.where(low, pltpu.roll(left, DH, 1), 0.0)
    qs[pl.ds(2 * rows, rows)] = jnp.where(low, right, 0.0)
    qs[pl.ds(3 * rows, rows)] = jnp.where(low, pltpu.roll(right, DH, 1), 0.0)
    qs[pl.ds(4 * rows, 4 * rows)] = jnp.zeros((4 * rows, LANES), F32)
    me = kv_index()
    place = me * positions + iota((8, positions), 1)
    lane = iota((8, LANES), 1)
    for b in range(rows):
        query = qs[pl.ds(b, 8, stride=rows), :]
        block = cache[b]
        scores = lax.dot_general(
            query.astype(BF16), block, (((1,), (1,)), ((), ())), preferred_element_type=F32
        )
        scores = scores * scale + (gate[b] + new_gate[b : b + 1])
        live = place < lengths[b]
        own = jnp.sum(query * new_row, axis=1, keepdims=True) * scale
        own = jnp.where(me == b, own, EMPTY_SCORE)
        top = jnp.max(jnp.where(live, scores, EMPTY_SCORE), axis=1, keepdims=True)
        top = jnp.maximum(top, own)
        weights = jnp.where(live, jnp.exp(scores - top), 0.0)
        own_weight = jnp.where(me == b, jnp.exp(own - top), 0.0)
        total = jnp.sum(weights, axis=1, keepdims=True) + own_weight
        value = jnp.dot(weights.astype(BF16), block, preferred_element_type=F32)
        value = value + rounded(own_weight) * new_row
        value = jnp.where(lane == 0, top, jnp.where(lane == 1, total, value))
        os[pl.ds(b, 8, stride=rows), :] = value
    heads = [os[pl.ds(h * rows, rows)] for h in range(4)]
    low_out = jnp.where(low, pltpu.roll(heads[0], DH, 1), heads[1]).astype(BF16)
    high_out = jnp.where(low, pltpu.roll(heads[2], DH, 1), heads[3]).astype(BF16)
    lane = iota((rows, LANES), 1)
    stats = jnp.zeros((rows, LANES), F32)
    for h in range(4):
        pieces = [*in_pieces(heads[h][:, 0:1], 3), *in_pieces(heads[h][:, 1:2], 2)]
        for k, piece in enumerate(pieces):
            stats = jnp.where(lane == 8 * h + k, piece, stats)
    stats = (stats[:8] + pltpu.roll(stats[8:], 32, 1)).astype(BF16)
    for k in range(out.shape[0]):
        out[k, pl.ds(0, rows)] = low_out
        out[k, pl.ds(rows, rows)] = high_out
        out[k, pl.ds(2 * rows, 8)] = stats


def k_combine(recv, sums, w_out, gain, out, tile):
    devices = recv.shape[0]
    rows = (recv.shape[1] - 8) // 2
    heads = 4 * DH
    source = iota((LANES, 4 * heads), 0)
    column = iota((LANES, 4 * heads), 1)
    half = (column // heads) % 2
    first = 32 * half + 8 * ((column % heads) // DH)
    is_top = column < 2 * heads
    begin = jnp.where(is_top, first, first + 3)
    end = jnp.where(is_top, first + 3, first + 5)
    spread = jnp.where((source >= begin) & (source < end), 1.0, 0.0).astype(BF16)
    stats = recv[:, pl.ds(2 * rows, 8), :].reshape(devices * 8, LANES)
    wide = jnp.dot(stats, spread, preferred_element_type=F32).reshape(devices, 8, 4 * heads)
    blocks = []
    for half in range(2):
        tops = wide[:, :, half * heads : (half + 1) * heads]
        totals = wide[:, :, (2 + half) * heads : (3 + half) * heads]
        scales = jnp.exp(tops - jnp.max(tops, axis=0, keepdims=True))
        total = jnp.sum(totals * scales, axis=0)
        low = recv[:, pl.ds(8 * half, 8), :].astype(F32)
        high = recv[:, pl.ds(rows + 8 * half, 8), :].astype(F32)
        low = jnp.sum(low * scales[:, :, :LANES], axis=0)
        high = jnp.sum(high * scales[:, :, LANES:], axis=0)
        blocks.append(jnp.concatenate([low, high], axis=1) / total)
    attended = jnp.concatenate(blocks, axis=0).astype(BF16)
    attn_part = jnp.dot(attended, w_out[...], preferred_element_type=F32).astype(BF16)
    wide = attended.astype(F32)
    mean = wide[:, :LANES] * sums[0:1, :] + wide[:, LANES:] * sums[1:2, :]
    mean_row = as_row(in_pieces(jnp.sum(mean, axis=1, keepdims=True), 2))
    own = gain.shape[1]
    tile[...] = jnp.zeros(tile.shape, F32)
    tile[0:1, :own] = gain[...]
    gains = in_pieces(pltpu.roll(tile[...], lax.axis_index("tp") * own, 1)[0:1], 3)
    row = iota((8, LANES), 0)
    tail = jnp.where(row == 0, mean_row, 0.0)
    for k, piece in enumerate(gains):
        tail = jnp.where(row == 1 + k, piece, tail)
    tail = tail.astype(BF16)
    for k in range(out.shape[0]):
        out[k, pl.ds(0, rows)] = attn_part
        out[k, pl.ds(rows, 8)] = tail


def k_expand(recv, x, tok, w_gate, w_up, out, scaled_out, tile):
    rows = x.shape[0]
    added = summed(recv, 0, rows)
    tail = summed(recv, rows, 8)
    mean = as_column(tail[0:1], rows, (0, 1))
    gain = tail[1:2] + tail[2:3] + tail[3:4]
    centre = (tok[:, 0:1] + mean) / D
    centred = x[...] + added - centre
    scaled = centred * gain
    scaled_out[...] = scaled
    squares = as_row(in_pieces(jnp.sum(centred * centred, axis=1, keepdims=True), 2))
    scaled = scaled.astype(BF16)
    pieces = tile.shape[0] // (8 * rows)
    tiles = 3 * pieces
    columns = w_gate.shape[1]
    for k, weight in enumerate((w_gate, w_up)):
        part = jnp.dot(scaled, weight[...], preferred_element_type=F32)
        pad = jnp.zeros((rows, tiles * LANES - columns), F32)
        part = jnp.concatenate([part, pad], axis=1)
        for t in range(tiles):
            at = 8 * (t // 3) + 3 * k + t % 3
            tile[pl.ds(at, rows, stride=8 * pieces), :] = part[:, t * LANES : (t + 1) * LANES]
    for h in range(pieces):
        tile[pl.ds(8 * h + 6, rows, stride=8 * pieces), :] = jnp.broadcast_to(
            squares, (rows, LANES)
        )
        tile[pl.ds(8 * h + 7, rows, stride=8 * pieces), :] = jnp.zeros((rows, LANES), F32)
    for k in range(out.shape[0]):
        out[k] = tile[pl.ds(8 * k, 8), :].astype(BF16)


def k_hidden(recv, scaled, out, mid_out):
    rows = scaled.shape[0]
    total = summed(recv, 0, 8)
    spread = as_column(total[6:7], rows, (0, 1)) / D
    shrink = lax.rsqrt(spread + EPSILON)
    mid_out[...] = rounded(scaled[...] * shrink)
    mine = iota((rows, 1), 0) == kv_index() // (out.shape[0] // rows)
    own = jnp.sum(jnp.where(mine, shrink, 0.0), axis=0, keepdims=True)
    total = total * own
    up = pltpu.roll(total, 5, 0)
    hidden = total / (1.0 + jnp.exp(-total)) * up
    hidden = jnp.where(iota((8, LANES), 0) < 3, hidden, 0.0).astype(BF16)
    for k in range(out.shape[0]):
        out[k] = hidden


def k_shrink(recv, w_down, out, tile):
    rows = out.shape[1]
    pieces = recv.shape[0] // rows
    for k in range(recv.shape[0]):
        tile[pl.ds(8 * k, 8), :] = recv[k].astype(F32)
    part = jnp.zeros((rows, LANES), F32)
    columns = w_down.shape[0]
    for t in range(3 * pieces):
        at = 8 * (t // 3) + t % 3
        size = min(LANES, columns - t * LANES)
        hidden = tile[pl.ds(at, rows, stride=8 * pieces), :][:, :size].astype(BF16)
        part = part + jnp.dot(
            hidden, w_down[pl.ds(t * LANES, size), :], preferred_element_type=F32
        )
    part = part.astype(BF16)
    for k in range(out.shape[0]):
        out[k] = part


def k_sums(recv, mid, out, mix_out):
    rows, width = mid.shape
    mixture = mid[...] + summed(recv, 0, rows)
    mix_out[...] = mixture
    centre = jnp.sum(mixture, axis=1, keepdims=True) / width
    square = jnp.sum((mixture - centre) ** 2, axis=1, keepdims=True)
    message = as_row([centre, square])
    for k in range(out.shape[0]):
        out[k] = message


def k_finish(recv, mix, gain, out):
    rows, width = mix.shape
    devices = recv.shape[0]
    total = recv[0]
    for k in range(1, devices):
        total = total + recv[k]
    middle = total / devices
    spread = (recv[0] - middle) ** 2
    for k in range(1, devices):
        spread = spread + (recv[k] - middle) ** 2
    square = jnp.where(iota((1, LANES), 1) < rows, spread * width, total)
    centre = as_column(middle, rows, (0,))
    shrink = lax.rsqrt(as_column(square, rows, (0, 1)) / D + EPSILON)
    own = out.shape[1]
    scaled = (mix[...] - centre) * shrink
    scaled = pltpu.roll(scaled, width - lax.axis_index("tp") * own, 1)[:, :own]
    out[...] = (scaled * gain[...]).astype(BF16)


def on_device(
    tokens,
    live_lengths,
    kv_cache,
    gate_sums,
    w_query,
    w_key,
    w_value,
    w_forget,
    forget_bias,
    w_out,
    first_gain,
    w_gate,
    w_up,
    w_down,
    second_gain,
):
    rows, own = tokens.shape
    kv, tp = lax.axis_size(KV), lax.axis_size("tp")
    width = own * tp
    block = ((rows, LANES), F32)
    (message,) = kernel(
        k_tokens, [((tp, rows, width), BF16)], [VMEM], [pltpu.VMEM((rows, width), F32)]
    )(tokens)
    message, x = kernel(
        k_project,
        [((kv, 2 * rows + 8, LANES), BF16), block],
        [VMEM, VMEM, VMEM, VMEM, ANY, VMEM],
        [
            pltpu.VMEM((rows, LANES), F32),
            pltpu.VMEM((width, w_forget.shape[1]), BF16),
            pltpu.SemaphoreType.DMA,
        ],
    )(exchanged(message, "tp"), w_query, w_key, w_value, w_forget, w_out)
    message, tok, sums = kernel(
        k_attend,
        [((kv, 2 * rows + 8, LANES), BF16), block, ((2, LANES), F32)],
        [VMEM, SMEM, SMEM, VMEM, VMEM],
        [pltpu.VMEM((8 * rows, LANES), F32), pltpu.VMEM((8 * rows, LANES), F32)],
    )(exchanged(message, KV), live_lengths, forget_bias, kv_cache, gate_sums)
    (message,) = kernel(
        k_combine, [((tp, rows + 8, width), BF16)], [VMEM] * 4, [pltpu.VMEM((8, width), F32)]
    )(exchanged(message, KV), sums, w_out, first_gain[None])
    message, scaled = kernel(
        k_expand,
        [((kv, 8, LANES), BF16), block],
        [VMEM] * 5,
        [pltpu.VMEM((8 * kv, LANES), F32)],
    )(exchanged(message, "tp"), x, tok, w_gate, w_up)
    message, mid = kernel(k_hidden, [((kv, 8, LANES), BF16), block], [VMEM] * 2)(
        exchanged(message, KV), scaled
    )
    (message,) = kernel(
        k_shrink, [((tp, rows, width), BF16)], [VMEM] * 2, [pltpu.VMEM((8 * kv, LANES), F32)]
    )(exchanged(message, KV), w_down)
    message, mix = kernel(k_sums, [((kv, 1, LANES), F32), block], [VMEM] * 2)(
        exchanged(message, "tp"), mid
    )
    (out,) = kernel(k_finish, [((rows, own), BF16)], [VMEM] * 3)(
        exchanged(message, KV), mix, second_gain[None]
    )
    return out


def solution(mesh):
    split = Mesh(mesh.devices.reshape(8, 4, mesh.shape["tp"]), ("kv_0", "kv_1", "tp"))
    placed = (
        P(None, KV_TP),
        P(),
        P(None, KV, "tp"),
        P(None, "tp", KV),
        P(KV, "tp"),
        P(KV, "tp"),
        P(KV, "tp"),
        P(),
        P(),
        P("tp", KV),
        P(KV_TP),
        P(KV, "tp"),
        P(KV, "tp"),
        P("tp", KV),
        P(KV_TP),
    )
    return jax.shard_map(
        on_device, mesh=split, in_specs=placed, out_specs=P(None, KV_TP), check_vma=False
    )
```

time: 153 us -> 155 us (1.013)
  blocking collectives: 11.8 us -> 93.8 us
  waiting for transfers between devices: 66.3 us -> 9.53 us
  starting transfers between devices: 46.9 us -> 18.6 us
  Pallas kernels: 0 us -> 21.4 us
  other arithmetic: 9.97 us -> 0 us
  matrix products: 6.14 us -> 0 us
    all_to_all x1 -> x6, blocking collectives: 11.8 us -> 93.8 us  [exchanged(): return lax.all_to_all(pieces, axis, 0, 0, tiled=True)]
    all_to_all x7 -> x2, waiting for transfers between devices: 66.3 us -> 9.53 us  [exchanged(): return lax.all_to_all(pieces, axis, 0, 0, tiled=True)]
    all_to_all x7 -> x2, starting transfers between devices: 46.9 us -> 18.6 us  [exchanged(): return lax.all_to_all(pieces, axis, 0, 0, tiled=True)]
    pallas_call x0 -> x9, Pallas kernels: none -> 21.4 us  [the longest x1 6.59 us: on_device(): kernel(k_attend, [((kv, 2 * rows + 8, LANES), BF16), block, ((2, LANES),...]
    unnamed x21 -> x14, local copies, waits for them, and re-layouts: 1.08 us -> 9.35 us
    dot_general x11 -> x0, matrix products: 6.14 us -> none  [the longest x1 1.01 us: on_device(): query_part = jnp.dot(rows_bf, w_query, preferred_element_type=F32)]
    broadcast_in_dim x11 -> x0, local copies, waits for them, and re-layouts: 4.75 us -> none  [the longest x7 3.23 us: sent_to_all(): jnp.broadcast_to(shard[None], (devices, *shard.shape))]
    reduce_sum x15 -> x0, other arithmetic: 2.49 us -> none  [the longest x1 0.94 us: on_device(): out_part = jnp.sum(w_out.astype(F32), axis=1)]
  transfers between devices with their start and end apart: 7 -> 2, of which waited for: 7 -> 2; matrix products, arithmetic and copies ran while one was open for 1% -> 4% of each run, Pallas kernels for 0% -> 0%
where the time goes in v2:
time: 155 us; the launch traced here: 154 us
  blocking collectives  93.8 us (61%)
  Pallas kernels  21.4 us (14%)
  starting transfers between devices  18.6 us (12%)
  local copies, waits for them, and re-layouts  10.7 us (7%)
  waiting for transfers between devices  9.53 us (6%)
    all_to_all x6, blocking collectives, exchanged(): return lax.all_to_all(pieces, axis, 0, 0, tiled=True)  93.8 us
    all_to_all x2, starting transfers between devices, exchanged(): return lax.all_to_all(pieces, axis, 0, 0, tiled=True)  18.6 us
    all_to_all x2, waiting for transfers between devices, exchanged(): return lax.all_to_all(pieces, axis, 0, 0, tiled=True)  9.53 us
    unnamed x14, local copies, waits for them, and re-layouts  9.35 us
    pallas_call x1, Pallas kernels, on_device(): kernel(k_attend, [((kv, 2 * rows + 8, LANES), BF16), block, ((2, LANES),...  6.59 us
  transfers between devices with their start and end apart: 2, of which 2 were waited for; matrix products, arithmetic and copies ran while one was open for 4% of the time, Pallas kernels for 0%

profile of v2, /device:TPU:1, one launch (start us, length us, event | category | flops | bytes accessed | tf_op | source)
XLA Modules:
  0.0 154.1 jit_solution(14635525671658173968)
XLA Ops:
  0.0 1.3 copy.16.tokens
  1.3 1.4 shard_map.145
  2.7 10.1 %all-to-all-start = ((bf16[16,16,128]{2,1,0:T(8,128)(2,1)}), bf16[16,16,128]{2,1,0:T(8,128)(2,1)S(1)}, u32[]{:S(2)}, u32[]{:S(2)}) async-start(bf16[16,16,128]{2,1,0:T(8,128)(2,1)} %shard_map.145), calls=%async_computation | async-start | bytes 131072 | tf_op jit(solution)/shard_map/all_to_all | solution.py:35
  12.8 2.2 %copy.19.w_forget = bf16[4096,16]{1,0:T(8,128)(2,1)} copy(bf16[4096,16]{0,1:T(8,128)(2,1)} %param.22) | data formatting | bytes 262144 | tf_op args[7]
  15.1 1.4 copy.17.w_key
  16.5 1.4 copy.18.w_value
  17.9 2.7 %all-to-all-done.recv = bf16[16,16,128]{2,1,0:T(8,128)(2,1)S(1)} async-done(((bf16[16,16,128]{2,1,0:T(8,128)(2,1)}), bf16[16,16,128]{2,1,0:T(8,128)(2,1)S(1)}, u32[]{:S(2)}, u32[]{:S(2)}) %all-to-all-start) | async-done | bytes 65568 | tf_op jit(solution)/shard_map/all_to_all | solution.py:35
  20.7 0.0 copy-start.1
  20.7 0.6 copy-done.1
  21.3 2.7 %shard_map.146 = (bf16[32,40,128]{2,1,0:T(8,128)(2,1)}, f32[16,128]{1,0:T(8,128)}) custom-call(bf16[16,16,128]{2,1,0:T(8,128)(2,1)} %copy-done.1, bf16[128,256]{1,0:T(8,128)(2,1)} %w_query.1, bf16[128,64]{1,0:T(8,128)(2,1)} %copy.17.w_key, bf16[128,64]{1,0:T(8,128)(2,1)} %copy.18.w_value, bf16[4096,16]{1,0:T(8,128)(2,1)} %copy.19.w_forget, ...), custom_call_target="tpu_custom_call" | custom-call | tf_op jit(solution)/shard_map/pallas_call | solution.py:356
  24.0 0.0 copy-start.2
  24.0 24.6 %all_to_all.40.recv = bf16[32,40,128]{2,1,0:T(8,128)(2,1)} all-to-all(bf16[32,40,128]{2,1,0:T(8,128)(2,1)} %get-tuple-element.16), channel_id=1, replica_groups=mesh['kv_0'=8,'kv_1'=4,'tp'=16] {'kv_0','kv_1'}, dimensions={0} | all-to-all | bytes 655360 | tf_op jit(solution)/shard_map/all_to_all | solution.py:35
  48.6 6.6 %shard_map.147 = (bf16[32,40,128]{2,1,0:T(8,128)(2,1)}, f32[16,128]{1,0:T(8,128)}, f32[2,128]{1,0:T(2,128)}) custom-call(bf16[32,40,128]{2,1,0:T(8,128)(2,1)} %all_to_all.40.recv, s32[16]{0:T(128)} %lengths.1, f32[16]{0:T(128)} %bias.1, bf16[16,512,128]{2,1,0:T(8,128)(2,1)} %cache.1, f32[16,1,512]{2,1,0:T(1,128)} %gate.1), custom_call_target="tpu_custom_call" | custom-call | tf_op jit(solution)/shard_map/pallas_call | solution.py:366
  55.2 15.4 %all_to_all.41.recv = bf16[32,40,128]{2,1,0:T(8,128)(2,1)} all-to-all(bf16[32,40,128]{2,1,0:T(8,128)(2,1)} %get-tuple-element.17), channel_id=1, replica_groups=mesh['kv_0'=8,'kv_1'=4,'tp'=16] {'kv_0','kv_1'}, dimensions={0} | all-to-all | bytes 655360 | tf_op jit(solution)/shard_map/all_to_all | solution.py:35
  70.5 2.2 %shard_map.148 = bf16[16,24,128]{2,1,0:T(8,128)(2,1)} custom-call(bf16[32,40,128]{2,1,0:T(8,128)(2,1)} %all_to_all.41.recv, f32[2,128]{1,0:T(2,128)} %get-tuple-element.18.sums, bf16[256,128]{1,0:T(8,128)(2,1)} %w_out.3, f32[1,8]{1,0:T(1,128)} %bitcast.2), custom_call_target="tpu_custom_call" | custom-call | tf_op jit(solution)/shard_map/pallas_call | solution.py:372
  72.7 8.5 %all-to-all-start.3 = ((bf16[16,24,128]{2,1,0:T(8,128)(2,1)}), bf16[16,24,128]{2,1,0:T(8,128)(2,1)S(1)}, u32[]{:S(2)}, u32[]{:S(2)}) async-start(bf16[16,24,128]{2,1,0:T(8,128)(2,1)} %shard_map.148), calls=%async_computation.3 | async-start | bytes 196608 | tf_op jit(solution)/shard_map/all_to_all | solution.py:35
  81.2 0.0 copy-done.2
  81.2 0.8 copy.20.w_gate
  82.1 0.0 copy-done.3
  82.1 0.8 copy.21.w_up
  82.9 6.8 %all-to-all-done.3.recv = bf16[16,24,128]{2,1,0:T(8,128)(2,1)S(1)} async-done(((bf16[16,24,128]{2,1,0:T(8,128)(2,1)}), bf16[16,24,128]{2,1,0:T(8,128)(2,1)S(1)}, u32[]{:S(2)}, u32[]{:S(2)}) %all-to-all-start.3) | async-done | bytes 98336 | tf_op jit(solution)/shard_map/all_to_all | solution.py:35
  89.7 0.6 copy-done
  90.3 2.1 %shard_map.149 = (bf16[32,8,128]{2,1,0:T(8,128)(2,1)}, f32[16,128]{1,0:T(8,128)}) custom-call(bf16[16,24,128]{2,1,0:T(8,128)(2,1)} %copy-done, f32[16,128]{1,0:T(8,128)} %get-tuple-element.19.x, f32[16,128]{1,0:T(8,128)} %get-tuple-element.20.tok, bf16[128,704]{1,0:T(8,128)(2,1)} %copy.20.w_gate, bf16[128,704]{1,0:T(8,128)(2,1)} %copy.21.w_up), custom_call_target="tpu_custom_call" | custom-call | tf_op jit(solution)/shard_map/pallas_call | solution.py:375
  92.4 13.7 %all_to_all.42.recv = bf16[32,8,128]{2,1,0:T(8,128)(2,1)} all-to-all(bf16[32,8,128]{2,1,0:T(8,128)(2,1)} %get-tuple-element.21), channel_id=1, replica_groups=mesh['kv_0'=8,'kv_1'=4,'tp'=16] {'kv_0','kv_1'}, dimensions={0} | all-to-all | bytes 131072 | tf_op jit(solution)/shard_map/all_to_all | solution.py:35
  106.1 1.6 %shard_map.150 = (bf16[32,8,128]{2,1,0:T(8,128)(2,1)}, f32[16,128]{1,0:T(8,128)}) custom-call(bf16[32,8,128]{2,1,0:T(8,128)(2,1)} %all_to_all.42.recv, f32[16,128]{1,0:T(8,128)} %get-tuple-element.22.scaled), custom_call_target="tpu_custom_call" | custom-call | tf_op jit(solution)/shard_map/pallas_call | solution.py:381
  107.7 13.4 %all_to_all.43.recv = bf16[32,8,128]{2,1,0:T(8,128)(2,1)} all-to-all(bf16[32,8,128]{2,1,0:T(8,128)(2,1)} %get-tuple-element.23), channel_id=1, replica_groups=mesh['kv_0'=8,'kv_1'=4,'tp'=16] {'kv_0','kv_1'}, dimensions={0} | all-to-all | bytes 131072 | tf_op jit(solution)/shard_map/all_to_all | solution.py:35
  121.1 1.8 %shard_map.151 = bf16[16,16,128]{2,1,0:T(8,128)(2,1)} custom-call(bf16[32,8,128]{2,1,0:T(8,128)(2,1)} %all_to_all.43.recv, bf16[704,128]{1,0:T(8,128)(2,1)} %w_down.1), custom_call_target="tpu_custom_call" | custom-call | tf_op jit(solution)/shard_map/pallas_call | solution.py:384
  122.8 14.0 %all_to_all.44.recv = bf16[16,16,128]{2,1,0:T(8,128)(2,1)} all-to-all(bf16[16,16,128]{2,1,0:T(8,128)(2,1)} %shard_map.151), channel_id=1, replica_groups=mesh['kv_0'=8,'kv_1'=4,'tp'=16] {'tp'}, dimensions={0} | all-to-all | bytes 131072 | tf_op jit(solution)/shard_map/all_to_all | solution.py:35
  136.8 1.6 %shard_map.152 = (f32[32,1,128]{2,1,0:T(1,128)}, f32[16,128]{1,0:T(8,128)}) custom-call(bf16[16,16,128]{2,1,0:T(8,128)(2,1)} %all_to_all.44.recv, f32[16,128]{1,0:T(8,128)} %get-tuple-element.24.mid), custom_call_target="tpu_custom_call" | custom-call | tf_op jit(solution)/shard_map/pallas_call | solution.py:387
  138.4 12.8 %all_to_all.45.recv = f32[32,1,128]{2,1,0:T(1,128)} all-to-all(f32[32,1,128]{2,1,0:T(1,128)} %get-tuple-element.25), channel_id=1, replica_groups=mesh['kv_0'=8,'kv_1'=4,'tp'=16] {'kv_0','kv_1'}, dimensions={0} | all-to-all | bytes 32768 | tf_op jit(solution)/shard_map/all_to_all | solution.py:35
  151.2 1.6 %shard_map.153 = bf16[16,8]{1,0:T(8,128)(2,1)} custom-call(f32[32,1,128]{2,1,0:T(1,128)} %all_to_all.45.recv, f32[16,128]{1,0:T(8,128)} %get-tuple-element.26.mix, f32[1,8]{1,0:T(1,128)} %bitcast.3), custom_call_target="tpu_custom_call" | custom-call | tf_op jit(solution)/shard_map/pallas_call | solution.py:390
  152.8 1.3 copy.22
  (2 shorter events, 0.0 us)
Async XLA Ops:
  2.7 17.9 %all-to-all-start = ((bf16[16,16,128]{2,1,0:T(8,128)(2,1)}), bf16[16,16,128]{2,1,0:T(8,128)(2,1)S(1)}, u32[]{:S(2)}, u32[]{:S(2)}) async-start(bf16[16,16,128]{2,1,0:T(8,128)(2,1)} %shard_map.145), calls=%async_computation | async-start | bytes 131072 | tf_op jit(solution)/shard_map/all_to_all | solution.py:35
  20.7 0.6 copy-start.1
  24.0 57.2 %copy-start.2 = (bf16[128,704]{0,1:T(8,128)(2,1)S(1)}, bf16[128,704]{0,1:T(8,128)(2,1)}, u32[]{:S(2)}) copy-start(bf16[128,704]{0,1:T(8,128)(2,1)} %param.26) | copy-start | bytes 540676
  48.6 33.5 %copy-start.3 = (bf16[128,704]{0,1:T(8,128)(2,1)S(1)}, bf16[128,704]{0,1:T(8,128)(2,1)}, u32[]{:S(2)}) copy-start(bf16[128,704]{0,1:T(8,128)(2,1)} %param.27) | copy-start | bytes 540676
  72.7 17.0 %all-to-all-start.3 = ((bf16[16,24,128]{2,1,0:T(8,128)(2,1)}), bf16[16,24,128]{2,1,0:T(8,128)(2,1)S(1)}, u32[]{:S(2)}, u32[]{:S(2)}) async-start(bf16[16,24,128]{2,1,0:T(8,128)(2,1)} %shard_map.148), calls=%async_computation.3 | async-start | bytes 196608 | tf_op jit(solution)/shard_map/all_to_all | solution.py:35
  89.7 0.6 copy-start

commit v3 on v2

--- a/solution.py
+++ b/solution.py
@@ -24,10 +24,11 @@
 def kernel(body, outs, specs, scratch=()):
     return pl.pallas_call(
         body,
-        out_shape=[jax.ShapeDtypeStruct(shape, dtype) for shape, dtype in outs],
+        out_shape=[pltpu.VMEM(shape, dtype) for shape, dtype in outs],
         in_specs=specs,
         out_specs=[VMEM] * len(outs),
         scratch_shapes=scratch,
+        compiler_params=pltpu.CompilerParams(vmem_limit_bytes=8 * 2**20),
     )
 
 
@@ -60,6 +61,14 @@
     return iota((rows, LANES), 1) == iota((rows, LANES), 0) + rows * turn
 
 
+def across(left, right, sides):
+    return lax.dot_general(left, right, (sides, ((), ())), preferred_element_type=F32)
+
+
+LAST = ((1,), (1,))
+FIRST = ((0,), (0,))
+
+
 def as_row(columns):
     rows = columns[0].shape[0]
     tile = jnp.zeros((rows, LANES), F32)
@@ -82,36 +91,25 @@
     return total
 
 
-def k_tokens(tokens, out, tile):
-    own = tokens.shape[1]
-    tile[...] = jnp.zeros(tile.shape, F32)
-    tile[:, :own] = tokens[...].astype(F32)
-    placed = pltpu.roll(tile[...], lax.axis_index("tp") * own, 1).astype(BF16)
-    for k in range(out.shape[0]):
-        out[k] = placed
-
-
 def k_project(recv, w_query, w_key, w_value, w_forget, w_out, out, x_out, new_rows, wf, sem):
     rows = recv.shape[1]
-    width = wf.shape[0]
+    width = wf.shape[1]
     start = pl.multiple_of(kv_index() * width, width)
-    copy = pltpu.make_async_copy(w_forget.at[pl.ds(start, width)], wf, sem)
+    copy = pltpu.make_async_copy(w_forget.at[:, pl.ds(start, width)], wf, sem)
     copy.start()
-    x = summed(recv, 0, rows)
+    same = jnp.where(iota((width, width), 0) == iota((width, width), 1), 1.0, 0.0).astype(BF16)
+    x = across(recv[...], same, FIRST)
     x_out[...] = x
+    rows = x.shape[0]
     xb = x.astype(BF16)
     query = jnp.dot(xb, w_query[...], preferred_element_type=F32)
-    key = jnp.dot(xb, w_key[...], preferred_element_type=F32)
-    value = jnp.dot(xb, w_value[...], preferred_element_type=F32)
-    new_rows[:, :DH] = key
-    new_rows[:, DH:] = value
-    out_sums = lax.dot_general(
-        jnp.ones((8, LANES), BF16), w_out[...], (((1,), (1,)), ((), ())), preferred_element_type=F32
-    )
+    new_rows[:, :DH] = across(xb, w_key[...], LAST)
+    new_rows[:, DH:] = across(xb, w_value[...], LAST)
+    out_sums = across(jnp.ones((8, LANES), BF16), w_out[...], LAST)
     sums_hi, sums_lo = in_pieces(out_sums, 2)
     token_col = jnp.sum(x, axis=1, keepdims=True)
     copy.wait()
-    forget = jnp.dot(xb, wf[...], preferred_element_type=F32)
+    forget = across(xb, wf[...], LAST)
     mine = iota(forget.shape, 1) == lax.axis_index("tp")
     forget_col = jnp.sum(jnp.where(mine, forget, 0.0), axis=1, keepdims=True)
     small = as_row([*in_pieces(forget_col, 2), *in_pieces(token_col, 2)])
@@ -247,9 +245,9 @@
     scaled = scaled.astype(BF16)
     pieces = tile.shape[0] // (8 * rows)
     tiles = 3 * pieces
-    columns = w_gate.shape[1]
+    columns = w_gate.shape[0]
     for k, weight in enumerate((w_gate, w_up)):
-        part = jnp.dot(scaled, weight[...], preferred_element_type=F32)
+        part = across(scaled, weight[...], LAST)
         pad = jnp.zeros((rows, tiles * LANES - columns), F32)
         part = jnp.concatenate([part, pad], axis=1)
         for t in range(tiles):
@@ -310,7 +308,7 @@
         out[k] = message
 
 
-def k_finish(recv, mix, gain, out):
+def k_finish(recv, mix, gain, out, turned):
     rows, width = mix.shape
     devices = recv.shape[0]
     total = recv[0]
@@ -323,10 +321,12 @@
     square = jnp.where(iota((1, LANES), 1) < rows, spread * width, total)
     centre = as_column(middle, rows, (0,))
     shrink = lax.rsqrt(as_column(square, rows, (0, 1)) / D + EPSILON)
-    own = out.shape[1]
-    scaled = (mix[...] - centre) * shrink
-    scaled = pltpu.roll(scaled, width - lax.axis_index("tp") * own, 1)[:, :own]
-    out[...] = (scaled * gain[...]).astype(BF16)
+    own = out.shape[0]
+    scaled = ((mix[...] - centre) * shrink).T
+    at = pl.multiple_of(lax.axis_index("tp") * own, own)
+    turned[...] = scaled
+    gain_col = jnp.sum(jnp.where(diagonal(own, 0)[:, :own], gain[...], 0.0), axis=1, keepdims=True)
+    out[...] = (turned[pl.ds(at, own), :] * gain_col).astype(BF16)
 
 
 def on_device(
@@ -350,19 +350,24 @@
     kv, tp = lax.axis_size(KV), lax.axis_size("tp")
     width = own * tp
     block = ((rows, LANES), F32)
-    (message,) = kernel(
-        k_tokens, [((tp, rows, width), BF16)], [VMEM], [pltpu.VMEM((rows, width), F32)]
-    )(tokens)
+    message = jnp.broadcast_to(tokens.T[None], (tp, own, rows))
     message, x = kernel(
         k_project,
         [((kv, 2 * rows + 8, LANES), BF16), block],
         [VMEM, VMEM, VMEM, VMEM, ANY, VMEM],
         [
             pltpu.VMEM((rows, LANES), F32),
-            pltpu.VMEM((width, w_forget.shape[1]), BF16),
+            pltpu.VMEM((w_forget.shape[1], width), BF16),
             pltpu.SemaphoreType.DMA,
         ],
-    )(exchanged(message, "tp"), w_query, w_key, w_value, w_forget, w_out)
+    )(
+        exchanged(message, "tp").reshape(width, rows),
+        w_query,
+        w_key.T,
+        w_value.T,
+        w_forget.T,
+        w_out,
+    )
     message, tok, sums = kernel(
         k_attend,
         [((kv, 2 * rows + 8, LANES), BF16), block, ((2, LANES), F32)],
@@ -377,7 +382,7 @@
         [((kv, 8, LANES), BF16), block],
         [VMEM] * 5,
         [pltpu.VMEM((8 * kv, LANES), F32)],
-    )(exchanged(message, "tp"), x, tok, w_gate, w_up)
+    )(exchanged(message, "tp"), x, tok, w_gate.T, w_up.T)
     message, mid = kernel(k_hidden, [((kv, 8, LANES), BF16), block], [VMEM] * 2)(
         exchanged(message, KV), scaled
     )
@@ -387,10 +392,10 @@
     message, mix = kernel(k_sums, [((kv, 1, LANES), F32), block], [VMEM] * 2)(
         exchanged(message, "tp"), mid
     )
-    (out,) = kernel(k_finish, [((rows, own), BF16)], [VMEM] * 3)(
-        exchanged(message, KV), mix, second_gain[None]
-    )
-    return out
+    (out,) = kernel(
+        k_finish, [((own, rows), BF16)], [VMEM] * 3, [pltpu.VMEM((width, rows), F32)]
+    )(exchanged(message, KV), mix, second_gain[None])
+    return out.T
 
 
 def solution(mesh):

time: 155 us -> 138 us (0.89)
  blocking collectives: 93.8 us -> 121 us
  starting transfers between devices: 18.6 us -> 0 us
  Pallas kernels: 21.4 us -> 7.02 us
  waiting for transfers between devices: 9.53 us -> 0 us
  local copies, waits for them, and re-layouts: 10.7 us -> 8.97 us
    all_to_all x6 -> x8, blocking collectives: 93.8 us -> 121 us  [exchanged(): return lax.all_to_all(pieces, axis, 0, 0, tiled=True)]
    all_to_all x2 -> x0, starting transfers between devices: 18.6 us -> none  [exchanged(): return lax.all_to_all(pieces, axis, 0, 0, tiled=True)]
    all_to_all x2 -> x0, waiting for transfers between devices: 9.53 us -> none  [exchanged(): return lax.all_to_all(pieces, axis, 0, 0, tiled=True)]
    pallas_call x2 -> x1, Pallas kernels: 2.93 us -> 0.25 us  [on_device(): kernel(k_finish, [((own, rows), BF16)], [VMEM] * 3, [pltpu.VMEM((width, r...]
    pallas_call x1, Pallas kernels: 2.7 us -> 0.6 us  [on_device(): kernel(k_project, [((kv, 2 * rows + 8, LANES), BF16), block], [VMEM, VMEM...]
    pallas_call x1, Pallas kernels: 6.59 us -> 4.75 us  [on_device(): kernel(k_attend, [((kv, 2 * rows + 8, LANES), BF16), block, ((2, LANES),...]
    pallas_call x1, Pallas kernels: 2.06 us -> 0.39 us  [on_device(): kernel(k_expand, [((kv, 8, LANES), BF16), block], [VMEM] * 5, [pltpu.VMEM...]
    pallas_call x1, Pallas kernels: 2.16 us -> 0.53 us  [on_device(): kernel(k_combine, [((tp, rows + 8, width), BF16)], [VMEM] * 4, [pltpu.VME...]
  transfers between devices with their start and end apart: 2 -> 0, of which waited for: 2 -> 0; matrix products, arithmetic and copies ran while one was open for 4% -> 0% of each run, Pallas kernels for 0% -> 0%
where the time goes in v3:
time: 138 us; the launch traced here: 137 us
  blocking collectives  121 us (88%)
  local copies, waits for them, and re-layouts  8.97 us (7%)
  Pallas kernels  7.02 us (5%)
    all_to_all x8, blocking collectives, exchanged(): return lax.all_to_all(pieces, axis, 0, 0, tiled=True)  121 us
    unnamed x31, local copies, waits for them, and re-layouts  8.28 us
    pallas_call x1, Pallas kernels, on_device(): kernel(k_attend, [((kv, 2 * rows + 8, LANES), BF16), block, ((2, LANES),...  4.75 us

profile of v3, /device:TPU:1, one launch (start us, length us, event | category | flops | bytes accessed | tf_op | source)
XLA Modules:
  0.0 136.8 jit_solution(14602433436662880861)
XLA Ops:
  0.0 0.7 broadcast_in_dim.12
  0.7 16.8 %all_to_all.40 = bf16[16,8,16]{2,1,0:T(8,128)(2,1)S(1)} all-to-all(bf16[16,8,16]{2,1,0:T(8,128)(2,1)S(1)} %broadcast_in_dim.12), channel_id=1, replica_groups=mesh['kv_0'=8,'kv_1'=4,'tp'=16] {'tp'}, dimensions={0} | all-to-all | bytes 8192 | tf_op jit(solution)/shard_map/all_to_all | solution.py:36
  17.5 0.8 copy-done.1
  18.4 0.9 copy-done.6
  19.3 0.8 copy-done.7
  20.1 0.7 copy-done.9
  20.8 0.7 copy-done.10
  21.6 0.6 shard_map.145
  22.2 0.0 copy-start.4
  22.2 0.0 copy-start.5
  22.2 24.7 %all_to_all.41.recv = bf16[32,40,128]{2,1,0:T(8,128)(2,1)S(1)} all-to-all(bf16[32,40,128]{2,1,0:T(8,128)(2,1)S(1)} %get-tuple-element.16), channel_id=1, replica_groups=mesh['kv_0'=8,'kv_1'=4,'tp'=16] {'kv_0','kv_1'}, dimensions={0} | all-to-all | bytes 655360 | tf_op jit(solution)/shard_map/all_to_all | solution.py:36
  46.8 1.6 %copy-done = bf16[16,512,128]{2,1,0:T(8,128)(2,1)S(1)} copy-done((bf16[16,512,128]{2,1,0:T(8,128)(2,1)S(1)}, bf16[16,512,128]{2,1,0:T(8,128)(2,1)}, u32[]{:S(2)}) %copy-start) | copy-done | bytes 2097176
  48.4 0.8 copy-done.8
  49.2 0.7 copy-done.11
  49.9 0.7 copy-done.12
  50.5 4.8 %shard_map.146 = (bf16[32,40,128]{2,1,0:T(8,128)(2,1)S(1)}, f32[16,128]{1,0:T(8,128)S(1)}, f32[2,128]{1,0:T(2,128)S(1)}) custom-call(bf16[32,40,128]{2,1,0:T(8,128)(2,1)S(1)} %all_to_all.41.recv, s32[16]{0:T(128)S(1)} %copy-done.11, f32[16]{0:T(128)S(1)} %copy-done.12, bf16[16,512,128]{2,1,0:T(8,128)(2,1)S(1)} %copy-done, f32[16,1,512]{2,1,0:T(1,128)S(1)} %copy-done.8), custom_call_target="tpu_custom_call" | custom-call | tf_op jit(solution)/shard_map/pallas_call | solution.py:371
  55.3 16.2 %all_to_all.42.recv = bf16[32,40,128]{2,1,0:T(8,128)(2,1)S(1)} all-to-all(bf16[32,40,128]{2,1,0:T(8,128)(2,1)S(1)} %get-tuple-element.17), channel_id=1, replica_groups=mesh['kv_0'=8,'kv_1'=4,'tp'=16] {'kv_0','kv_1'}, dimensions={0} | all-to-all | bytes 655360 | tf_op jit(solution)/shard_map/all_to_all | solution.py:36
  71.4 0.0 copy-done.2
  71.4 0.0 copy-done.13
  71.4 0.5 shard_map.147
  72.0 14.2 %all_to_all.43.recv = bf16[16,24,128]{2,1,0:T(8,128)(2,1)S(1)} all-to-all(bf16[16,24,128]{2,1,0:T(8,128)(2,1)S(1)} %shard_map.147), channel_id=1, replica_groups=mesh['kv_0'=8,'kv_1'=4,'tp'=16] {'tp'}, dimensions={0} | all-to-all | bytes 196608 | tf_op jit(solution)/shard_map/all_to_all | solution.py:36
  86.2 0.0 copy-done.4
  86.2 0.4 shard_map.148
  86.6 12.6 %all_to_all.44.recv = bf16[32,8,128]{2,1,0:T(8,128)(2,1)S(1)} all-to-all(bf16[32,8,128]{2,1,0:T(8,128)(2,1)S(1)} %get-tuple-element.21), channel_id=1, replica_groups=mesh['kv_0'=8,'kv_1'=4,'tp'=16] {'kv_0','kv_1'}, dimensions={0} | all-to-all | bytes 131072 | tf_op jit(solution)/shard_map/all_to_all | solution.py:36
  99.2 0.1 shard_map.149
  99.3 11.9 %all_to_all.45.recv = bf16[32,8,128]{2,1,0:T(8,128)(2,1)S(1)} all-to-all(bf16[32,8,128]{2,1,0:T(8,128)(2,1)S(1)} %get-tuple-element.23), channel_id=1, replica_groups=mesh['kv_0'=8,'kv_1'=4,'tp'=16] {'kv_0','kv_1'}, dimensions={0} | all-to-all | bytes 131072 | tf_op jit(solution)/shard_map/all_to_all | solution.py:36
  111.3 0.2 shard_map.150
  111.4 12.7 %all_to_all.46.recv = bf16[16,16,128]{2,1,0:T(8,128)(2,1)S(1)} all-to-all(bf16[16,16,128]{2,1,0:T(8,128)(2,1)S(1)} %shard_map.150), channel_id=1, replica_groups=mesh['kv_0'=8,'kv_1'=4,'tp'=16] {'tp'}, dimensions={0} | all-to-all | bytes 131072 | tf_op jit(solution)/shard_map/all_to_all | solution.py:36
  124.1 0.2 shard_map.151
  124.3 11.6 %all_to_all.47.recv = f32[32,1,128]{2,1,0:T(1,128)S(1)} all-to-all(f32[32,1,128]{2,1,0:T(1,128)S(1)} %get-tuple-element.25), channel_id=1, replica_groups=mesh['kv_0'=8,'kv_1'=4,'tp'=16] {'kv_0','kv_1'}, dimensions={0} | all-to-all | bytes 32768 | tf_op jit(solution)/shard_map/all_to_all | solution.py:36
  135.9 0.2 shard_map.152
  136.2 0.6 copy.16
  (16 shorter events, 0.0 us)
Async XLA Ops:
  0.7 70.8 %copy-start.2 = (bf16[256,128]{1,0:T(8,128)(2,1)S(1)}, bf16[256,128]{1,0:T(8,128)(2,1)}, u32[]{:S(2)}) copy-start(bf16[256,128]{1,0:T(8,128)(2,1)} %w_out.3) | copy-start | bytes 196612
  0.7 70.8 %copy-start.13 = (f32[8]{0:T(128)S(1)}, f32[8]{0:T(128)}, u32[]{:S(2)}) copy-start(f32[8]{0:T(128)} %param.25) | copy-start | bytes 100
  17.5 0.8 copy-start.1
  18.4 0.9 copy-start.6
  19.3 0.8 copy-start.7
  20.1 0.7 copy-start.9
  20.8 0.7 copy-start.10
  22.2 64.0 %copy-start.4 = (bf16[128,704]{0,1:T(8,128)(2,1)S(1)}, bf16[128,704]{0,1:T(8,128)(2,1)}, u32[]{:S(2)}) copy-start(bf16[128,704]{0,1:T(8,128)(2,1)} %param.26) | copy-start | bytes 540676
  22.2 64.0 %copy-start.5 = (bf16[128,704]{0,1:T(8,128)(2,1)S(1)}, bf16[128,704]{0,1:T(8,128)(2,1)}, u32[]{:S(2)}) copy-start(bf16[128,704]{0,1:T(8,128)(2,1)} %param.27) | copy-start | bytes 540676
  46.8 1.6 %copy-start = (bf16[16,512,128]{2,1,0:T(8,128)(2,1)S(1)}, bf16[16,512,128]{2,1,0:T(8,128)(2,1)}, u32[]{:S(2)}) copy-start(bf16[16,512,128]{2,1,0:T(8,128)(2,1)} %cache.1) | copy-start | bytes 6291460
  48.4 0.8 copy-start.8
  49.2 0.7 copy-start.11
  49.9 0.7 copy-start.12
  50.5 60.8 %copy-start.3 = (bf16[704,128]{1,0:T(8,128)(2,1)S(1)}, bf16[704,128]{1,0:T(8,128)(2,1)}, u32[]{:S(2)}) copy-start(bf16[704,128]{1,0:T(8,128)(2,1)} %w_down.1) | copy-start | bytes 540676
  50.5 85.4 %copy-start.14 = (f32[8]{0:T(128)S(1)}, f32[8]{0:T(128)}, u32[]{:S(2)}) copy-start(f32[8]{0:T(128)} %param.29) | copy-start | bytes 100

commit v4 on v3

--- a/solution.py
+++ b/solution.py
@@ -1,3 +1,5 @@
+import functools
+
 import jax
 import jax.numpy as jnp
 from jax import lax
@@ -21,10 +23,13 @@
 ANY = pl.BlockSpec(memory_space=pl.ANY)
 
 
-def kernel(body, outs, specs, scratch=()):
+def kernel(body, outs, specs, scratch=(), last=False):
     return pl.pallas_call(
         body,
-        out_shape=[pltpu.VMEM(shape, dtype) for shape, dtype in outs],
+        out_shape=[
+            jax.ShapeDtypeStruct(shape, dtype) if last else pltpu.VMEM(shape, dtype)
+            for shape, dtype in outs
+        ],
         in_specs=specs,
         out_specs=[VMEM] * len(outs),
         scratch_shapes=scratch,
@@ -91,12 +96,38 @@
     return total
 
 
-def k_project(recv, w_query, w_key, w_value, w_forget, w_out, out, x_out, new_rows, wf, sem):
-    rows = recv.shape[1]
+def k_weights(query, key, value, forget, w_out, gain, bias, query_o, key_o, value_o, forget_o, w_out_o, tail_o, sem):
+    width = forget_o.shape[1]
+    start = pl.multiple_of(kv_index() * width, width)
+    pairs = [(w_out, w_out_o), (query, query_o), (key, key_o), (value, value_o)]
+    pairs.append((forget.at[:, pl.ds(start, width)], forget_o))
+    copies = [pltpu.make_async_copy(a, b, sem.at[k]) for k, (a, b) in enumerate(pairs)]
+    for copy in copies:
+        copy.start()
+    own = gain.shape[1]
+    spread = jnp.where(iota((own, LANES), 1) == iota((own, LANES), 0) + lax.axis_index("tp") * own, 1.0, 0.0)
+    column = jnp.sum(jnp.where(diagonal(own, 0)[:, :own], gain[...], 0.0), axis=1, keepdims=True)
+    gains = in_pieces(jnp.sum(spread * column, axis=0, keepdims=True), 3)
+    row = iota((8, LANES), 0)
+    for copy in copies:
+        copy.wait()
+    sums = across(jnp.ones((8, LANES), BF16), w_out_o[...], LAST)
+    sums_hi, sums_lo = in_pieces(sums, 2)
+    tail = jnp.where(row == 2, sums_hi[:, :LANES], 0.0)
+    tail = jnp.where(row == 3, sums_hi[:, LANES:], tail)
+    tail = jnp.where(row == 4, sums_lo[:, :LANES], tail)
+    tail_o[0] = jnp.where(row == 5, sums_lo[:, LANES:], tail)
+    mine = iota(bias.shape, 1) == lax.axis_index("tp")
+    once = jnp.where(kv_index() == 0, 1.0, 0.0)
+    own_bias = jnp.sum(jnp.where(mine, bias[...], 0.0), axis=1, keepdims=True) * once
+    tail = jnp.where(row == 0, own_bias, 0.0)
+    for k, piece in enumerate(gains):
+        tail = jnp.where(row == 1 + k, piece, tail)
+    tail_o[1] = tail
+
+
+def k_project(recv, w_query, w_key, w_value, wf, tails, out, x_out, new_rows):
     width = wf.shape[1]
-    start = pl.multiple_of(kv_index() * width, width)
-    copy = pltpu.make_async_copy(w_forget.at[:, pl.ds(start, width)], wf, sem)
-    copy.start()
     same = jnp.where(iota((width, width), 0) == iota((width, width), 1), 1.0, 0.0).astype(BF16)
     x = across(recv[...], same, FIRST)
     x_out[...] = x
@@ -105,20 +136,14 @@
     query = jnp.dot(xb, w_query[...], preferred_element_type=F32)
     new_rows[:, :DH] = across(xb, w_key[...], LAST)
     new_rows[:, DH:] = across(xb, w_value[...], LAST)
-    out_sums = across(jnp.ones((8, LANES), BF16), w_out[...], LAST)
-    sums_hi, sums_lo = in_pieces(out_sums, 2)
+    forget = across(xb, wf[...], LAST)
     token_col = jnp.sum(x, axis=1, keepdims=True)
-    copy.wait()
-    forget = across(xb, wf[...], LAST)
     mine = iota(forget.shape, 1) == lax.axis_index("tp")
     forget_col = jnp.sum(jnp.where(mine, forget, 0.0), axis=1, keepdims=True)
+    forget_col = forget_col + tails[1, 0:1, 0:1]
     small = as_row([*in_pieces(forget_col, 2), *in_pieces(token_col, 2)])
     row = iota((8, LANES), 0)
-    tail = jnp.where(row == 1, small, 0.0)
-    tail = jnp.where(row == 2, sums_hi[:, :LANES], tail)
-    tail = jnp.where(row == 3, sums_hi[:, LANES:], tail)
-    tail = jnp.where(row == 4, sums_lo[:, :LANES], tail)
-    tail = jnp.where(row == 5, sums_lo[:, LANES:], tail)
+    tail = jnp.where(row == 1, small, tails[0])
     left = query[:, :LANES].astype(BF16)
     right = query[:, LANES:].astype(BF16)
     for b in range(rows):
@@ -129,9 +154,28 @@
             out[k, pl.ds(2 * rows, 8)] = own_tail
 
 
-def k_attend(recv, lengths, bias, cache, gate, out, tok_out, sums_out, qs, os):
+def k_prepare(lengths, cache, gate, cache_o, keys_o, gate_o, gate_v, sem, gate_sem):
+    rows, positions = cache.shape[:2]
+    copies = [pltpu.make_async_copy(cache.at[b], cache_o.at[b], sem.at[b]) for b in range(rows)]
+    gates = pltpu.make_async_copy(gate, gate_v, gate_sem)
+    gates.start()
+    for copy in copies:
+        copy.start()
+    gates.wait()
+    place = kv_index() * positions + iota((8, positions), 1)
+    first = iota((8, positions), 0) < 4
+    for m in range(rows // 2):
+        one = jnp.where(place < lengths[2 * m], gate_v[2 * m], EMPTY_SCORE)
+        two = jnp.where(place < lengths[2 * m + 1], gate_v[2 * m + 1], EMPTY_SCORE)
+        gate_o[m] = jnp.where(first, one, two)
+    for b in range(rows):
+        copies[b].wait()
+        keys_o[b // 2, pl.ds(DH * (b % 2), DH), :] = cache_o[b].T[:DH]
+
+
+def k_attend(recv, cache, keys, gate, out, tok_out, sums_out, qs, os):
     rows = cache.shape[0]
-    positions = cache.shape[1]
+    heads = 4
     scale = DH**-0.5
     left = rounded(summed(recv, 0, rows))
     right = rounded(summed(recv, rows, rows))
@@ -141,43 +185,55 @@
     sums_out[0:1, :] = tail[2:3] + tail[4:5]
     sums_out[1:2, :] = tail[3:4] + tail[5:6]
     tok_out[...] = jnp.broadcast_to(as_column(small, rows, (2, 3)), tok_out.shape)
-    fetched = as_column(small, rows, (0, 1)) + bias[lax.axis_index("tp")]
+    even = iota((rows, LANES), 0) % 2 == 0
+    low = iota((rows, LANES), 1) < DH
+    keep = even == low
+    left_turned = pltpu.roll(left, DH, 1)
+    right_turned = pltpu.roll(right, DH, 1)
+    placed = (
+        jnp.where(even, left, left_turned),
+        jnp.where(even, left_turned, left),
+        jnp.where(even, right, right_turned),
+        jnp.where(even, right_turned, right),
+    )
+    for h, block in enumerate(placed):
+        qs[pl.ds(h, rows, stride=heads), :] = jnp.where(keep, block, 0.0)
+    all_rows = rows * heads
+    owner = iota((all_rows, LANES), 0) // heads
+    lane = iota((all_rows, LANES), 1)
+    fetched = jnp.where((lane == owner) | (lane == owner + rows), small, 0.0)
+    fetched = jnp.sum(fetched, axis=1, keepdims=True)
     new_gate = jnp.minimum(fetched, 0.0) - jnp.log(1.0 + jnp.exp(-jnp.abs(fetched)))
-    low = iota((rows, LANES), 1) < DH
-    qs[pl.ds(0, rows)] = jnp.where(low, left, 0.0)
-    qs[pl.ds(rows, rows)] = jnp.where(low, pltpu.roll(left, DH, 1), 0.0)
-    qs[pl.ds(2 * rows, rows)] = jnp.where(low, right, 0.0)
-    qs[pl.ds(3 * rows, rows)] = jnp.where(low, pltpu.roll(right, DH, 1), 0.0)
-    qs[pl.ds(4 * rows, 4 * rows)] = jnp.zeros((4 * rows, LANES), F32)
-    me = kv_index()
-    place = me * positions + iota((8, positions), 1)
+    lane = iota((1, LANES), 1)
+    new_key = jnp.where(lane < DH, new_row, pltpu.roll(jnp.broadcast_to(new_row, (8, LANES)), DH, 1)[0:1])
+    own = jnp.sum(qs[...] * new_key, axis=1, keepdims=True) * scale
+    mine = iota((all_rows, 1), 0) // heads == kv_index()
+    own = jnp.where(mine, own, EMPTY_SCORE)
     lane = iota((8, LANES), 1)
-    for b in range(rows):
-        query = qs[pl.ds(b, 8, stride=rows), :]
-        block = cache[b]
-        scores = lax.dot_general(
-            query.astype(BF16), block, (((1,), (1,)), ((), ())), preferred_element_type=F32
+    first = iota((8, LANES), 0) < heads
+    for m in range(rows // 2):
+        at = slice(8 * m, 8 * m + 8)
+        scores = jnp.dot(
+            qs[pl.ds(8 * m, 8), :].astype(BF16), keys[m], preferred_element_type=F32
         )
-        scores = scores * scale + (gate[b] + new_gate[b : b + 1])
-        live = place < lengths[b]
-        own = jnp.sum(query * new_row, axis=1, keepdims=True) * scale
-        own = jnp.where(me == b, own, EMPTY_SCORE)
-        top = jnp.max(jnp.where(live, scores, EMPTY_SCORE), axis=1, keepdims=True)
-        top = jnp.maximum(top, own)
-        weights = jnp.where(live, jnp.exp(scores - top), 0.0)
-        own_weight = jnp.where(me == b, jnp.exp(own - top), 0.0)
+        scores = scores * scale + (gate[m] + new_gate[at])
+        top = jnp.maximum(jnp.max(scores, axis=1, keepdims=True), own[at])
+        top = jnp.maximum(top, 0.1 * EMPTY_SCORE)
+        weights = jnp.exp(scores - top)
+        own_weight = jnp.exp(own[at] - top)
         total = jnp.sum(weights, axis=1, keepdims=True) + own_weight
+        block = jnp.concatenate([cache[2 * m], cache[2 * m + 1]], axis=1)
         value = jnp.dot(weights.astype(BF16), block, preferred_element_type=F32)
+        value = jnp.where(first, value[:, :LANES], value[:, LANES:])
         value = value + rounded(own_weight) * new_row
-        value = jnp.where(lane == 0, top, jnp.where(lane == 1, total, value))
-        os[pl.ds(b, 8, stride=rows), :] = value
-    heads = [os[pl.ds(h * rows, rows)] for h in range(4)]
-    low_out = jnp.where(low, pltpu.roll(heads[0], DH, 1), heads[1]).astype(BF16)
-    high_out = jnp.where(low, pltpu.roll(heads[2], DH, 1), heads[3]).astype(BF16)
+        os[pl.ds(8 * m, 8), :] = jnp.where(lane == 0, top, jnp.where(lane == 1, total, value))
+    blocks = [os[pl.ds(h, rows, stride=heads), :] for h in range(heads)]
+    low_out = jnp.where(low, pltpu.roll(blocks[0], DH, 1), blocks[1]).astype(BF16)
+    high_out = jnp.where(low, pltpu.roll(blocks[2], DH, 1), blocks[3]).astype(BF16)
     lane = iota((rows, LANES), 1)
     stats = jnp.zeros((rows, LANES), F32)
-    for h in range(4):
-        pieces = [*in_pieces(heads[h][:, 0:1], 3), *in_pieces(heads[h][:, 1:2], 2)]
+    for h in range(heads):
+        pieces = [*in_pieces(blocks[h][:, 0:1], 3), *in_pieces(blocks[h][:, 1:2], 2)]
         for k, piece in enumerate(pieces):
             stats = jnp.where(lane == 8 * h + k, piece, stats)
     stats = (stats[:8] + pltpu.roll(stats[8:], 32, 1)).astype(BF16)
@@ -187,7 +243,7 @@
         out[k, pl.ds(2 * rows, 8)] = stats
 
 
-def k_combine(recv, sums, w_out, gain, out, tile):
+def k_combine(recv, sums, w_out, tails, out):
     devices = recv.shape[0]
     rows = (recv.shape[1] - 8) // 2
     heads = 4 * DH
@@ -217,14 +273,8 @@
     wide = attended.astype(F32)
     mean = wide[:, :LANES] * sums[0:1, :] + wide[:, LANES:] * sums[1:2, :]
     mean_row = as_row(in_pieces(jnp.sum(mean, axis=1, keepdims=True), 2))
-    own = gain.shape[1]
-    tile[...] = jnp.zeros(tile.shape, F32)
-    tile[0:1, :own] = gain[...]
-    gains = in_pieces(pltpu.roll(tile[...], lax.axis_index("tp") * own, 1)[0:1], 3)
     row = iota((8, LANES), 0)
-    tail = jnp.where(row == 0, mean_row, 0.0)
-    for k, piece in enumerate(gains):
-        tail = jnp.where(row == 1 + k, piece, tail)
+    tail = jnp.where(row == 0, mean_row, tails[1])
     tail = tail.astype(BF16)
     for k in range(out.shape[0]):
         out[k, pl.ds(0, rows)] = attn_part
@@ -351,32 +401,61 @@
     width = own * tp
     block = ((rows, LANES), F32)
     message = jnp.broadcast_to(tokens.T[None], (tp, own, rows))
+    in_hbm = functools.partial(pltpu.with_memory_space_constraint, memory_space=pltpu.HBM)
+    recv = exchanged(message, "tp").reshape(width, rows)
+    heads = w_query.shape[1]
+    w_query, w_key, w_value, w_forget, w_out, tails = kernel(
+        k_weights,
+        [
+            ((width, heads), BF16),
+            ((DH, width), BF16),
+            ((DH, width), BF16),
+            ((w_forget.shape[1], width), BF16),
+            ((heads, width), BF16),
+            ((2, 8, LANES), F32),
+        ],
+        [ANY] * 5 + [VMEM] * 2,
+        [pltpu.SemaphoreType.DMA((5,))],
+    )(
+        in_hbm(w_query),
+        in_hbm(w_key.T),
+        in_hbm(w_value.T),
+        in_hbm(w_forget.T),
+        in_hbm(w_out),
+        first_gain[None],
+        forget_bias[None],
+    )
     message, x = kernel(
         k_project,
         [((kv, 2 * rows + 8, LANES), BF16), block],
-        [VMEM, VMEM, VMEM, VMEM, ANY, VMEM],
+        [VMEM] * 6,
+        [pltpu.VMEM((rows, LANES), F32)],
+    )(recv, w_query, w_key, w_value, w_forget, tails)
+    recv = exchanged(message, KV)
+    positions = kv_cache.shape[1]
+    kv_cache, keys, gate_sums = kernel(
+        k_prepare,
         [
-            pltpu.VMEM((rows, LANES), F32),
-            pltpu.VMEM((w_forget.shape[1], width), BF16),
+            (kv_cache.shape, BF16),
+            ((rows // 2, 2 * DH, positions), BF16),
+            ((rows // 2, 8, positions), F32),
+        ],
+        [SMEM, ANY, ANY],
+        [
+            pltpu.VMEM(gate_sums.shape, F32),
+            pltpu.SemaphoreType.DMA((rows,)),
             pltpu.SemaphoreType.DMA,
         ],
-    )(
-        exchanged(message, "tp").reshape(width, rows),
-        w_query,
-        w_key.T,
-        w_value.T,
-        w_forget.T,
-        w_out,
-    )
+    )(live_lengths, in_hbm(kv_cache), in_hbm(gate_sums))
     message, tok, sums = kernel(
         k_attend,
         [((kv, 2 * rows + 8, LANES), BF16), block, ((2, LANES), F32)],
-        [VMEM, SMEM, SMEM, VMEM, VMEM],
-        [pltpu.VMEM((8 * rows, LANES), F32), pltpu.VMEM((8 * rows, LANES), F32)],
-    )(exchanged(message, KV), live_lengths, forget_bias, kv_cache, gate_sums)
-    (message,) = kernel(
-        k_combine, [((tp, rows + 8, width), BF16)], [VMEM] * 4, [pltpu.VMEM((8, width), F32)]
-    )(exchanged(message, KV), sums, w_out, first_gain[None])
+        [VMEM] * 4,
+        [pltpu.VMEM((4 * rows, LANES), F32), pltpu.VMEM((4 * rows, LANES), F32)],
+    )(recv, kv_cache, keys, gate_sums)
+    (message,) = kernel(k_combine, [((tp, rows + 8, width), BF16)], [VMEM] * 4)(
+        exchanged(message, KV), sums, w_out, tails
+    )
     message, scaled = kernel(
         k_expand,
         [((kv, 8, LANES), BF16), block],
@@ -393,7 +472,7 @@
         exchanged(message, "tp"), mid
     )
     (out,) = kernel(
-        k_finish, [((own, rows), BF16)], [VMEM] * 3, [pltpu.VMEM((width, rows), F32)]
+        k_finish, [((own, rows), BF16)], [VMEM] * 3, [pltpu.VMEM((width, rows), F32)], last=True
     )(exchanged(message, KV), mix, second_gain[None])
     return out.T
 

time: 138 us -> 129 us (0.935)
  blocking collectives: 121 us -> 79.2 us
  starting transfers between devices: 0 us -> 21.4 us
  waiting for transfers between devices: 0 us -> 13.1 us
  local copies, waits for them, and re-layouts: 8.97 us -> 4.8 us
  Pallas kernels: 7.02 us -> 9.46 us
    all_to_all x8 -> x6, blocking collectives: 121 us -> 79.2 us  [exchanged(): return lax.all_to_all(pieces, axis, 0, 0, tiled=True)]
    all_to_all x0 -> x2, starting transfers between devices: none -> 21.4 us  [exchanged(): return lax.all_to_all(pieces, axis, 0, 0, tiled=True)]
    all_to_all x0 -> x2, waiting for transfers between devices: none -> 13.1 us  [exchanged(): return lax.all_to_all(pieces, axis, 0, 0, tiled=True)]
    pallas_call x2 -> x4, Pallas kernels: 1.13 us -> 6.24 us  [the longest x1 3.45 us: on_device(): kernel(k_prepare, [(kv_cache.shape, BF16), ((rows // 2, 2 * DH, positions...]
    unnamed x31 -> x18, local copies, waits for them, and re-layouts: 8.28 us -> 3.51 us
    pallas_call x1, Pallas kernels: 4.75 us -> 1.5 us  [on_device(): kernel(k_attend, [((kv, 2 * rows + 8, LANES), BF16), block, ((2, LANES),...]
  transfers between devices with their start and end apart: 0 -> 2, of which waited for: 0 -> 2; matrix products, arithmetic and copies ran while one was open for 0% -> 0% of each run, Pallas kernels for 0% -> 4%
where the time goes in v4:
time: 129 us; the launch traced here: 128 us
  blocking collectives  79.2 us (61%)
  starting transfers between devices  21.4 us (17%)
  waiting for transfers between devices  13.1 us (10%)
  Pallas kernels  9.46 us (7%)
  local copies, waits for them, and re-layouts  4.8 us (4%)
    all_to_all x6, blocking collectives, exchanged(): return lax.all_to_all(pieces, axis, 0, 0, tiled=True)  79.2 us
    all_to_all x2, starting transfers between devices, exchanged(): return lax.all_to_all(pieces, axis, 0, 0, tiled=True)  21.4 us
    all_to_all x2, waiting for transfers between devices, exchanged(): return lax.all_to_all(pieces, axis, 0, 0, tiled=True)  13.1 us
    unnamed x18, local copies, waits for them, and re-layouts  3.51 us
    pallas_call x1, Pallas kernels, on_device(): kernel(k_prepare, [(kv_cache.shape, BF16), ((rows // 2, 2 * DH, positions...  3.45 us
  transfers between devices with their start and end apart: 2, of which 2 were waited for; matrix products, arithmetic and copies ran while one was open for 0% of the time, Pallas kernels for 4%

profile of v4, /device:TPU:1, one launch (start us, length us, event | category | flops | bytes accessed | tf_op | source)
XLA Modules:
  0.0 128.0 jit_solution(8396604548644164530)
XLA Ops:
  0.0 1.3 %broadcast_in_dim.15 = bf16[16,8,16]{2,1,0:T(8,128)(2,1)} broadcast(bf16[8,16]{1,0:T(8,128)(2,1)} %bitcast.20), dimensions={1,2} | broadcast | bytes 4352 | tf_op jit(solution)/shard_map/broadcast_in_dim | solution.py:403
  1.3 10.1 %all-to-all-start = ((bf16[16,8,16]{2,1,0:T(8,128)(2,1)}), bf16[16,8,16]{2,1,0:T(8,128)(2,1)S(1)}, u32[]{:S(2)}, u32[]{:S(2)}) async-start(bf16[16,8,16]{2,1,0:T(8,128)(2,1)} %broadcast_in_dim.15), calls=%async_computation | async-start | bytes 65536 | tf_op jit(solution)/shard_map/all_to_all | solution.py:41
  11.4 0.6 copy-done.5
  12.1 0.7 copy-done.6
  12.7 1.1 shard_map.145
  13.8 5.1 %all-to-all-done = bf16[16,8,16]{2,1,0:T(8,128)(2,1)S(1)} async-done(((bf16[16,8,16]{2,1,0:T(8,128)(2,1)}), bf16[16,8,16]{2,1,0:T(8,128)(2,1)S(1)}, u32[]{:S(2)}, u32[]{:S(2)}) %all-to-all-start) | async-done | bytes 4128 | tf_op jit(solution)/shard_map/all_to_all | solution.py:41
  18.9 1.2 shard_map.146
  20.1 11.3 %all-to-all-start.1 = ((bf16[32,40,128]{2,1,0:T(8,128)(2,1)}), bf16[32,40,128]{2,1,0:T(8,128)(2,1)S(1)}, u32[]{:S(2)}, u32[]{:S(2)}) async-start(bf16[32,40,128]{2,1,0:T(8,128)(2,1)} %get-tuple-element.30), calls=%async_computation.1 | async-start | bytes 655360 | tf_op jit(solution)/shard_map/all_to_all | solution.py:41
  31.4 0.0 copy-start.7
  31.4 0.6 copy-done.7
  32.0 3.5 %shard_map.147 = (bf16[16,512,128]{2,1,0:T(8,128)(2,1)S(1)}, bf16[8,128,512]{2,1,0:T(8,128)(2,1)S(1)}, f32[8,8,512]{2,1,0:T(8,128)S(1)}) custom-call(s32[16]{0:T(128)S(1)} %copy-done.7, bf16[16,512,128]{2,1,0:T(8,128)(2,1)} %cache.1, f32[16,1,512]{2,1,0:T(1,128)} %gate.1), custom_call_target="tpu_custom_call" | custom-call | tf_op jit(solution)/shard_map/pallas_call | solution.py:436
  35.5 0.0 copy-start.3
  35.5 0.6 copy-done.3
  36.1 8.0 %all-to-all-done.1.recv = bf16[32,40,128]{2,1,0:T(8,128)(2,1)S(1)} async-done(((bf16[32,40,128]{2,1,0:T(8,128)(2,1)}), bf16[32,40,128]{2,1,0:T(8,128)(2,1)S(1)}, u32[]{:S(2)}, u32[]{:S(2)}) %all-to-all-start.1) | async-done | bytes 327712 | tf_op jit(solution)/shard_map/all_to_all | solution.py:41
  44.1 0.9 copy-done.4
  45.0 1.5 %shard_map.148 = (bf16[32,40,128]{2,1,0:T(8,128)(2,1)S(1)}, f32[16,128]{1,0:T(8,128)S(1)}, f32[2,128]{1,0:T(2,128)S(1)}) custom-call(bf16[32,40,128]{2,1,0:T(8,128)(2,1)S(1)} %all-to-all-done.1.recv, bf16[16,512,128]{2,1,0:T(8,128)(2,1)S(1)} %get-tuple-element.31.cache, bf16[8,128,512]{2,1,0:T(8,128)(2,1)S(1)} %get-tuple-element.32.keys, ...), custom_call_target="tpu_custom_call" | custom-call | tf_op jit(solution)/shard_map/pallas_call | solution.py:450
  46.5 0.0 copy-start.8
  46.6 16.2 %all_to_all.40.recv = bf16[32,40,128]{2,1,0:T(8,128)(2,1)S(1)} all-to-all(bf16[32,40,128]{2,1,0:T(8,128)(2,1)S(1)} %get-tuple-element.34), channel_id=1, replica_groups=mesh['kv_0'=8,'kv_1'=4,'tp'=16] {'kv_0','kv_1'}, dimensions={0} | all-to-all | bytes 655360 | tf_op jit(solution)/shard_map/all_to_all | solution.py:41
  62.7 0.5 shard_map.149
  63.3 14.2 %all_to_all.41.recv = bf16[16,24,128]{2,1,0:T(8,128)(2,1)S(1)} all-to-all(bf16[16,24,128]{2,1,0:T(8,128)(2,1)S(1)} %shard_map.149), channel_id=1, replica_groups=mesh['kv_0'=8,'kv_1'=4,'tp'=16] {'tp'}, dimensions={0} | all-to-all | bytes 196608 | tf_op jit(solution)/shard_map/all_to_all | solution.py:41
  77.4 0.0 copy-done.1
  77.4 0.0 copy-done.2
  77.5 0.4 shard_map.150
  77.9 12.6 %all_to_all.42.recv = bf16[32,8,128]{2,1,0:T(8,128)(2,1)S(1)} all-to-all(bf16[32,8,128]{2,1,0:T(8,128)(2,1)S(1)} %get-tuple-element.39), channel_id=1, replica_groups=mesh['kv_0'=8,'kv_1'=4,'tp'=16] {'kv_0','kv_1'}, dimensions={0} | all-to-all | bytes 131072 | tf_op jit(solution)/shard_map/all_to_all | solution.py:41
  90.5 0.1 shard_map.151
  90.6 11.9 %all_to_all.43.recv = bf16[32,8,128]{2,1,0:T(8,128)(2,1)S(1)} all-to-all(bf16[32,8,128]{2,1,0:T(8,128)(2,1)S(1)} %get-tuple-element.41), channel_id=1, replica_groups=mesh['kv_0'=8,'kv_1'=4,'tp'=16] {'kv_0','kv_1'}, dimensions={0} | all-to-all | bytes 131072 | tf_op jit(solution)/shard_map/all_to_all | solution.py:41
  102.6 0.0 copy-done
  102.6 0.2 shard_map.152
  102.7 12.7 %all_to_all.44.recv = bf16[16,16,128]{2,1,0:T(8,128)(2,1)S(1)} all-to-all(bf16[16,16,128]{2,1,0:T(8,128)(2,1)S(1)} %shard_map.152), channel_id=1, replica_groups=mesh['kv_0'=8,'kv_1'=4,'tp'=16] {'tp'}, dimensions={0} | all-to-all | bytes 131072 | tf_op jit(solution)/shard_map/all_to_all | solution.py:41
  115.4 0.2 shard_map.153
  115.6 11.6 %all_to_all.45.recv = f32[32,1,128]{2,1,0:T(1,128)S(1)} all-to-all(f32[32,1,128]{2,1,0:T(1,128)S(1)} %get-tuple-element.43), channel_id=1, replica_groups=mesh['kv_0'=8,'kv_1'=4,'tp'=16] {'kv_0','kv_1'}, dimensions={0} | all-to-all | bytes 32768 | tf_op jit(solution)/shard_map/all_to_all | solution.py:41
  127.2 0.8 shard_map.154
  (7 shorter events, 0.0 us)
Async XLA Ops:
  1.3 17.6 %all-to-all-start = ((bf16[16,8,16]{2,1,0:T(8,128)(2,1)}), bf16[16,8,16]{2,1,0:T(8,128)(2,1)S(1)}, u32[]{:S(2)}, u32[]{:S(2)}) async-start(bf16[16,8,16]{2,1,0:T(8,128)(2,1)} %broadcast_in_dim.15), calls=%async_computation | async-start | bytes 65536 | tf_op jit(solution)/shard_map/all_to_all | solution.py:41
  11.4 0.7 copy-start.5
  12.1 0.7 copy-start.6
  20.1 24.1 %all-to-all-start.1 = ((bf16[32,40,128]{2,1,0:T(8,128)(2,1)}), bf16[32,40,128]{2,1,0:T(8,128)(2,1)S(1)}, u32[]{:S(2)}, u32[]{:S(2)}) async-start(bf16[32,40,128]{2,1,0:T(8,128)(2,1)} %get-tuple-element.30), calls=%async_computation.1 | async-start | bytes 655360 | tf_op jit(solution)/shard_map/all_to_all | solution.py:41
  31.4 0.7 copy-start.7
  35.5 0.6 copy-start.3
  44.1 0.9 copy-start.4
  45.0 32.4 %copy-start.1 = (bf16[128,704]{0,1:T(8,128)(2,1)S(1)}, bf16[128,704]{0,1:T(8,128)(2,1)}, u32[]{:S(2)}) copy-start(bf16[128,704]{0,1:T(8,128)(2,1)} %param.26) | copy-start | bytes 540676
  45.0 32.4 %copy-start.2 = (bf16[128,704]{0,1:T(8,128)(2,1)S(1)}, bf16[128,704]{0,1:T(8,128)(2,1)}, u32[]{:S(2)}) copy-start(bf16[128,704]{0,1:T(8,128)(2,1)} %param.27) | copy-start | bytes 540676
  45.0 57.5 %copy-start = (bf16[704,128]{1,0:T(8,128)(2,1)S(1)}, bf16[704,128]{1,0:T(8,128)(2,1)}, u32[]{:S(2)}) copy-start(bf16[704,128]{1,0:T(8,128)(2,1)} %w_down.1) | copy-start | bytes 540676
  46.5 80.7 %copy-start.8 = (f32[8]{0:T(128)S(1)}, f32[8]{0:T(128)}, u32[]{:S(2)}) copy-start(f32[8]{0:T(128)} %param.29) | copy-start | bytes 100

commit v5 on v4

--- a/solution.py
+++ b/solution.py
@@ -96,21 +96,40 @@
     return total
 
 
-def k_weights(query, key, value, forget, w_out, gain, bias, query_o, key_o, value_o, forget_o, w_out_o, tail_o, sem):
+def k_weights(
+    query,
+    key,
+    value,
+    forget,
+    w_out,
+    gain_hbm,
+    bias_hbm,
+    query_o,
+    key_o,
+    value_o,
+    forget_o,
+    w_out_o,
+    tail_o,
+    gain,
+    bias,
+    sem,
+):
     width = forget_o.shape[1]
     start = pl.multiple_of(kv_index() * width, width)
     pairs = [(w_out, w_out_o), (query, query_o), (key, key_o), (value, value_o)]
     pairs.append((forget.at[:, pl.ds(start, width)], forget_o))
+    pairs.extend([(gain_hbm, gain), (bias_hbm, bias)])
     copies = [pltpu.make_async_copy(a, b, sem.at[k]) for k, (a, b) in enumerate(pairs)]
     for copy in copies:
         copy.start()
-    own = gain.shape[1]
-    spread = jnp.where(iota((own, LANES), 1) == iota((own, LANES), 0) + lax.axis_index("tp") * own, 1.0, 0.0)
-    column = jnp.sum(jnp.where(diagonal(own, 0)[:, :own], gain[...], 0.0), axis=1, keepdims=True)
-    gains = in_pieces(jnp.sum(spread * column, axis=0, keepdims=True), 3)
     row = iota((8, LANES), 0)
     for copy in copies:
         copy.wait()
+    own = gain.shape[1]
+    place = iota((own, LANES), 0) + lax.axis_index("tp") * own
+    spread = jnp.where(iota((own, LANES), 1) == place, 1.0, 0.0)
+    column = jnp.sum(jnp.where(diagonal(own, 0)[:, :own], gain[...], 0.0), axis=1, keepdims=True)
+    gains = in_pieces(jnp.sum(spread * column, axis=0, keepdims=True), 3)
     sums = across(jnp.ones((8, LANES), BF16), w_out_o[...], LAST)
     sums_hi, sums_lo = in_pieces(sums, 2)
     tail = jnp.where(row == 2, sums_hi[:, :LANES], 0.0)
@@ -154,27 +173,35 @@
             out[k, pl.ds(2 * rows, 8)] = own_tail
 
 
-def k_prepare(lengths, cache, gate, cache_o, keys_o, gate_o, gate_v, sem, gate_sem):
+def k_prepare(lengths, cache, gate, keys_o, values_o, cache_v, gate_v, sem, gate_sem):
     rows, positions = cache.shape[:2]
-    copies = [pltpu.make_async_copy(cache.at[b], cache_o.at[b], sem.at[b]) for b in range(rows)]
+    copies = [pltpu.make_async_copy(cache.at[b], cache_v.at[b], sem.at[b]) for b in range(rows)]
     gates = pltpu.make_async_copy(gate, gate_v, gate_sem)
     gates.start()
     for copy in copies:
         copy.start()
     gates.wait()
     place = kv_index() * positions + iota((8, positions), 1)
-    first = iota((8, positions), 0) < 4
+    row = iota((16, positions), 0)
     for m in range(rows // 2):
-        one = jnp.where(place < lengths[2 * m], gate_v[2 * m], EMPTY_SCORE)
-        two = jnp.where(place < lengths[2 * m + 1], gate_v[2 * m + 1], EMPTY_SCORE)
-        gate_o[m] = jnp.where(first, one, two)
+        extra = jnp.zeros((16, positions), F32)
+        for k in range(2):
+            b = 2 * m + k
+            masked = jnp.where(place < lengths[b], gate_v[b], EMPTY_SCORE)
+            for n, piece in enumerate(in_pieces(masked, 3)):
+                extra = jnp.where(row == 3 * k + n, piece[0:1], extra)
+        keys_o[m, pl.ds(2 * DH, 16), :] = extra.astype(BF16)
     for b in range(rows):
         copies[b].wait()
-        keys_o[b // 2, pl.ds(DH * (b % 2), DH), :] = cache_o[b].T[:DH]
-
-
-def k_attend(recv, cache, keys, gate, out, tok_out, sums_out, qs, os):
-    rows = cache.shape[0]
+        keys_o[b // 2, pl.ds(DH * (b % 2), DH), :] = cache_v[b].T[:DH]
+        if b % 2:
+            values_o[b // 2] = jnp.concatenate(
+                [cache_v[b - 1][:, DH:], cache_v[b][:, DH:]], axis=1
+            )
+
+
+def k_attend(recv, keys, values, out, tok_out, sums_out, qs, os):
+    rows = 2 * keys.shape[0]
     heads = 4
     scale = DH**-0.5
     left = rounded(summed(recv, 0, rows))
@@ -205,35 +232,40 @@
     fetched = jnp.sum(fetched, axis=1, keepdims=True)
     new_gate = jnp.minimum(fetched, 0.0) - jnp.log(1.0 + jnp.exp(-jnp.abs(fetched)))
     lane = iota((1, LANES), 1)
-    new_key = jnp.where(lane < DH, new_row, pltpu.roll(jnp.broadcast_to(new_row, (8, LANES)), DH, 1)[0:1])
+    new_turned = pltpu.roll(jnp.broadcast_to(new_row, (8, LANES)), DH, 1)[0:1]
+    new_key = jnp.where(lane < DH, new_row, new_turned)
+    new_value = jnp.where(lane < DH, new_turned, new_row)
     own = jnp.sum(qs[...] * new_key, axis=1, keepdims=True) * scale
     mine = iota((all_rows, 1), 0) // heads == kv_index()
     own = jnp.where(mine, own, EMPTY_SCORE)
     lane = iota((8, LANES), 1)
-    first = iota((8, LANES), 0) < heads
+    spot = jnp.where(iota((8, LANES), 0) < heads, DH, 0)
+    extra = iota((8, 16), 1) - 3 * (iota((8, 16), 0) // heads)
+    extra = jnp.where((extra >= 0) & (extra < 3), 1.0, 0.0)
     for m in range(rows // 2):
         at = slice(8 * m, 8 * m + 8)
-        scores = jnp.dot(
-            qs[pl.ds(8 * m, 8), :].astype(BF16), keys[m], preferred_element_type=F32
-        )
-        scores = scores * scale + (gate[m] + new_gate[at])
+        query = jnp.concatenate([qs[pl.ds(8 * m, 8), :] * scale, extra], axis=1)
+        scores = jnp.dot(query.astype(BF16), keys[m], preferred_element_type=F32)
+        scores = scores + new_gate[at]
         top = jnp.maximum(jnp.max(scores, axis=1, keepdims=True), own[at])
         top = jnp.maximum(top, 0.1 * EMPTY_SCORE)
         weights = jnp.exp(scores - top)
         own_weight = jnp.exp(own[at] - top)
         total = jnp.sum(weights, axis=1, keepdims=True) + own_weight
-        block = jnp.concatenate([cache[2 * m], cache[2 * m + 1]], axis=1)
-        value = jnp.dot(weights.astype(BF16), block, preferred_element_type=F32)
-        value = jnp.where(first, value[:, :LANES], value[:, LANES:])
-        value = value + rounded(own_weight) * new_row
-        os[pl.ds(8 * m, 8), :] = jnp.where(lane == 0, top, jnp.where(lane == 1, total, value))
+        value = jnp.dot(weights.astype(BF16), values[m], preferred_element_type=F32)
+        value = value + rounded(own_weight) * new_value
+        spare = jnp.where(lane == spot, top, jnp.where(lane == spot + 1, total, value))
+        os[pl.ds(8 * m, 8), :] = spare
     blocks = [os[pl.ds(h, rows, stride=heads), :] for h in range(heads)]
-    low_out = jnp.where(low, pltpu.roll(blocks[0], DH, 1), blocks[1]).astype(BF16)
-    high_out = jnp.where(low, pltpu.roll(blocks[2], DH, 1), blocks[3]).astype(BF16)
+    turned = [pltpu.roll(block, DH, 1) for block in blocks]
+    firsts = [jnp.where(even, block, turn) for block, turn in zip(blocks, turned)]
+    seconds = [jnp.where(even, turn, block) for block, turn in zip(blocks, turned)]
+    low_out = jnp.where(low, firsts[0], seconds[1]).astype(BF16)
+    high_out = jnp.where(low, firsts[2], seconds[3]).astype(BF16)
     lane = iota((rows, LANES), 1)
     stats = jnp.zeros((rows, LANES), F32)
     for h in range(heads):
-        pieces = [*in_pieces(blocks[h][:, 0:1], 3), *in_pieces(blocks[h][:, 1:2], 2)]
+        pieces = [*in_pieces(seconds[h][:, 0:1], 3), *in_pieces(seconds[h][:, 1:2], 2)]
         for k, piece in enumerate(pieces):
             stats = jnp.where(lane == 8 * h + k, piece, stats)
     stats = (stats[:8] + pltpu.roll(stats[8:], 32, 1)).astype(BF16)
@@ -414,16 +446,20 @@
             ((heads, width), BF16),
             ((2, 8, LANES), F32),
         ],
-        [ANY] * 5 + [VMEM] * 2,
-        [pltpu.SemaphoreType.DMA((5,))],
+        [ANY] * 7,
+        [
+            pltpu.VMEM((1, own), F32),
+            pltpu.VMEM((1, w_forget.shape[1]), F32),
+            pltpu.SemaphoreType.DMA((7,)),
+        ],
     )(
         in_hbm(w_query),
         in_hbm(w_key.T),
         in_hbm(w_value.T),
         in_hbm(w_forget.T),
         in_hbm(w_out),
-        first_gain[None],
-        forget_bias[None],
+        in_hbm(first_gain[None]),
+        in_hbm(forget_bias[None]),
     )
     message, x = kernel(
         k_project,
@@ -433,15 +469,15 @@
     )(recv, w_query, w_key, w_value, w_forget, tails)
     recv = exchanged(message, KV)
     positions = kv_cache.shape[1]
-    kv_cache, keys, gate_sums = kernel(
+    keys, values = kernel(
         k_prepare,
         [
-            (kv_cache.shape, BF16),
-            ((rows // 2, 2 * DH, positions), BF16),
-            ((rows // 2, 8, positions), F32),
+            ((rows // 2, 2 * DH + 16, positions), BF16),
+            ((rows // 2, positions, 2 * DH), BF16),
         ],
         [SMEM, ANY, ANY],
         [
+            pltpu.VMEM(kv_cache.shape, BF16),
             pltpu.VMEM(gate_sums.shape, F32),
             pltpu.SemaphoreType.DMA((rows,)),
             pltpu.SemaphoreType.DMA,
@@ -450,9 +486,9 @@
     message, tok, sums = kernel(
         k_attend,
         [((kv, 2 * rows + 8, LANES), BF16), block, ((2, LANES), F32)],
-        [VMEM] * 4,
+        [VMEM] * 3,
         [pltpu.VMEM((4 * rows, LANES), F32), pltpu.VMEM((4 * rows, LANES), F32)],
-    )(recv, kv_cache, keys, gate_sums)
+    )(recv, keys, values)
     (message,) = kernel(k_combine, [((tp, rows + 8, width), BF16)], [VMEM] * 4)(
         exchanged(message, KV), sums, w_out, tails
     )

time: 129 us -> 128 us (level)
  local copies, waits for them, and re-layouts: 4.8 us -> 1.95 us
  Pallas kernels: 9.46 us -> 10.8 us
  waiting for transfers between devices: 13.1 us -> 14.4 us
    unnamed x18 -> x10, local copies, waits for them, and re-layouts: 3.51 us -> 0.67 us
    all_to_all x2, waiting for transfers between devices: 13.1 us -> 14.4 us  [exchanged(): return lax.all_to_all(pieces, axis, 0, 0, tiled=True)]
where the time goes in v5:
time: 128 us
  blocking collectives  79.2 us (62%)
  starting transfers between devices  21.4 us (17%)
  waiting for transfers between devices  14.4 us (11%)
  Pallas kernels  10.8 us (8%)
  local copies, waits for them, and re-layouts  1.95 us (2%)
    all_to_all x6, blocking collectives, exchanged(): return lax.all_to_all(pieces, axis, 0, 0, tiled=True)  79.2 us
    all_to_all x2, starting transfers between devices, exchanged(): return lax.all_to_all(pieces, axis, 0, 0, tiled=True)  21.4 us
    all_to_all x2, waiting for transfers between devices, exchanged(): return lax.all_to_all(pieces, axis, 0, 0, tiled=True)  14.4 us
    pallas_call x1, Pallas kernels, on_device(): kernel(k_prepare, [((rows // 2, 2 * DH + 16, positions), BF16), ((rows //...  4 us
  transfers between devices with their start and end apart: 2, of which 2 were waited for; matrix products, arithmetic and copies ran while one was open for 0% of the time, Pallas kernels for 4%

profile of v5, /device:TPU:1, one launch (start us, length us, event | category | flops | bytes accessed | tf_op | source)
XLA Modules:
  0.0 127.9 jit_solution(1575766907745251629)
XLA Ops:
  0.0 1.3 %broadcast_in_dim.15 = bf16[16,8,16]{2,1,0:T(8,128)(2,1)} broadcast(bf16[8,16]{1,0:T(8,128)(2,1)} %bitcast.18), dimensions={1,2} | broadcast | bytes 4352 | tf_op jit(solution)/shard_map/broadcast_in_dim | solution.py:435
  1.3 10.1 %all-to-all-start = ((bf16[16,8,16]{2,1,0:T(8,128)(2,1)}), bf16[16,8,16]{2,1,0:T(8,128)(2,1)S(1)}, u32[]{:S(2)}, u32[]{:S(2)}) async-start(bf16[16,8,16]{2,1,0:T(8,128)(2,1)} %broadcast_in_dim.15), calls=%async_computation | async-start | bytes 65536 | tf_op jit(solution)/shard_map/all_to_all | solution.py:41
  11.4 1.1 shard_map.145
  12.5 6.4 %all-to-all-done = bf16[16,8,16]{2,1,0:T(8,128)(2,1)S(1)} async-done(((bf16[16,8,16]{2,1,0:T(8,128)(2,1)}), bf16[16,8,16]{2,1,0:T(8,128)(2,1)S(1)}, u32[]{:S(2)}, u32[]{:S(2)}) %all-to-all-start) | async-done | bytes 4128 | tf_op jit(solution)/shard_map/all_to_all | solution.py:41
  18.9 1.2 shard_map.146
  20.0 11.3 %all-to-all-start.1 = ((bf16[32,40,128]{2,1,0:T(8,128)(2,1)}), bf16[32,40,128]{2,1,0:T(8,128)(2,1)S(1)}, u32[]{:S(2)}, u32[]{:S(2)}) async-start(bf16[32,40,128]{2,1,0:T(8,128)(2,1)} %get-tuple-element.29), calls=%async_computation.1 | async-start | bytes 655360 | tf_op jit(solution)/shard_map/all_to_all | solution.py:41
  31.4 0.0 copy-start.3
  31.4 0.6 copy-done.3
  32.0 4.0 %shard_map.147 = (bf16[8,144,512]{2,1,0:T(8,128)(2,1)S(1)}, bf16[8,512,128]{2,1,0:T(8,128)(2,1)S(1)}) custom-call(s32[16]{0:T(128)S(1)} %copy-done.3, bf16[16,512,128]{2,1,0:T(8,128)(2,1)} %cache.1, f32[16,1,512]{2,1,0:T(1,128)} %gate.1), custom_call_target="tpu_custom_call" | custom-call | tf_op jit(solution)/shard_map/pallas_call | solution.py:472
  36.0 0.0 copy-start.1
  36.0 0.0 copy-start.2
  36.0 8.1 %all-to-all-done.1.recv = bf16[32,40,128]{2,1,0:T(8,128)(2,1)S(1)} async-done(((bf16[32,40,128]{2,1,0:T(8,128)(2,1)}), bf16[32,40,128]{2,1,0:T(8,128)(2,1)S(1)}, u32[]{:S(2)}, u32[]{:S(2)}) %all-to-all-start.1) | async-done | bytes 327712 | tf_op jit(solution)/shard_map/all_to_all | solution.py:41
  44.1 0.0 copy-start
  44.1 0.0 copy-start.4
  44.1 2.3 %shard_map.148 = (bf16[32,40,128]{2,1,0:T(8,128)(2,1)S(1)}, f32[16,128]{1,0:T(8,128)S(1)}, f32[2,128]{1,0:T(2,128)S(1)}) custom-call(bf16[32,40,128]{2,1,0:T(8,128)(2,1)S(1)} %all-to-all-done.1.recv, bf16[8,144,512]{2,1,0:T(8,128)(2,1)S(1)} %get-tuple-element.30.keys, bf16[8,512,128]{2,1,0:T(8,128)(2,1)S(1)} %get-tuple-element.31.values), custom_call_target="tpu_custom_call" | custom-call | tf_op jit(solution)/shard_map/pallas_call | solution.py:486
  46.4 16.2 %all_to_all.40.recv = bf16[32,40,128]{2,1,0:T(8,128)(2,1)S(1)} all-to-all(bf16[32,40,128]{2,1,0:T(8,128)(2,1)S(1)} %get-tuple-element.32), channel_id=1, replica_groups=mesh['kv_0'=8,'kv_1'=4,'tp'=16] {'kv_0','kv_1'}, dimensions={0} | all-to-all | bytes 655360 | tf_op jit(solution)/shard_map/all_to_all | solution.py:41
  62.5 0.5 shard_map.149
  63.1 14.2 %all_to_all.41.recv = bf16[16,24,128]{2,1,0:T(8,128)(2,1)S(1)} all-to-all(bf16[16,24,128]{2,1,0:T(8,128)(2,1)S(1)} %shard_map.149), channel_id=1, replica_groups=mesh['kv_0'=8,'kv_1'=4,'tp'=16] {'tp'}, dimensions={0} | all-to-all | bytes 196608 | tf_op jit(solution)/shard_map/all_to_all | solution.py:41
  77.3 0.0 copy-done.1
  77.3 0.0 copy-done.2
  77.3 0.4 shard_map.150
  77.7 12.6 %all_to_all.42.recv = bf16[32,8,128]{2,1,0:T(8,128)(2,1)S(1)} all-to-all(bf16[32,8,128]{2,1,0:T(8,128)(2,1)S(1)} %get-tuple-element.37), channel_id=1, replica_groups=mesh['kv_0'=8,'kv_1'=4,'tp'=16] {'kv_0','kv_1'}, dimensions={0} | all-to-all | bytes 131072 | tf_op jit(solution)/shard_map/all_to_all | solution.py:41
  90.3 0.1 shard_map.151
  90.4 11.9 %all_to_all.43.recv = bf16[32,8,128]{2,1,0:T(8,128)(2,1)S(1)} all-to-all(bf16[32,8,128]{2,1,0:T(8,128)(2,1)S(1)} %get-tuple-element.39), channel_id=1, replica_groups=mesh['kv_0'=8,'kv_1'=4,'tp'=16] {'kv_0','kv_1'}, dimensions={0} | all-to-all | bytes 131072 | tf_op jit(solution)/shard_map/all_to_all | solution.py:41
  102.4 0.0 copy-done
  102.4 0.2 shard_map.152
  102.5 12.7 %all_to_all.44.recv = bf16[16,16,128]{2,1,0:T(8,128)(2,1)S(1)} all-to-all(bf16[16,16,128]{2,1,0:T(8,128)(2,1)S(1)} %shard_map.152), channel_id=1, replica_groups=mesh['kv_0'=8,'kv_1'=4,'tp'=16] {'tp'}, dimensions={0} | all-to-all | bytes 131072 | tf_op jit(solution)/shard_map/all_to_all | solution.py:41
  115.2 0.2 shard_map.153
  115.4 11.6 %all_to_all.45.recv = f32[32,1,128]{2,1,0:T(1,128)S(1)} all-to-all(f32[32,1,128]{2,1,0:T(1,128)S(1)} %get-tuple-element.41), channel_id=1, replica_groups=mesh['kv_0'=8,'kv_1'=4,'tp'=16] {'kv_0','kv_1'}, dimensions={0} | all-to-all | bytes 32768 | tf_op jit(solution)/shard_map/all_to_all | solution.py:41
  127.0 0.0 copy-done.4
  127.0 0.8 shard_map.154
Async XLA Ops:
  1.3 17.6 %all-to-all-start = ((bf16[16,8,16]{2,1,0:T(8,128)(2,1)}), bf16[16,8,16]{2,1,0:T(8,128)(2,1)S(1)}, u32[]{:S(2)}, u32[]{:S(2)}) async-start(bf16[16,8,16]{2,1,0:T(8,128)(2,1)} %broadcast_in_dim.15), calls=%async_computation | async-start | bytes 65536 | tf_op jit(solution)/shard_map/all_to_all | solution.py:41
  20.0 24.1 %all-to-all-start.1 = ((bf16[32,40,128]{2,1,0:T(8,128)(2,1)}), bf16[32,40,128]{2,1,0:T(8,128)(2,1)S(1)}, u32[]{:S(2)}, u32[]{:S(2)}) async-start(bf16[32,40,128]{2,1,0:T(8,128)(2,1)} %get-tuple-element.29), calls=%async_computation.1 | async-start | bytes 655360 | tf_op jit(solution)/shard_map/all_to_all | solution.py:41
  31.4 0.7 copy-start.3
  36.0 41.2 %copy-start.1 = (bf16[128,704]{0,1:T(8,128)(2,1)S(1)}, bf16[128,704]{0,1:T(8,128)(2,1)}, u32[]{:S(2)}) copy-start(bf16[128,704]{0,1:T(8,128)(2,1)} %param.26) | copy-start | bytes 540676
  36.0 41.2 %copy-start.2 = (bf16[128,704]{0,1:T(8,128)(2,1)S(1)}, bf16[128,704]{0,1:T(8,128)(2,1)}, u32[]{:S(2)}) copy-start(bf16[128,704]{0,1:T(8,128)(2,1)} %param.27) | copy-start | bytes 540676
  44.1 58.3 %copy-start = (bf16[704,128]{1,0:T(8,128)(2,1)S(1)}, bf16[704,128]{1,0:T(8,128)(2,1)}, u32[]{:S(2)}) copy-start(bf16[704,128]{1,0:T(8,128)(2,1)} %w_down.1) | copy-start | bytes 540676
  44.1 82.9 %copy-start.4 = (f32[8]{0:T(128)S(1)}, f32[8]{0:T(128)}, u32[]{:S(2)}) copy-start(f32[8]{0:T(128)} %param.29) | copy-start | bytes 100

commit v6 on v5

--- a/solution.py
+++ b/solution.py
@@ -94,6 +94,25 @@
     for k in range(1, ref.shape[0]):
         total = total + ref[k, pl.ds(start, size)].astype(F32)
     return total
+
+
+def tiles_of(block):
+    return [block[4 * t : 4 * t + 4] for t in range(block.shape[0] // 4)]
+
+
+def put(out, k, tiles):
+    for t, tile in enumerate(tiles):
+        out[k, t] = tile
+
+
+def tiles_summed(ref, start, count):
+    tiles = []
+    for t in range(start, start + count):
+        total = ref[0, t].astype(F32)
+        for k in range(1, ref.shape[0]):
+            total = total + ref[k, t].astype(F32)
+        tiles.append(total)
+    return tiles[0] if count == 1 else jnp.concatenate(tiles, axis=0)
 
 
 def k_weights(
@@ -131,11 +150,8 @@
     column = jnp.sum(jnp.where(diagonal(own, 0)[:, :own], gain[...], 0.0), axis=1, keepdims=True)
     gains = in_pieces(jnp.sum(spread * column, axis=0, keepdims=True), 3)
     sums = across(jnp.ones((8, LANES), BF16), w_out_o[...], LAST)
-    sums_hi, sums_lo = in_pieces(sums, 2)
-    tail = jnp.where(row == 2, sums_hi[:, :LANES], 0.0)
-    tail = jnp.where(row == 3, sums_hi[:, LANES:], tail)
-    tail = jnp.where(row == 4, sums_lo[:, :LANES], tail)
-    tail_o[0] = jnp.where(row == 5, sums_lo[:, LANES:], tail)
+    tail = jnp.where(row == 2, sums[:, :LANES], 0.0)
+    tail_o[0] = jnp.where(row == 3, sums[:, LANES:], tail)
     mine = iota(bias.shape, 1) == lax.axis_index("tp")
     once = jnp.where(kv_index() == 0, 1.0, 0.0)
     own_bias = jnp.sum(jnp.where(mine, bias[...], 0.0), axis=1, keepdims=True) * once
@@ -163,17 +179,14 @@
     small = as_row([*in_pieces(forget_col, 2), *in_pieces(token_col, 2)])
     row = iota((8, LANES), 0)
     tail = jnp.where(row == 1, small, tails[0])
-    left = query[:, :LANES].astype(BF16)
-    right = query[:, LANES:].astype(BF16)
+    tiles = tiles_of(query[:, :LANES].astype(BF16)) + tiles_of(query[:, LANES:].astype(BF16))
     for b in range(rows):
-        own_tail = jnp.where(row == 0, new_rows[pl.ds(b, 1), :], tail).astype(BF16)
+        own_tail = jnp.where(row == 0, new_rows[pl.ds(b, 1), :], tail)[:4].astype(BF16)
         for k in range(b, out.shape[0], rows):
-            out[k, pl.ds(0, rows)] = left
-            out[k, pl.ds(rows, rows)] = right
-            out[k, pl.ds(2 * rows, 8)] = own_tail
-
-
-def k_prepare(lengths, cache, gate, keys_o, values_o, cache_v, gate_v, sem, gate_sem):
+            put(out, k, [*tiles, own_tail])
+
+
+def k_prepare(lengths, cache, gate, keys_o, values_o, gate_o, cache_v, gate_v, sem, gate_sem):
     rows, positions = cache.shape[:2]
     copies = [pltpu.make_async_copy(cache.at[b], cache_v.at[b], sem.at[b]) for b in range(rows)]
     gates = pltpu.make_async_copy(gate, gate_v, gate_sem)
@@ -182,15 +195,11 @@
         copy.start()
     gates.wait()
     place = kv_index() * positions + iota((8, positions), 1)
-    row = iota((16, positions), 0)
+    first = iota((8, positions), 0) < 4
     for m in range(rows // 2):
-        extra = jnp.zeros((16, positions), F32)
-        for k in range(2):
-            b = 2 * m + k
-            masked = jnp.where(place < lengths[b], gate_v[b], EMPTY_SCORE)
-            for n, piece in enumerate(in_pieces(masked, 3)):
-                extra = jnp.where(row == 3 * k + n, piece[0:1], extra)
-        keys_o[m, pl.ds(2 * DH, 16), :] = extra.astype(BF16)
+        one = jnp.where(place < lengths[2 * m], gate_v[2 * m], EMPTY_SCORE)
+        two = jnp.where(place < lengths[2 * m + 1], gate_v[2 * m + 1], EMPTY_SCORE)
+        gate_o[m] = jnp.where(first, one, two)
     for b in range(rows):
         copies[b].wait()
         keys_o[b // 2, pl.ds(DH * (b % 2), DH), :] = cache_v[b].T[:DH]
@@ -200,17 +209,16 @@
             )
 
 
-def k_attend(recv, keys, values, out, tok_out, sums_out, qs, os):
+def k_attend(recv, keys, values, gate, out, tok_out, sums_out, qs, os):
     rows = 2 * keys.shape[0]
     heads = 4
     scale = DH**-0.5
-    left = rounded(summed(recv, 0, rows))
-    right = rounded(summed(recv, rows, rows))
-    tail = summed(recv, 2 * rows, 8)
+    left = rounded(tiles_summed(recv, 0, rows // 4))
+    right = rounded(tiles_summed(recv, rows // 4, rows // 4))
+    tail = tiles_summed(recv, rows // 2, 1)
     new_row = rounded(tail[0:1])
     small = tail[1:2]
-    sums_out[0:1, :] = tail[2:3] + tail[4:5]
-    sums_out[1:2, :] = tail[3:4] + tail[5:6]
+    sums_out[...] = tail[2:4]
     tok_out[...] = jnp.broadcast_to(as_column(small, rows, (2, 3)), tok_out.shape)
     even = iota((rows, LANES), 0) % 2 == 0
     low = iota((rows, LANES), 1) < DH
@@ -240,13 +248,11 @@
     own = jnp.where(mine, own, EMPTY_SCORE)
     lane = iota((8, LANES), 1)
     spot = jnp.where(iota((8, LANES), 0) < heads, DH, 0)
-    extra = iota((8, 16), 1) - 3 * (iota((8, 16), 0) // heads)
-    extra = jnp.where((extra >= 0) & (extra < 3), 1.0, 0.0)
     for m in range(rows // 2):
         at = slice(8 * m, 8 * m + 8)
-        query = jnp.concatenate([qs[pl.ds(8 * m, 8), :] * scale, extra], axis=1)
-        scores = jnp.dot(query.astype(BF16), keys[m], preferred_element_type=F32)
-        scores = scores + new_gate[at]
+        query = (qs[pl.ds(8 * m, 8), :] * scale).astype(BF16)
+        scores = jnp.dot(query, keys[m], preferred_element_type=F32)
+        scores = scores + (gate[m] + new_gate[at])
         top = jnp.maximum(jnp.max(scores, axis=1, keepdims=True), own[at])
         top = jnp.maximum(top, 0.1 * EMPTY_SCORE)
         weights = jnp.exp(scores - top)
@@ -268,38 +274,44 @@
         pieces = [*in_pieces(seconds[h][:, 0:1], 3), *in_pieces(seconds[h][:, 1:2], 2)]
         for k, piece in enumerate(pieces):
             stats = jnp.where(lane == 8 * h + k, piece, stats)
-    stats = (stats[:8] + pltpu.roll(stats[8:], 32, 1)).astype(BF16)
+    packed = stats[:4]
+    for g in range(1, rows // 4):
+        packed = packed + pltpu.roll(stats, 32 * g, 1)[4 * g : 4 * g + 4]
+    tiles = [*tiles_of(low_out), *tiles_of(high_out), packed.astype(BF16)]
     for k in range(out.shape[0]):
-        out[k, pl.ds(0, rows)] = low_out
-        out[k, pl.ds(rows, rows)] = high_out
-        out[k, pl.ds(2 * rows, 8)] = stats
+        put(out, k, tiles)
 
 
 def k_combine(recv, sums, w_out, tails, out):
     devices = recv.shape[0]
-    rows = (recv.shape[1] - 8) // 2
+    tiles = (recv.shape[1] - 1) // 2
+    rows = 4 * tiles
     heads = 4 * DH
-    source = iota((LANES, 4 * heads), 0)
-    column = iota((LANES, 4 * heads), 1)
-    half = (column // heads) % 2
-    first = 32 * half + 8 * ((column % heads) // DH)
-    is_top = column < 2 * heads
+    source = iota((LANES, 2 * heads), 0) % 32
+    column = iota((LANES, 2 * heads), 1)
+    first = 8 * ((column % heads) // DH)
+    is_top = column < heads
     begin = jnp.where(is_top, first, first + 3)
     end = jnp.where(is_top, first + 3, first + 5)
     spread = jnp.where((source >= begin) & (source < end), 1.0, 0.0).astype(BF16)
-    stats = recv[:, pl.ds(2 * rows, 8), :].reshape(devices * 8, LANES)
-    wide = jnp.dot(stats, spread, preferred_element_type=F32).reshape(devices, 8, 4 * heads)
+    stats = recv[:, 2 * tiles].astype(F32)
+    stats = jnp.concatenate([stats, stats], axis=1)
+    group = iota(stats.shape, 2) // 32 - iota(stats.shape, 1) // 4
     blocks = []
     for half in range(2):
-        tops = wide[:, :, half * heads : (half + 1) * heads]
-        totals = wide[:, :, (2 + half) * heads : (3 + half) * heads]
+        mine = jnp.where(group == 2 * half, stats, 0.0).astype(BF16).reshape(devices * 8, LANES)
+        wide = jnp.dot(mine, spread, preferred_element_type=F32).reshape(devices, 8, 2 * heads)
+        tops = wide[:, :, :heads]
+        totals = wide[:, :, heads:]
         scales = jnp.exp(tops - jnp.max(tops, axis=0, keepdims=True))
         total = jnp.sum(totals * scales, axis=0)
-        low = recv[:, pl.ds(8 * half, 8), :].astype(F32)
-        high = recv[:, pl.ds(rows + 8 * half, 8), :].astype(F32)
-        low = jnp.sum(low * scales[:, :, :LANES], axis=0)
-        high = jnp.sum(high * scales[:, :, LANES:], axis=0)
-        blocks.append(jnp.concatenate([low, high], axis=1) / total)
+        sides = []
+        for side in range(2):
+            at = tiles * side + 2 * half
+            part = [recv[:, at + t].astype(F32) for t in range(2)]
+            part = jnp.concatenate(part, axis=1)
+            sides.append(jnp.sum(part * scales[:, :, side * LANES : (side + 1) * LANES], axis=0))
+        blocks.append(jnp.concatenate(sides, axis=1) / total)
     attended = jnp.concatenate(blocks, axis=0).astype(BF16)
     attn_part = jnp.dot(attended, w_out[...], preferred_element_type=F32).astype(BF16)
     wide = attended.astype(F32)
@@ -307,16 +319,15 @@
     mean_row = as_row(in_pieces(jnp.sum(mean, axis=1, keepdims=True), 2))
     row = iota((8, LANES), 0)
     tail = jnp.where(row == 0, mean_row, tails[1])
-    tail = tail.astype(BF16)
+    pieces = [*tiles_of(attn_part), tail[:4].astype(BF16)]
     for k in range(out.shape[0]):
-        out[k, pl.ds(0, rows)] = attn_part
-        out[k, pl.ds(rows, 8)] = tail
+        put(out, k, pieces)
 
 
 def k_expand(recv, x, tok, w_gate, w_up, out, scaled_out, tile):
     rows = x.shape[0]
-    added = summed(recv, 0, rows)
-    tail = summed(recv, rows, 8)
+    added = tiles_summed(recv, 0, rows // 4)
+    tail = tiles_summed(recv, rows // 4, 1)
     mean = as_column(tail[0:1], rows, (0, 1))
     gain = tail[1:2] + tail[2:3] + tail[3:4]
     centre = (tok[:, 0:1] + mean) / D
@@ -463,17 +474,18 @@
     )
     message, x = kernel(
         k_project,
-        [((kv, 2 * rows + 8, LANES), BF16), block],
+        [((kv, rows // 2 + 1, 4, LANES), BF16), block],
         [VMEM] * 6,
         [pltpu.VMEM((rows, LANES), F32)],
     )(recv, w_query, w_key, w_value, w_forget, tails)
     recv = exchanged(message, KV)
     positions = kv_cache.shape[1]
-    keys, values = kernel(
+    keys, values, gate_sums = kernel(
         k_prepare,
         [
-            ((rows // 2, 2 * DH + 16, positions), BF16),
+            ((rows // 2, 2 * DH, positions), BF16),
             ((rows // 2, positions, 2 * DH), BF16),
+            ((rows // 2, 8, positions), F32),
         ],
         [SMEM, ANY, ANY],
         [
@@ -485,11 +497,11 @@
     )(live_lengths, in_hbm(kv_cache), in_hbm(gate_sums))
     message, tok, sums = kernel(
         k_attend,
-        [((kv, 2 * rows + 8, LANES), BF16), block, ((2, LANES), F32)],
-        [VMEM] * 3,
+        [((kv, rows // 2 + 1, 4, LANES), BF16), block, ((2, LANES), F32)],
+        [VMEM] * 4,
         [pltpu.VMEM((4 * rows, LANES), F32), pltpu.VMEM((4 * rows, LANES), F32)],
-    )(recv, keys, values)
-    (message,) = kernel(k_combine, [((tp, rows + 8, width), BF16)], [VMEM] * 4)(
+    )(recv, keys, values, gate_sums)
+    (message,) = kernel(k_combine, [((tp, rows // 4 + 1, 4, width), BF16)], [VMEM] * 4)(
         exchanged(message, KV), sums, w_out, tails
     )
     message, scaled = kernel(

time: 128 us -> 127 us (level)
  no operation moved by 1% of the time
where the time goes in v6:
time: 127 us; the launch traced here: 126 us
  blocking collectives  78 us (61%)
  starting transfers between devices  21.4 us (17%)
  waiting for transfers between devices  14.1 us (11%)
  Pallas kernels  10.8 us (9%)
  local copies, waits for them, and re-layouts  1.95 us (2%)
    all_to_all x6, blocking collectives, exchanged(): return lax.all_to_all(pieces, axis, 0, 0, tiled=True)  78 us
    all_to_all x2, starting transfers between devices, exchanged(): return lax.all_to_all(pieces, axis, 0, 0, tiled=True)  21.4 us
    all_to_all x2, waiting for transfers between devices, exchanged(): return lax.all_to_all(pieces, axis, 0, 0, tiled=True)  14.1 us
    pallas_call x1, Pallas kernels, on_device(): kernel(k_prepare, [((rows // 2, 2 * DH, positions), BF16), ((rows // 2, p...  3.91 us
  transfers between devices with their start and end apart: 2, of which 2 were waited for; matrix products, arithmetic and copies ran while one was open for 0% of the time, Pallas kernels for 4%

profile of v6, /device:TPU:1, one launch (start us, length us, event | category | flops | bytes accessed | tf_op | source)
XLA Modules:
  0.0 126.4 jit_solution(9362751489215961655)
XLA Ops:
  0.0 1.3 %broadcast_in_dim.15 = bf16[16,8,16]{2,1,0:T(8,128)(2,1)} broadcast(bf16[8,16]{1,0:T(8,128)(2,1)} %bitcast.18), dimensions={1,2} | broadcast | bytes 4352 | tf_op jit(solution)/shard_map/broadcast_in_dim | solution.py:446
  1.3 10.1 %all-to-all-start = ((bf16[16,8,16]{2,1,0:T(8,128)(2,1)}), bf16[16,8,16]{2,1,0:T(8,128)(2,1)S(1)}, u32[]{:S(2)}, u32[]{:S(2)}) async-start(bf16[16,8,16]{2,1,0:T(8,128)(2,1)} %broadcast_in_dim.15), calls=%async_computation | async-start | bytes 65536 | tf_op jit(solution)/shard_map/all_to_all | solution.py:41
  11.4 1.1 shard_map.145
  12.5 6.4 %all-to-all-done = bf16[16,8,16]{2,1,0:T(8,128)(2,1)S(1)} async-done(((bf16[16,8,16]{2,1,0:T(8,128)(2,1)}), bf16[16,8,16]{2,1,0:T(8,128)(2,1)S(1)}, u32[]{:S(2)}, u32[]{:S(2)}) %all-to-all-start) | async-done | bytes 4128 | tf_op jit(solution)/shard_map/all_to_all | solution.py:41
  18.9 1.2 shard_map.146
  20.1 11.3 %all-to-all-start.1 = ((bf16[32,9,4,128]{3,2,1,0:T(4,128)(2,1)}), bf16[32,9,4,128]{3,2,1,0:T(4,128)(2,1)S(1)}, u32[]{:S(2)}, u32[]{:S(2)}) async-start(bf16[32,9,4,128]{3,2,1,0:T(4,128)(2,1)} %get-tuple-element.30), calls=%async_computation.1 | async-start | bytes 589824 | tf_op jit(solution)/shard_map/all_to_all | solution.py:41
  31.4 0.0 copy-start.3
  31.4 0.6 copy-done.3
  32.0 3.9 %shard_map.147 = (bf16[8,128,512]{2,1,0:T(8,128)(2,1)S(1)}, bf16[8,512,128]{2,1,0:T(8,128)(2,1)S(1)}, f32[8,8,512]{2,1,0:T(8,128)S(1)}) custom-call(s32[16]{0:T(128)S(1)} %copy-done.3, bf16[16,512,128]{2,1,0:T(8,128)(2,1)} %cache.1, f32[16,1,512]{2,1,0:T(1,128)} %gate.1), custom_call_target="tpu_custom_call" | custom-call | tf_op jit(solution)/shard_map/pallas_call | solution.py:483
  36.0 0.0 copy-start
  36.0 0.0 copy-start.1
  36.0 7.7 %all-to-all-done.1.recv = bf16[32,9,4,128]{3,2,1,0:T(4,128)(2,1)S(1)} async-done(((bf16[32,9,4,128]{3,2,1,0:T(4,128)(2,1)}), bf16[32,9,4,128]{3,2,1,0:T(4,128)(2,1)S(1)}, u32[]{:S(2)}, u32[]{:S(2)}) %all-to-all-start.1) | async-done | bytes 294944 | tf_op jit(solution)/shard_map/all_to_all | solution.py:41
  43.7 0.0 copy-start.2
  43.7 0.0 copy-start.4
  43.7 2.3 %shard_map.148 = (bf16[32,9,4,128]{3,2,1,0:T(4,128)(2,1)S(1)}, f32[16,128]{1,0:T(8,128)S(1)}, f32[2,128]{1,0:T(2,128)S(1)}) custom-call(bf16[32,9,4,128]{3,2,1,0:T(4,128)(2,1)S(1)} %all-to-all-done.1.recv, bf16[8,128,512]{2,1,0:T(8,128)(2,1)S(1)} %get-tuple-element.31.keys, bf16[8,512,128]{2,1,0:T(8,128)(2,1)S(1)} %get-tuple-element.32.values, ...), custom_call_target="tpu_custom_call" | custom-call | tf_op jit(solution)/shard_map/pallas_call | solution.py:498
  46.0 15.2 %all_to_all.40.recv = bf16[32,9,4,128]{3,2,1,0:T(4,128)(2,1)S(1)} all-to-all(bf16[32,9,4,128]{3,2,1,0:T(4,128)(2,1)S(1)} %get-tuple-element.34), channel_id=1, replica_groups=mesh['kv_0'=8,'kv_1'=4,'tp'=16] {'kv_0','kv_1'}, dimensions={0} | all-to-all | bytes 589824 | tf_op jit(solution)/shard_map/all_to_all | solution.py:41
  61.2 0.6 shard_map.149
  61.8 14.2 %all_to_all.41.recv = bf16[16,5,4,128]{3,2,1,0:T(4,128)(2,1)S(1)} all-to-all(bf16[16,5,4,128]{3,2,1,0:T(4,128)(2,1)S(1)} %shard_map.149), channel_id=1, replica_groups=mesh['kv_0'=8,'kv_1'=4,'tp'=16] {'tp'}, dimensions={0} | all-to-all | bytes 163840 | tf_op jit(solution)/shard_map/all_to_all | solution.py:41
  76.0 0.0 copy-done
  76.0 0.0 copy-done.1
  76.0 0.4 shard_map.150
  76.4 12.4 %all_to_all.42.recv = bf16[32,8,128]{2,1,0:T(8,128)(2,1)S(1)} all-to-all(bf16[32,8,128]{2,1,0:T(8,128)(2,1)S(1)} %get-tuple-element.39), channel_id=1, replica_groups=mesh['kv_0'=8,'kv_1'=4,'tp'=16] {'kv_0','kv_1'}, dimensions={0} | all-to-all | bytes 131072 | tf_op jit(solution)/shard_map/all_to_all | solution.py:41
  88.8 0.1 shard_map.151
  88.9 11.9 %all_to_all.43.recv = bf16[32,8,128]{2,1,0:T(8,128)(2,1)S(1)} all-to-all(bf16[32,8,128]{2,1,0:T(8,128)(2,1)S(1)} %get-tuple-element.41), channel_id=1, replica_groups=mesh['kv_0'=8,'kv_1'=4,'tp'=16] {'kv_0','kv_1'}, dimensions={0} | all-to-all | bytes 131072 | tf_op jit(solution)/shard_map/all_to_all | solution.py:41
  100.8 0.0 copy-done.2
  100.8 0.2 shard_map.152
  101.0 12.8 %all_to_all.44.recv = bf16[16,16,128]{2,1,0:T(8,128)(2,1)S(1)} all-to-all(bf16[16,16,128]{2,1,0:T(8,128)(2,1)S(1)} %shard_map.152), channel_id=1, replica_groups=mesh['kv_0'=8,'kv_1'=4,'tp'=16] {'tp'}, dimensions={0} | all-to-all | bytes 131072 | tf_op jit(solution)/shard_map/all_to_all | solution.py:41
  113.8 0.2 shard_map.153
  113.9 11.6 %all_to_all.45.recv = f32[32,1,128]{2,1,0:T(1,128)S(1)} all-to-all(f32[32,1,128]{2,1,0:T(1,128)S(1)} %get-tuple-element.43), channel_id=1, replica_groups=mesh['kv_0'=8,'kv_1'=4,'tp'=16] {'kv_0','kv_1'}, dimensions={0} | all-to-all | bytes 32768 | tf_op jit(solution)/shard_map/all_to_all | solution.py:41
  125.5 0.0 copy-done.4
  125.5 0.8 shard_map.154
Async XLA Ops:
  1.3 17.6 %all-to-all-start = ((bf16[16,8,16]{2,1,0:T(8,128)(2,1)}), bf16[16,8,16]{2,1,0:T(8,128)(2,1)S(1)}, u32[]{:S(2)}, u32[]{:S(2)}) async-start(bf16[16,8,16]{2,1,0:T(8,128)(2,1)} %broadcast_in_dim.15), calls=%async_computation | async-start | bytes 65536 | tf_op jit(solution)/shard_map/all_to_all | solution.py:41
  20.1 23.6 %all-to-all-start.1 = ((bf16[32,9,4,128]{3,2,1,0:T(4,128)(2,1)}), bf16[32,9,4,128]{3,2,1,0:T(4,128)(2,1)S(1)}, u32[]{:S(2)}, u32[]{:S(2)}) async-start(bf16[32,9,4,128]{3,2,1,0:T(4,128)(2,1)} %get-tuple-element.30), calls=%async_computation.1 | async-start | bytes 589824 | tf_op jit(solution)/shard_map/all_to_all | solution.py:41
  31.4 0.7 copy-start.3
  36.0 40.0 %copy-start = (bf16[128,704]{0,1:T(8,128)(2,1)S(1)}, bf16[128,704]{0,1:T(8,128)(2,1)}, u32[]{:S(2)}) copy-start(bf16[128,704]{0,1:T(8,128)(2,1)} %param.26) | copy-start | bytes 540676
  36.0 40.0 %copy-start.1 = (bf16[128,704]{0,1:T(8,128)(2,1)S(1)}, bf16[128,704]{0,1:T(8,128)(2,1)}, u32[]{:S(2)}) copy-start(bf16[128,704]{0,1:T(8,128)(2,1)} %param.27) | copy-start | bytes 540676
  43.7 57.1 %copy-start.2 = (bf16[704,128]{1,0:T(8,128)(2,1)S(1)}, bf16[704,128]{1,0:T(8,128)(2,1)}, u32[]{:S(2)}) copy-start(bf16[704,128]{1,0:T(8,128)(2,1)} %w_down.1) | copy-start | bytes 540676
  43.7 81.9 %copy-start.4 = (f32[8]{0:T(128)S(1)}, f32[8]{0:T(128)}, u32[]{:S(2)}) copy-start(f32[8]{0:T(128)} %param.29) | copy-start | bytes 100

commit v7 on v6

--- a/solution.py
+++ b/solution.py
@@ -199,18 +199,18 @@
     for m in range(rows // 2):
         one = jnp.where(place < lengths[2 * m], gate_v[2 * m], EMPTY_SCORE)
         two = jnp.where(place < lengths[2 * m + 1], gate_v[2 * m + 1], EMPTY_SCORE)
-        gate_o[m] = jnp.where(first, one, two)
+        gate_o[m // 2, pl.ds(8 * (m % 2), 8), :] = jnp.where(first, one, two)
     for b in range(rows):
         copies[b].wait()
-        keys_o[b // 2, pl.ds(DH * (b % 2), DH), :] = cache_v[b].T[:DH]
+        keys_o[b // 4, pl.ds(DH * (b % 4), DH), :] = cache_v[b].T[:DH]
         if b % 2:
-            values_o[b // 2] = jnp.concatenate(
+            values_o[b // 4, :, pl.ds(LANES * (b % 4 // 2), LANES)] = jnp.concatenate(
                 [cache_v[b - 1][:, DH:], cache_v[b][:, DH:]], axis=1
             )
 
 
 def k_attend(recv, keys, values, gate, out, tok_out, sums_out, qs, os):
-    rows = 2 * keys.shape[0]
+    rows = 4 * keys.shape[0]
     heads = 4
     scale = DH**-0.5
     left = rounded(tiles_summed(recv, 0, rows // 4))
@@ -246,11 +246,14 @@
     own = jnp.sum(qs[...] * new_key, axis=1, keepdims=True) * scale
     mine = iota((all_rows, 1), 0) // heads == kv_index()
     own = jnp.where(mine, own, EMPTY_SCORE)
-    lane = iota((8, LANES), 1)
-    spot = jnp.where(iota((8, LANES), 0) < heads, DH, 0)
-    for m in range(rows // 2):
-        at = slice(8 * m, 8 * m + 8)
-        query = (qs[pl.ds(8 * m, 8), :] * scale).astype(BF16)
+    lane = iota((16, LANES), 1)
+    spot = jnp.where(iota((16, LANES), 0) % 8 < heads, DH, 0)
+    upper = iota((16, LANES), 0) < 8
+    for m in range(rows // 4):
+        at = slice(16 * m, 16 * m + 16)
+        query = qs[pl.ds(16 * m, 16), :] * scale
+        query = [jnp.where(upper, query, 0.0), jnp.where(upper, 0.0, query)]
+        query = jnp.concatenate(query, axis=1).astype(BF16)
         scores = jnp.dot(query, keys[m], preferred_element_type=F32)
         scores = scores + (gate[m] + new_gate[at])
         top = jnp.maximum(jnp.max(scores, axis=1, keepdims=True), own[at])
@@ -259,9 +262,10 @@
         own_weight = jnp.exp(own[at] - top)
         total = jnp.sum(weights, axis=1, keepdims=True) + own_weight
         value = jnp.dot(weights.astype(BF16), values[m], preferred_element_type=F32)
+        value = jnp.where(upper, value[:, :LANES], value[:, LANES:])
         value = value + rounded(own_weight) * new_value
         spare = jnp.where(lane == spot, top, jnp.where(lane == spot + 1, total, value))
-        os[pl.ds(8 * m, 8), :] = spare
+        os[pl.ds(16 * m, 16), :] = spare
     blocks = [os[pl.ds(h, rows, stride=heads), :] for h in range(heads)]
     turned = [pltpu.roll(block, DH, 1) for block in blocks]
     firsts = [jnp.where(even, block, turn) for block, turn in zip(blocks, turned)]
@@ -366,7 +370,7 @@
     total = total * own
     up = pltpu.roll(total, 5, 0)
     hidden = total / (1.0 + jnp.exp(-total)) * up
-    hidden = jnp.where(iota((8, LANES), 0) < 3, hidden, 0.0).astype(BF16)
+    hidden = jnp.where(iota((8, LANES), 0) < 3, hidden, 0.0)[:4].astype(BF16)
     for k in range(out.shape[0]):
         out[k] = hidden
 
@@ -375,13 +379,13 @@
     rows = out.shape[1]
     pieces = recv.shape[0] // rows
     for k in range(recv.shape[0]):
-        tile[pl.ds(8 * k, 8), :] = recv[k].astype(F32)
+        tile[pl.ds(4 * k, 4), :] = recv[k].astype(F32)
     part = jnp.zeros((rows, LANES), F32)
     columns = w_down.shape[0]
     for t in range(3 * pieces):
-        at = 8 * (t // 3) + t % 3
+        at = 4 * (t // 3) + t % 3
         size = min(LANES, columns - t * LANES)
-        hidden = tile[pl.ds(at, rows, stride=8 * pieces), :][:, :size].astype(BF16)
+        hidden = tile[pl.ds(at, rows, stride=4 * pieces), :][:, :size].astype(BF16)
         part = part + jnp.dot(
             hidden, w_down[pl.ds(t * LANES, size), :], preferred_element_type=F32
         )
@@ -483,9 +487,9 @@
     keys, values, gate_sums = kernel(
         k_prepare,
         [
-            ((rows // 2, 2 * DH, positions), BF16),
-            ((rows // 2, positions, 2 * DH), BF16),
-            ((rows // 2, 8, positions), F32),
+            ((rows // 4, 4 * DH, positions), BF16),
+            ((rows // 4, positions, 4 * DH), BF16),
+            ((rows // 4, 16, positions), F32),
         ],
         [SMEM, ANY, ANY],
         [
@@ -510,11 +514,11 @@
         [VMEM] * 5,
         [pltpu.VMEM((8 * kv, LANES), F32)],
     )(exchanged(message, "tp"), x, tok, w_gate.T, w_up.T)
-    message, mid = kernel(k_hidden, [((kv, 8, LANES), BF16), block], [VMEM] * 2)(
+    message, mid = kernel(k_hidden, [((kv, 4, LANES), BF16), block], [VMEM] * 2)(
         exchanged(message, KV), scaled
     )
     (message,) = kernel(
-        k_shrink, [((tp, rows, width), BF16)], [VMEM] * 2, [pltpu.VMEM((8 * kv, LANES), F32)]
+        k_shrink, [((tp, rows, width), BF16)], [VMEM] * 2, [pltpu.VMEM((4 * kv, LANES), F32)]
     )(exchanged(message, KV), w_down)
     message, mix = kernel(k_sums, [((kv, 1, LANES), F32), block], [VMEM] * 2)(
         exchanged(message, "tp"), mid

time: 127 us -> 126 us (level)
  no operation moved by 1% of the time
where the time goes in v7:
time: 126 us; the launch traced here: 125 us
  blocking collectives  77.9 us (62%)
  starting transfers between devices  21.4 us (17%)
  waiting for transfers between devices  14.1 us (11%)
  Pallas kernels  10 us (8%)
  local copies, waits for them, and re-layouts  1.95 us (2%)
    all_to_all x6, blocking collectives, exchanged(): return lax.all_to_all(pieces, axis, 0, 0, tiled=True)  77.9 us
    all_to_all x2, starting transfers between devices, exchanged(): return lax.all_to_all(pieces, axis, 0, 0, tiled=True)  21.4 us
    all_to_all x2, waiting for transfers between devices, exchanged(): return lax.all_to_all(pieces, axis, 0, 0, tiled=True)  14.1 us
    pallas_call x1, Pallas kernels, on_device(): kernel(k_prepare, [((rows // 4, 4 * DH, positions), BF16), ((rows // 4, p...  3.91 us
  transfers between devices with their start and end apart: 2, of which 2 were waited for; matrix products, arithmetic and copies ran while one was open for 0% of the time, Pallas kernels for 4%

profile of v7, /device:TPU:1, one launch (start us, length us, event | category | flops | bytes accessed | tf_op | source)
XLA Modules:
  0.0 125.4 jit_solution(2714748704812861971)
XLA Ops:
  0.0 1.3 %broadcast_in_dim.15 = bf16[16,8,16]{2,1,0:T(8,128)(2,1)} broadcast(bf16[8,16]{1,0:T(8,128)(2,1)} %bitcast.18), dimensions={1,2} | broadcast | bytes 4352 | tf_op jit(solution)/shard_map/broadcast_in_dim | solution.py:450
  1.3 10.1 %all-to-all-start = ((bf16[16,8,16]{2,1,0:T(8,128)(2,1)}), bf16[16,8,16]{2,1,0:T(8,128)(2,1)S(1)}, u32[]{:S(2)}, u32[]{:S(2)}) async-start(bf16[16,8,16]{2,1,0:T(8,128)(2,1)} %broadcast_in_dim.15), calls=%async_computation | async-start | bytes 65536 | tf_op jit(solution)/shard_map/all_to_all | solution.py:41
  11.4 1.1 shard_map.145
  12.5 6.4 %all-to-all-done = bf16[16,8,16]{2,1,0:T(8,128)(2,1)S(1)} async-done(((bf16[16,8,16]{2,1,0:T(8,128)(2,1)}), bf16[16,8,16]{2,1,0:T(8,128)(2,1)S(1)}, u32[]{:S(2)}, u32[]{:S(2)}) %all-to-all-start) | async-done | bytes 4128 | tf_op jit(solution)/shard_map/all_to_all | solution.py:41
  18.9 1.2 shard_map.146
  20.1 11.3 %all-to-all-start.1 = ((bf16[32,9,4,128]{3,2,1,0:T(4,128)(2,1)}), bf16[32,9,4,128]{3,2,1,0:T(4,128)(2,1)S(1)}, u32[]{:S(2)}, u32[]{:S(2)}) async-start(bf16[32,9,4,128]{3,2,1,0:T(4,128)(2,1)} %get-tuple-element.30), calls=%async_computation.1 | async-start | bytes 589824 | tf_op jit(solution)/shard_map/all_to_all | solution.py:41
  31.4 0.0 copy-start.3
  31.4 0.6 copy-done.3
  32.0 3.9 %shard_map.147 = (bf16[4,256,512]{2,1,0:T(8,128)(2,1)S(1)}, bf16[4,512,256]{2,1,0:T(8,128)(2,1)S(1)}, f32[4,16,512]{2,1,0:T(8,128)S(1)}) custom-call(s32[16]{0:T(128)S(1)} %copy-done.3, bf16[16,512,128]{2,1,0:T(8,128)(2,1)} %cache.1, f32[16,1,512]{2,1,0:T(1,128)} %gate.1), custom_call_target="tpu_custom_call" | custom-call | tf_op jit(solution)/shard_map/pallas_call | solution.py:487
  36.0 0.0 copy-start
  36.0 0.0 copy-start.1
  36.0 7.7 %all-to-all-done.1.recv = bf16[32,9,4,128]{3,2,1,0:T(4,128)(2,1)S(1)} async-done(((bf16[32,9,4,128]{3,2,1,0:T(4,128)(2,1)}), bf16[32,9,4,128]{3,2,1,0:T(4,128)(2,1)S(1)}, u32[]{:S(2)}, u32[]{:S(2)}) %all-to-all-start.1) | async-done | bytes 294944 | tf_op jit(solution)/shard_map/all_to_all | solution.py:41
  43.7 0.0 copy-start.2
  43.7 0.0 copy-start.4
  43.7 1.5 %shard_map.148 = (bf16[32,9,4,128]{3,2,1,0:T(4,128)(2,1)S(1)}, f32[16,128]{1,0:T(8,128)S(1)}, f32[2,128]{1,0:T(2,128)S(1)}) custom-call(bf16[32,9,4,128]{3,2,1,0:T(4,128)(2,1)S(1)} %all-to-all-done.1.recv, bf16[4,256,512]{2,1,0:T(8,128)(2,1)S(1)} %get-tuple-element.31.keys, bf16[4,512,256]{2,1,0:T(8,128)(2,1)S(1)} %get-tuple-element.32.values, ...), custom_call_target="tpu_custom_call" | custom-call | tf_op jit(solution)/shard_map/pallas_call | solution.py:502
  45.2 15.2 %all_to_all.40.recv = bf16[32,9,4,128]{3,2,1,0:T(4,128)(2,1)S(1)} all-to-all(bf16[32,9,4,128]{3,2,1,0:T(4,128)(2,1)S(1)} %get-tuple-element.34), channel_id=1, replica_groups=mesh['kv_0'=8,'kv_1'=4,'tp'=16] {'kv_0','kv_1'}, dimensions={0} | all-to-all | bytes 589824 | tf_op jit(solution)/shard_map/all_to_all | solution.py:41
  60.4 0.6 shard_map.149
  61.0 14.2 %all_to_all.41.recv = bf16[16,5,4,128]{3,2,1,0:T(4,128)(2,1)S(1)} all-to-all(bf16[16,5,4,128]{3,2,1,0:T(4,128)(2,1)S(1)} %shard_map.149), channel_id=1, replica_groups=mesh['kv_0'=8,'kv_1'=4,'tp'=16] {'tp'}, dimensions={0} | all-to-all | bytes 163840 | tf_op jit(solution)/shard_map/all_to_all | solution.py:41
  75.2 0.0 copy-done
  75.2 0.0 copy-done.1
  75.2 0.4 shard_map.150
  75.6 12.4 %all_to_all.42.recv = bf16[32,8,128]{2,1,0:T(8,128)(2,1)S(1)} all-to-all(bf16[32,8,128]{2,1,0:T(8,128)(2,1)S(1)} %get-tuple-element.39), channel_id=1, replica_groups=mesh['kv_0'=8,'kv_1'=4,'tp'=16] {'kv_0','kv_1'}, dimensions={0} | all-to-all | bytes 131072 | tf_op jit(solution)/shard_map/all_to_all | solution.py:41
  88.0 0.2 shard_map.151
  88.2 11.7 %all_to_all.43.recv = bf16[32,4,128]{2,1,0:T(4,128)(2,1)S(1)} all-to-all(bf16[32,4,128]{2,1,0:T(4,128)(2,1)S(1)} %get-tuple-element.41), channel_id=1, replica_groups=mesh['kv_0'=8,'kv_1'=4,'tp'=16] {'kv_0','kv_1'}, dimensions={0} | all-to-all | bytes 65536 | tf_op jit(solution)/shard_map/all_to_all | solution.py:41
  99.8 0.0 copy-done.2
  99.8 0.2 shard_map.152
  100.0 12.8 %all_to_all.44.recv = bf16[16,16,128]{2,1,0:T(8,128)(2,1)S(1)} all-to-all(bf16[16,16,128]{2,1,0:T(8,128)(2,1)S(1)} %shard_map.152), channel_id=1, replica_groups=mesh['kv_0'=8,'kv_1'=4,'tp'=16] {'tp'}, dimensions={0} | all-to-all | bytes 131072 | tf_op jit(solution)/shard_map/all_to_all | solution.py:41
  112.8 0.2 shard_map.153
  113.0 11.6 %all_to_all.45.recv = f32[32,1,128]{2,1,0:T(1,128)S(1)} all-to-all(f32[32,1,128]{2,1,0:T(1,128)S(1)} %get-tuple-element.43), channel_id=1, replica_groups=mesh['kv_0'=8,'kv_1'=4,'tp'=16] {'kv_0','kv_1'}, dimensions={0} | all-to-all | bytes 32768 | tf_op jit(solution)/shard_map/all_to_all | solution.py:41
  124.6 0.0 copy-done.4
  124.6 0.8 shard_map.154
Async XLA Ops:
  1.3 17.6 %all-to-all-start = ((bf16[16,8,16]{2,1,0:T(8,128)(2,1)}), bf16[16,8,16]{2,1,0:T(8,128)(2,1)S(1)}, u32[]{:S(2)}, u32[]{:S(2)}) async-start(bf16[16,8,16]{2,1,0:T(8,128)(2,1)} %broadcast_in_dim.15), calls=%async_computation | async-start | bytes 65536 | tf_op jit(solution)/shard_map/all_to_all | solution.py:41
  20.1 23.6 %all-to-all-start.1 = ((bf16[32,9,4,128]{3,2,1,0:T(4,128)(2,1)}), bf16[32,9,4,128]{3,2,1,0:T(4,128)(2,1)S(1)}, u32[]{:S(2)}, u32[]{:S(2)}) async-start(bf16[32,9,4,128]{3,2,1,0:T(4,128)(2,1)} %get-tuple-element.30), calls=%async_computation.1 | async-start | bytes 589824 | tf_op jit(solution)/shard_map/all_to_all | solution.py:41
  31.4 0.7 copy-start.3
  36.0 39.2 %copy-start = (bf16[128,704]{0,1:T(8,128)(2,1)S(1)}, bf16[128,704]{0,1:T(8,128)(2,1)}, u32[]{:S(2)}) copy-start(bf16[128,704]{0,1:T(8,128)(2,1)} %param.26) | copy-start | bytes 540676
  36.0 39.2 %copy-start.1 = (bf16[128,704]{0,1:T(8,128)(2,1)S(1)}, bf16[128,704]{0,1:T(8,128)(2,1)}, u32[]{:S(2)}) copy-start(bf16[128,704]{0,1:T(8,128)(2,1)} %param.27) | copy-start | bytes 540676
  43.7 56.2 %copy-start.2 = (bf16[704,128]{1,0:T(8,128)(2,1)S(1)}, bf16[704,128]{1,0:T(8,128)(2,1)}, u32[]{:S(2)}) copy-start(bf16[704,128]{1,0:T(8,128)(2,1)} %w_down.1) | copy-start | bytes 540676
  43.7 80.9 %copy-start.4 = (f32[8]{0:T(128)S(1)}, f32[8]{0:T(128)}, u32[]{:S(2)}) copy-start(f32[8]{0:T(128)} %param.29) | copy-start | bytes 100

commit v8 on v7

--- a/solution.py
+++ b/solution.py
@@ -23,7 +23,7 @@
 ANY = pl.BlockSpec(memory_space=pl.ANY)
 
 
-def kernel(body, outs, specs, scratch=(), last=False):
+def kernel(body, outs, specs, scratch=(), last=False, flops=None):
     return pl.pallas_call(
         body,
         out_shape=[
@@ -33,6 +33,8 @@
         in_specs=specs,
         out_specs=[VMEM] * len(outs),
         scratch_shapes=scratch,
+        cost_estimate=flops
+        and pl.CostEstimate(flops=flops, bytes_accessed=flops // 100, transcendentals=0),
         compiler_params=pltpu.CompilerParams(vmem_limit_bytes=8 * 2**20),
     )
 
@@ -115,70 +117,52 @@
     return tiles[0] if count == 1 else jnp.concatenate(tiles, axis=0)
 
 
-def k_weights(
-    query,
-    key,
-    value,
-    forget,
-    w_out,
-    gain_hbm,
-    bias_hbm,
-    query_o,
-    key_o,
-    value_o,
-    forget_o,
-    w_out_o,
-    tail_o,
-    gain,
-    bias,
-    sem,
-):
-    width = forget_o.shape[1]
-    start = pl.multiple_of(kv_index() * width, width)
-    pairs = [(w_out, w_out_o), (query, query_o), (key, key_o), (value, value_o)]
-    pairs.append((forget.at[:, pl.ds(start, width)], forget_o))
-    pairs.extend([(gain_hbm, gain), (bias_hbm, bias)])
+def k_start(turned_hbm, gain_hbm, out, turned, gain, sem):
+    pairs = ((turned_hbm, turned), (gain_hbm, gain))
     copies = [pltpu.make_async_copy(a, b, sem.at[k]) for k, (a, b) in enumerate(pairs)]
     for copy in copies:
         copy.start()
-    row = iota((8, LANES), 0)
     for copy in copies:
         copy.wait()
-    own = gain.shape[1]
-    place = iota((own, LANES), 0) + lax.axis_index("tp") * own
-    spread = jnp.where(iota((own, LANES), 1) == place, 1.0, 0.0)
+    own, rows = turned.shape
     column = jnp.sum(jnp.where(diagonal(own, 0)[:, :own], gain[...], 0.0), axis=1, keepdims=True)
-    gains = in_pieces(jnp.sum(spread * column, axis=0, keepdims=True), 3)
-    sums = across(jnp.ones((8, LANES), BF16), w_out_o[...], LAST)
-    tail = jnp.where(row == 2, sums[:, :LANES], 0.0)
-    tail_o[0] = jnp.where(row == 3, sums[:, LANES:], tail)
+    pad = jnp.zeros((own, LANES - rows), F32)
+    tile = jnp.concatenate([turned[...].astype(F32), pad], axis=1)
+    for k, piece in enumerate(in_pieces(column, 3)):
+        tile = jnp.where(iota(tile.shape, 1) == rows + k, piece, tile)
+    tile = tile.astype(BF16)
+    for k in range(out.shape[0]):
+        out[k] = tile
+
+
+def k_project(recv, w_query, w_key, w_value, w_forget, w_out, bias, out, x_out, gain_out, new_rows):
+    width = recv.shape[0]
+    same = jnp.where(iota((width, width), 0) == iota((width, width), 1), 1.0, 0.0).astype(BF16)
+    rows = new_rows.shape[0]
+    both = across(recv[:, : 2 * rows], same, FIRST)
+    x = both[:rows]
+    x_out[...] = x
+    gain = both[rows : rows + 1] + both[rows + 1 : rows + 2] + both[rows + 2 : rows + 3]
+    gain_out[...] = jnp.broadcast_to(gain, gain_out.shape)
+    xb = x.astype(BF16)
+    row = iota((8, LANES), 0)
+    sums = across(jnp.ones((8, LANES), BF16), w_out[...], LAST)
     mine = iota(bias.shape, 1) == lax.axis_index("tp")
     once = jnp.where(kv_index() == 0, 1.0, 0.0)
     own_bias = jnp.sum(jnp.where(mine, bias[...], 0.0), axis=1, keepdims=True) * once
-    tail = jnp.where(row == 0, own_bias, 0.0)
-    for k, piece in enumerate(gains):
-        tail = jnp.where(row == 1 + k, piece, tail)
-    tail_o[1] = tail
-
-
-def k_project(recv, w_query, w_key, w_value, wf, tails, out, x_out, new_rows):
-    width = wf.shape[1]
-    same = jnp.where(iota((width, width), 0) == iota((width, width), 1), 1.0, 0.0).astype(BF16)
-    x = across(recv[...], same, FIRST)
-    x_out[...] = x
-    rows = x.shape[0]
-    xb = x.astype(BF16)
     query = jnp.dot(xb, w_query[...], preferred_element_type=F32)
     new_rows[:, :DH] = across(xb, w_key[...], LAST)
     new_rows[:, DH:] = across(xb, w_value[...], LAST)
-    forget = across(xb, wf[...], LAST)
+    start = pl.multiple_of(kv_index() * width, width)
+    forget = across(xb, w_forget[:, pl.ds(start, width)], LAST)
     token_col = jnp.sum(x, axis=1, keepdims=True)
     mine = iota(forget.shape, 1) == lax.axis_index("tp")
     forget_col = jnp.sum(jnp.where(mine, forget, 0.0), axis=1, keepdims=True)
-    forget_col = forget_col + tails[1, 0:1, 0:1]
+    forget_col = forget_col + own_bias
     small = as_row([*in_pieces(forget_col, 2), *in_pieces(token_col, 2)])
-    row = iota((8, LANES), 0)
-    tail = jnp.where(row == 1, small, tails[0])
+    tail = jnp.where(row == 1, small, 0.0)
+    tail = jnp.where(row == 2, sums[:, :LANES], tail)
+    tail = jnp.where(row == 3, sums[:, LANES:], tail)
     tiles = tiles_of(query[:, :LANES].astype(BF16)) + tiles_of(query[:, LANES:].astype(BF16))
     for b in range(rows):
         own_tail = jnp.where(row == 0, new_rows[pl.ds(b, 1), :], tail)[:4].astype(BF16)
@@ -286,7 +270,7 @@
         put(out, k, tiles)
 
 
-def k_combine(recv, sums, w_out, tails, out):
+def k_combine(recv, sums, w_out, out):
     devices = recv.shape[0]
     tiles = (recv.shape[1] - 1) // 2
     rows = 4 * tiles
@@ -317,26 +301,19 @@
             sides.append(jnp.sum(part * scales[:, :, side * LANES : (side + 1) * LANES], axis=0))
         blocks.append(jnp.concatenate(sides, axis=1) / total)
     attended = jnp.concatenate(blocks, axis=0).astype(BF16)
-    attn_part = jnp.dot(attended, w_out[...], preferred_element_type=F32).astype(BF16)
     wide = attended.astype(F32)
     mean = wide[:, :LANES] * sums[0:1, :] + wide[:, LANES:] * sums[1:2, :]
-    mean_row = as_row(in_pieces(jnp.sum(mean, axis=1, keepdims=True), 2))
-    row = iota((8, LANES), 0)
-    tail = jnp.where(row == 0, mean_row, tails[1])
-    pieces = [*tiles_of(attn_part), tail[:4].astype(BF16)]
-    for k in range(out.shape[0]):
-        put(out, k, pieces)
-
-
-def k_expand(recv, x, tok, w_gate, w_up, out, scaled_out, tile):
+    mean = jnp.sum(mean, axis=1, keepdims=True) / D
+    attn_part = jnp.dot(attended, w_out[...], preferred_element_type=F32)
+    attn_part = (attn_part - mean).astype(BF16)
+    for k in range(out.shape[0]):
+        out[k] = attn_part
+
+
+def k_expand(recv, x, tok, gain, w_gate, w_up, out, scaled_out, tile):
     rows = x.shape[0]
-    added = tiles_summed(recv, 0, rows // 4)
-    tail = tiles_summed(recv, rows // 4, 1)
-    mean = as_column(tail[0:1], rows, (0, 1))
-    gain = tail[1:2] + tail[2:3] + tail[3:4]
-    centre = (tok[:, 0:1] + mean) / D
-    centred = x[...] + added - centre
-    scaled = centred * gain
+    centred = x[...] - tok[:, 0:1] / D + summed(recv, 0, rows)
+    scaled = centred * gain[0:1, :]
     scaled_out[...] = scaled
     squares = as_row(in_pieces(jnp.sum(centred * centred, axis=1, keepdims=True), 2))
     scaled = scaled.astype(BF16)
@@ -447,41 +424,33 @@
     kv, tp = lax.axis_size(KV), lax.axis_size("tp")
     width = own * tp
     block = ((rows, LANES), F32)
-    message = jnp.broadcast_to(tokens.T[None], (tp, own, rows))
     in_hbm = functools.partial(pltpu.with_memory_space_constraint, memory_space=pltpu.HBM)
-    recv = exchanged(message, "tp").reshape(width, rows)
-    heads = w_query.shape[1]
-    w_query, w_key, w_value, w_forget, w_out, tails = kernel(
-        k_weights,
+    (message,) = kernel(
+        k_start,
+        [((tp, own, LANES), BF16)],
+        [ANY] * 2,
         [
-            ((width, heads), BF16),
-            ((DH, width), BF16),
-            ((DH, width), BF16),
-            ((w_forget.shape[1], width), BF16),
-            ((heads, width), BF16),
-            ((2, 8, LANES), F32),
+            pltpu.VMEM((own, rows), BF16),
+            pltpu.VMEM((1, own), F32),
+            pltpu.SemaphoreType.DMA((2,)),
         ],
-        [ANY] * 7,
-        [
-            pltpu.VMEM((1, own), F32),
-            pltpu.VMEM((1, w_forget.shape[1]), F32),
-            pltpu.SemaphoreType.DMA((7,)),
-        ],
+        flops=10**11,
+    )(in_hbm(tokens.T), in_hbm(first_gain[None]))
+    recv = exchanged(message, "tp").reshape(width, LANES)
+    message, x, gain = kernel(
+        k_project,
+        [((kv, rows // 2 + 1, 4, LANES), BF16), block, ((8, LANES), F32)],
+        [VMEM] * 7,
+        [pltpu.VMEM((rows, LANES), F32)],
     )(
-        in_hbm(w_query),
-        in_hbm(w_key.T),
-        in_hbm(w_value.T),
-        in_hbm(w_forget.T),
-        in_hbm(w_out),
-        in_hbm(first_gain[None]),
-        in_hbm(forget_bias[None]),
-    )
-    message, x = kernel(
-        k_project,
-        [((kv, rows // 2 + 1, 4, LANES), BF16), block],
-        [VMEM] * 6,
-        [pltpu.VMEM((rows, LANES), F32)],
-    )(recv, w_query, w_key, w_value, w_forget, tails)
+        recv,
+        w_query,
+        w_key.T,
+        w_value.T,
+        w_forget.T,
+        w_out,
+        forget_bias[None],
+    )
     recv = exchanged(message, KV)
     positions = kv_cache.shape[1]
     keys, values, gate_sums = kernel(
@@ -505,15 +474,15 @@
         [VMEM] * 4,
         [pltpu.VMEM((4 * rows, LANES), F32), pltpu.VMEM((4 * rows, LANES), F32)],
     )(recv, keys, values, gate_sums)
-    (message,) = kernel(k_combine, [((tp, rows // 4 + 1, 4, width), BF16)], [VMEM] * 4)(
-        exchanged(message, KV), sums, w_out, tails
+    (message,) = kernel(k_combine, [((tp, rows, width), BF16)], [VMEM] * 3)(
+        exchanged(message, KV), sums, w_out
     )
     message, scaled = kernel(
         k_expand,
         [((kv, 8, LANES), BF16), block],
-        [VMEM] * 5,
+        [VMEM] * 6,
         [pltpu.VMEM((8 * kv, LANES), F32)],
-    )(exchanged(message, "tp"), x, tok, w_gate.T, w_up.T)
+    )(exchanged(message, "tp"), x, tok, gain, w_gate.T, w_up.T)
     message, mid = kernel(k_hidden, [((kv, 4, LANES), BF16), block], [VMEM] * 2)(
         exchanged(message, KV), scaled
     )

time: 126 us -> 125 us (level)
  blocking collectives: 77.9 us -> 94.4 us
  starting transfers between devices: 21.4 us -> 12 us
  waiting for transfers between devices: 14.1 us -> 8.35 us
  local copies, waits for them, and re-layouts: 1.95 us -> 0.05 us
    all_to_all x6 -> x7, blocking collectives: 77.9 us -> 94.4 us  [exchanged(): return lax.all_to_all(pieces, axis, 0, 0, tiled=True)]
    all_to_all x2 -> x1, starting transfers between devices: 21.4 us -> 12 us  [exchanged(): return lax.all_to_all(pieces, axis, 0, 0, tiled=True)]
    all_to_all x2 -> x1, waiting for transfers between devices: 14.1 us -> 8.35 us  [exchanged(): return lax.all_to_all(pieces, axis, 0, 0, tiled=True)]
    broadcast_in_dim x1 -> x0, local copies, waits for them, and re-layouts: 1.28 us -> none  [on_device(): message = jnp.broadcast_to(tokens.T[None], (tp, own, rows))]
  transfers between devices with their start and end apart: 2 -> 1, of which waited for: 2 -> 1; matrix products, arithmetic and copies ran while one was open for 0% -> 0% of each run, Pallas kernels for 4% -> 3%
where the time goes in v8:
time: 125 us
  blocking collectives  94.4 us (76%)
  starting transfers between devices  12 us (10%)
  Pallas kernels  9.63 us (8%)
  waiting for transfers between devices  8.35 us (7%)
    all_to_all x7, blocking collectives, exchanged(): return lax.all_to_all(pieces, axis, 0, 0, tiled=True)  94.4 us
    all_to_all x1, starting transfers between devices, exchanged(): return lax.all_to_all(pieces, axis, 0, 0, tiled=True)  12 us
    all_to_all x1, waiting for transfers between devices, exchanged(): return lax.all_to_all(pieces, axis, 0, 0, tiled=True)  8.35 us
    pallas_call x1, Pallas kernels, on_device(): kernel(k_prepare, [((rows // 4, 4 * DH, positions), BF16), ((rows // 4, p...  3.92 us
  transfers between devices with their start and end apart: 1, of which 1 were waited for; matrix products, arithmetic and copies ran while one was open for 0% of the time, Pallas kernels for 3%

profile of v8, /device:TPU:1, one launch (start us, length us, event | category | flops | bytes accessed | tf_op | source)
XLA Modules:
  0.0 124.6 jit_solution(4460410741992997643)
XLA Ops:
  0.0 0.0 copy-start.6
  0.0 0.0 copy-start.7
  0.0 0.0 copy-start.8
  0.0 0.0 copy-start.9
  0.0 0.9 shard_map.145
  0.9 16.7 %all_to_all.40 = bf16[16,8,128]{2,1,0:T(8,128)(2,1)S(1)} all-to-all(bf16[16,8,128]{2,1,0:T(8,128)(2,1)S(1)} %shard_map.145), channel_id=1, replica_groups=mesh['kv_0'=8,'kv_1'=4,'tp'=16] {'tp'}, dimensions={0} | all-to-all | bytes 65536 | tf_op jit(solution)/shard_map/all_to_all | solution.py:43
  17.6 0.0 copy-done
  17.6 0.0 copy-done.4
  17.6 0.0 copy-done.5
  17.6 0.0 copy-done.6
  17.6 0.0 copy-done.7
  17.6 0.0 copy-done.8
  17.6 1.1 shard_map.146
  18.8 12.0 %all-to-all-start.1 = ((bf16[32,9,4,128]{3,2,1,0:T(4,128)(2,1)}), bf16[32,9,4,128]{3,2,1,0:T(4,128)(2,1)S(1)}, u32[]{:S(2)}, u32[]{:S(2)}) async-start(bf16[32,9,4,128]{3,2,1,0:T(4,128)(2,1)} %get-tuple-element.20), calls=%async_computation.1 | async-start | bytes 589824 | tf_op jit(solution)/shard_map/all_to_all | solution.py:43
  30.8 3.9 %shard_map.147 = (bf16[4,256,512]{2,1,0:T(8,128)(2,1)S(1)}, bf16[4,512,256]{2,1,0:T(8,128)(2,1)S(1)}, f32[4,16,512]{2,1,0:T(8,128)S(1)}) custom-call(s32[16]{0:T(128)S(1)} %copy-done.9, bf16[16,512,128]{2,1,0:T(8,128)(2,1)} %cache.1, f32[16,1,512]{2,1,0:T(1,128)} %gate.1), custom_call_target="tpu_custom_call" | custom-call | tf_op jit(solution)/shard_map/pallas_call | solution.py:456
  34.7 0.0 copy-start.1
  34.7 0.0 copy-start.2
  34.7 8.3 %all-to-all-done.1.recv = bf16[32,9,4,128]{3,2,1,0:T(4,128)(2,1)S(1)} async-done(((bf16[32,9,4,128]{3,2,1,0:T(4,128)(2,1)}), bf16[32,9,4,128]{3,2,1,0:T(4,128)(2,1)S(1)}, u32[]{:S(2)}, u32[]{:S(2)}) %all-to-all-start.1) | async-done | bytes 294944 | tf_op jit(solution)/shard_map/all_to_all | solution.py:43
  43.1 1.5 %shard_map.148 = (bf16[32,9,4,128]{3,2,1,0:T(4,128)(2,1)S(1)}, f32[16,128]{1,0:T(8,128)S(1)}, f32[2,128]{1,0:T(2,128)S(1)}) custom-call(bf16[32,9,4,128]{3,2,1,0:T(4,128)(2,1)S(1)} %all-to-all-done.1.recv, bf16[4,256,512]{2,1,0:T(8,128)(2,1)S(1)} %get-tuple-element.21.keys, bf16[4,512,256]{2,1,0:T(8,128)(2,1)S(1)} %get-tuple-element.22.values, ...), custom_call_target="tpu_custom_call" | custom-call | tf_op jit(solution)/shard_map/pallas_call | solution.py:471
  44.6 15.2 %all_to_all.41.recv = bf16[32,9,4,128]{3,2,1,0:T(4,128)(2,1)S(1)} all-to-all(bf16[32,9,4,128]{3,2,1,0:T(4,128)(2,1)S(1)} %get-tuple-element.24), channel_id=1, replica_groups=mesh['kv_0'=8,'kv_1'=4,'tp'=16] {'kv_0','kv_1'}, dimensions={0} | all-to-all | bytes 589824 | tf_op jit(solution)/shard_map/all_to_all | solution.py:43
  59.8 0.6 shard_map.149
  60.4 13.8 %all_to_all.42.recv = bf16[16,16,128]{2,1,0:T(8,128)(2,1)S(1)} all-to-all(bf16[16,16,128]{2,1,0:T(8,128)(2,1)S(1)} %shard_map.149), channel_id=1, replica_groups=mesh['kv_0'=8,'kv_1'=4,'tp'=16] {'tp'}, dimensions={0} | all-to-all | bytes 131072 | tf_op jit(solution)/shard_map/all_to_all | solution.py:43
  74.2 0.0 copy-done.1
  74.2 0.3 shard_map.150
  74.5 12.3 %all_to_all.43.recv = bf16[32,8,128]{2,1,0:T(8,128)(2,1)S(1)} all-to-all(bf16[32,8,128]{2,1,0:T(8,128)(2,1)S(1)} %get-tuple-element.29), channel_id=1, replica_groups=mesh['kv_0'=8,'kv_1'=4,'tp'=16] {'kv_0','kv_1'}, dimensions={0} | all-to-all | bytes 131072 | tf_op jit(solution)/shard_map/all_to_all | solution.py:43
  86.9 0.2 shard_map.151
  87.0 11.8 %all_to_all.44.recv = bf16[32,4,128]{2,1,0:T(4,128)(2,1)S(1)} all-to-all(bf16[32,4,128]{2,1,0:T(4,128)(2,1)S(1)} %get-tuple-element.31), channel_id=1, replica_groups=mesh['kv_0'=8,'kv_1'=4,'tp'=16] {'kv_0','kv_1'}, dimensions={0} | all-to-all | bytes 65536 | tf_op jit(solution)/shard_map/all_to_all | solution.py:43
  98.8 0.2 shard_map.152
  99.0 13.0 %all_to_all.45.recv = bf16[16,16,128]{2,1,0:T(8,128)(2,1)S(1)} all-to-all(bf16[16,16,128]{2,1,0:T(8,128)(2,1)S(1)} %shard_map.152), channel_id=1, replica_groups=mesh['kv_0'=8,'kv_1'=4,'tp'=16] {'tp'}, dimensions={0} | all-to-all | bytes 131072 | tf_op jit(solution)/shard_map/all_to_all | solution.py:43
  111.9 0.2 shard_map.153
  112.1 11.6 %all_to_all.46.recv = f32[32,1,128]{2,1,0:T(1,128)S(1)} all-to-all(f32[32,1,128]{2,1,0:T(1,128)S(1)} %get-tuple-element.33), channel_id=1, replica_groups=mesh['kv_0'=8,'kv_1'=4,'tp'=16] {'kv_0','kv_1'}, dimensions={0} | all-to-all | bytes 32768 | tf_op jit(solution)/shard_map/all_to_all | solution.py:43
  123.7 0.8 shard_map.154
  (9 shorter events, 0.0 us)
Async XLA Ops:
  0.0 17.6 %copy-start = (bf16[256,128]{1,0:T(8,128)(2,1)S(1)}, bf16[256,128]{1,0:T(8,128)(2,1)}, u32[]{:S(2)}) copy-start(bf16[256,128]{1,0:T(8,128)(2,1)} %w_out.3) | copy-start | bytes 196612
  0.0 17.6 %copy-start.4 = (bf16[4096,16]{0,1:T(8,128)(2,1)S(1)}, bf16[4096,16]{0,1:T(8,128)(2,1)}, u32[]{:S(2)}) copy-start(bf16[4096,16]{0,1:T(8,128)(2,1)} %param.22) | copy-start | bytes 393220
  0.0 17.6 %copy-start.5 = (bf16[128,256]{1,0:T(8,128)(2,1)S(1)}, bf16[128,256]{1,0:T(8,128)(2,1)}, u32[]{:S(2)}) copy-start(bf16[128,256]{1,0:T(8,128)(2,1)} %w_query.1) | copy-start | bytes 196612
  0.0 17.6 %copy-start.6 = (bf16[128,64]{0,1:T(8,128)(2,1)S(1)}, bf16[128,64]{0,1:T(8,128)(2,1)}, u32[]{:S(2)}) copy-start(bf16[128,64]{0,1:T(8,128)(2,1)} %param.20) | copy-start | bytes 49156
  0.0 17.6 %copy-start.7 = (bf16[128,64]{0,1:T(8,128)(2,1)S(1)}, bf16[128,64]{0,1:T(8,128)(2,1)}, u32[]{:S(2)}) copy-start(bf16[128,64]{0,1:T(8,128)(2,1)} %param.21) | copy-start | bytes 49156
  0.0 17.6 %copy-start.8 = (f32[16]{0:T(128)S(1)}, f32[16]{0:T(128)}, u32[]{:S(2)}) copy-start(f32[16]{0:T(128)} %param.23) | copy-start | bytes 196
  0.0 30.7 %copy-start.9 = (s32[16]{0:T(128)S(1)}, s32[16]{0:T(128)}, u32[]{:S(2)}) copy-start(s32[16]{0:T(128)} %lengths.1) | copy-start | bytes 196
  18.8 24.3 %all-to-all-start.1 = ((bf16[32,9,4,128]{3,2,1,0:T(4,128)(2,1)}), bf16[32,9,4,128]{3,2,1,0:T(4,128)(2,1)S(1)}, u32[]{:S(2)}, u32[]{:S(2)}) async-start(bf16[32,9,4,128]{3,2,1,0:T(4,128)(2,1)} %get-tuple-element.20), calls=%async_computation.1 | async-start | bytes 589824 | tf_op jit(solution)/shard_map/all_to_all | solution.py:43
  34.7 39.5 %copy-start.1 = (bf16[128,704]{0,1:T(8,128)(2,1)S(1)}, bf16[128,704]{0,1:T(8,128)(2,1)}, u32[]{:S(2)}) copy-start(bf16[128,704]{0,1:T(8,128)(2,1)} %param.26) | copy-start | bytes 540676
  34.7 39.5 %copy-start.2 = (bf16[128,704]{0,1:T(8,128)(2,1)S(1)}, bf16[128,704]{0,1:T(8,128)(2,1)}, u32[]{:S(2)}) copy-start(bf16[128,704]{0,1:T(8,128)(2,1)} %param.27) | copy-start | bytes 540676
  43.1 55.7 %copy-start.3 = (bf16[704,128]{1,0:T(8,128)(2,1)S(1)}, bf16[704,128]{1,0:T(8,128)(2,1)}, u32[]{:S(2)}) copy-start(bf16[704,128]{1,0:T(8,128)(2,1)} %w_down.1) | copy-start | bytes 540676
  43.1 80.6 %copy-start.10 = (f32[8]{0:T(128)S(1)}, f32[8]{0:T(128)}, u32[]{:S(2)}) copy-start(f32[8]{0:T(128)} %param.29) | copy-start | bytes 100

commit v9 on v8

--- a/solution.py
+++ b/solution.py
@@ -77,9 +77,11 @@
 
 
 def as_row(columns):
-    rows = columns[0].shape[0]
+    rows = columns[-1].shape[0]
     tile = jnp.zeros((rows, LANES), F32)
     for turn, column in enumerate(columns):
+        if column is None:
+            continue
         tile = jnp.where(diagonal(rows, turn), column, tile)
     return jnp.sum(tile, axis=0, keepdims=True)
 
@@ -126,20 +128,30 @@
         copy.wait()
     own, rows = turned.shape
     column = jnp.sum(jnp.where(diagonal(own, 0)[:, :own], gain[...], 0.0), axis=1, keepdims=True)
-    pad = jnp.zeros((own, LANES - rows), F32)
-    tile = jnp.concatenate([turned[...].astype(F32), pad], axis=1)
-    for k, piece in enumerate(in_pieces(column, 3)):
-        tile = jnp.where(iota(tile.shape, 1) == rows + k, piece, tile)
-    tile = tile.astype(BF16)
+    tile = turned[...].astype(F32)
+    pieces = [jnp.broadcast_to(piece, (own, rows)) for piece in in_pieces(column, 3)]
+    lane = iota((own, rows), 1)
+    extra = jnp.where(lane == 0, pieces[0], jnp.where(lane == 1, pieces[1], pieces[2]))
+    half = own // 2
+    pad = jnp.zeros((half, LANES - 4 * rows), F32)
+    sides = [tile[:half], extra[:half], tile[half:], extra[half:], pad]
+    tile = jnp.concatenate(sides, axis=1).astype(BF16)
     for k in range(out.shape[0]):
         out[k] = tile
 
 
 def k_project(recv, w_query, w_key, w_value, w_forget, w_out, bias, out, x_out, gain_out, new_rows):
-    width = recv.shape[0]
-    same = jnp.where(iota((width, width), 0) == iota((width, width), 1), 1.0, 0.0).astype(BF16)
+    width = x_out.shape[1]
     rows = new_rows.shape[0]
-    both = across(recv[:, : 2 * rows], same, FIRST)
+    sent = recv.shape[0]
+    source = iota((sent, width), 0)
+    target = 2 * source - source % 4
+    place = iota((sent, width), 1)
+    both = jnp.zeros((2 * rows, width), F32)
+    for side in range(2):
+        spread = jnp.where(place == target + 4 * side, 1.0, 0.0).astype(BF16)
+        part = recv[:, 2 * rows * side : 2 * rows * (side + 1)]
+        both = both + across(part, spread, FIRST)
     x = both[:rows]
     x_out[...] = x
     gain = both[rows : rows + 1] + both[rows + 1 : rows + 2] + both[rows + 2 : rows + 3]
@@ -315,39 +327,41 @@
     centred = x[...] - tok[:, 0:1] / D + summed(recv, 0, rows)
     scaled = centred * gain[0:1, :]
     scaled_out[...] = scaled
-    squares = as_row(in_pieces(jnp.sum(centred * centred, axis=1, keepdims=True), 2))
+    squares = in_pieces(jnp.sum(centred * centred, axis=1, keepdims=True), 2)
+    squares = as_row([None] * 6 + squares)
     scaled = scaled.astype(BF16)
-    pieces = tile.shape[0] // (8 * rows)
-    tiles = 3 * pieces
-    columns = w_gate.shape[0]
+    pieces = out.shape[0] // rows
+    size = w_gate.shape[0] // pieces
+    stride = 6 * pieces
+    pad = jnp.zeros((rows, 3 * LANES - size), F32)
     for k, weight in enumerate((w_gate, w_up)):
         part = across(scaled, weight[...], LAST)
-        pad = jnp.zeros((rows, tiles * LANES - columns), F32)
-        part = jnp.concatenate([part, pad], axis=1)
-        for t in range(tiles):
-            at = 8 * (t // 3) + 3 * k + t % 3
-            tile[pl.ds(at, rows, stride=8 * pieces), :] = part[:, t * LANES : (t + 1) * LANES]
-    for h in range(pieces):
-        tile[pl.ds(8 * h + 6, rows, stride=8 * pieces), :] = jnp.broadcast_to(
-            squares, (rows, LANES)
-        )
-        tile[pl.ds(8 * h + 7, rows, stride=8 * pieces), :] = jnp.zeros((rows, LANES), F32)
-    for k in range(out.shape[0]):
-        out[k] = tile[pl.ds(8 * k, 8), :].astype(BF16)
+        for h in range(pieces):
+            share = jnp.concatenate([part[:, h * size : (h + 1) * size], pad], axis=1)
+            for t in range(3):
+                block = share[:, t * LANES : (t + 1) * LANES]
+                if t == 2 and k == 0:
+                    block = block + squares
+                tile[pl.ds(6 * h + 3 * k + t, rows, stride=stride), :] = block
+    for k in range(out.shape[0]):
+        for t in range(3):
+            out[k, t] = tile[pl.ds(6 * k + 2 * t, 2), :].astype(BF16)
 
 
 def k_hidden(recv, scaled, out, mid_out):
     rows = scaled.shape[0]
-    total = summed(recv, 0, 8)
-    spread = as_column(total[6:7], rows, (0, 1)) / D
+    total = jnp.concatenate(
+        [jnp.sum(recv[:, t].astype(F32), axis=0) for t in range(recv.shape[1])], axis=0
+    )
+    spread = as_column(total[2:3], rows, (6, 7)) / D
     shrink = lax.rsqrt(spread + EPSILON)
     mid_out[...] = rounded(scaled[...] * shrink)
     mine = iota((rows, 1), 0) == kv_index() // (out.shape[0] // rows)
     own = jnp.sum(jnp.where(mine, shrink, 0.0), axis=0, keepdims=True)
     total = total * own
-    up = pltpu.roll(total, 5, 0)
-    hidden = total / (1.0 + jnp.exp(-total)) * up
-    hidden = jnp.where(iota((8, LANES), 0) < 3, hidden, 0.0)[:4].astype(BF16)
+    gate, up = total[:3], total[3:6]
+    hidden = gate / (1.0 + jnp.exp(-gate)) * up
+    hidden = jnp.concatenate([hidden, jnp.zeros((1, LANES), F32)], axis=0).astype(BF16)
     for k in range(out.shape[0]):
         out[k] = hidden
 
@@ -358,14 +372,13 @@
     for k in range(recv.shape[0]):
         tile[pl.ds(4 * k, 4), :] = recv[k].astype(F32)
     part = jnp.zeros((rows, LANES), F32)
-    columns = w_down.shape[0]
+    share = w_down.shape[0] // pieces
     for t in range(3 * pieces):
         at = 4 * (t // 3) + t % 3
-        size = min(LANES, columns - t * LANES)
+        start = share * (t // 3) + LANES * (t % 3)
+        size = min(LANES, share - LANES * (t % 3))
         hidden = tile[pl.ds(at, rows, stride=4 * pieces), :][:, :size].astype(BF16)
-        part = part + jnp.dot(
-            hidden, w_down[pl.ds(t * LANES, size), :], preferred_element_type=F32
-        )
+        part = part + jnp.dot(hidden, w_down[pl.ds(start, size), :], preferred_element_type=F32)
     part = part.astype(BF16)
     for k in range(out.shape[0]):
         out[k] = part
@@ -427,7 +440,7 @@
     in_hbm = functools.partial(pltpu.with_memory_space_constraint, memory_space=pltpu.HBM)
     (message,) = kernel(
         k_start,
-        [((tp, own, LANES), BF16)],
+        [((tp, own // 2, LANES), BF16)],
         [ANY] * 2,
         [
             pltpu.VMEM((own, rows), BF16),
@@ -436,7 +449,7 @@
         ],
         flops=10**11,
     )(in_hbm(tokens.T), in_hbm(first_gain[None]))
-    recv = exchanged(message, "tp").reshape(width, LANES)
+    recv = exchanged(message, "tp").reshape(width // 2, LANES)
     message, x, gain = kernel(
         k_project,
         [((kv, rows // 2 + 1, 4, LANES), BF16), block, ((8, LANES), F32)],
@@ -479,9 +492,9 @@
     )
     message, scaled = kernel(
         k_expand,
-        [((kv, 8, LANES), BF16), block],
+        [((kv, 3, 2, LANES), BF16), block],
         [VMEM] * 6,
-        [pltpu.VMEM((8 * kv, LANES), F32)],
+        [pltpu.VMEM((6 * kv, LANES), F32)],
     )(exchanged(message, "tp"), x, tok, gain, w_gate.T, w_up.T)
     message, mid = kernel(k_hidden, [((kv, 4, LANES), BF16), block], [VMEM] * 2)(
         exchanged(message, KV), scaled

time: 125 us -> 125 us (level)
  no operation moved by 1% of the time
where the time goes in v9:
time: 125 us
  blocking collectives  94.1 us (75%)
  starting transfers between devices  12.1 us (10%)
  Pallas kernels  9.88 us (8%)
  waiting for transfers between devices  8.35 us (7%)
    all_to_all x7, blocking collectives, exchanged(): return lax.all_to_all(pieces, axis, 0, 0, tiled=True)  94.1 us
    all_to_all x1, starting transfers between devices, exchanged(): return lax.all_to_all(pieces, axis, 0, 0, tiled=True)  12.1 us
    all_to_all x1, waiting for transfers between devices, exchanged(): return lax.all_to_all(pieces, axis, 0, 0, tiled=True)  8.35 us
    pallas_call x1, Pallas kernels, on_device(): kernel(k_prepare, [((rows // 4, 4 * DH, positions), BF16), ((rows // 4, p...  3.92 us
  transfers between devices with their start and end apart: 1, of which 1 were waited for; matrix products, arithmetic and copies ran while one was open for 0% of the time, Pallas kernels for 3%

profile of v9, /device:TPU:1, one launch (start us, length us, event | category | flops | bytes accessed | tf_op | source)
XLA Modules:
  0.0 124.6 jit_solution(2445839221480880117)
XLA Ops:
  0.0 0.0 copy-start.6
  0.0 0.0 copy-start.7
  0.0 0.0 copy-start.8
  0.0 0.0 copy-start.9
  0.0 0.9 shard_map.145
  1.0 16.6 %all_to_all.40 = bf16[16,4,128]{2,1,0:T(4,128)(2,1)S(1)} all-to-all(bf16[16,4,128]{2,1,0:T(4,128)(2,1)S(1)} %shard_map.145), channel_id=1, replica_groups=mesh['kv_0'=8,'kv_1'=4,'tp'=16] {'tp'}, dimensions={0} | all-to-all | bytes 32768 | tf_op jit(solution)/shard_map/all_to_all | solution.py:43
  17.6 0.0 copy-done
  17.6 0.0 copy-done.4
  17.6 0.0 copy-done.5
  17.6 0.0 copy-done.6
  17.6 0.0 copy-done.7
  17.6 0.0 copy-done.8
  17.6 1.2 shard_map.146
  18.8 12.1 %all-to-all-start.1 = ((bf16[32,9,4,128]{3,2,1,0:T(4,128)(2,1)}), bf16[32,9,4,128]{3,2,1,0:T(4,128)(2,1)S(1)}, u32[]{:S(2)}, u32[]{:S(2)}) async-start(bf16[32,9,4,128]{3,2,1,0:T(4,128)(2,1)} %get-tuple-element.20), calls=%async_computation.1 | async-start | bytes 589824 | tf_op jit(solution)/shard_map/all_to_all | solution.py:43
  30.9 3.9 %shard_map.147 = (bf16[4,256,512]{2,1,0:T(8,128)(2,1)S(1)}, bf16[4,512,256]{2,1,0:T(8,128)(2,1)S(1)}, f32[4,16,512]{2,1,0:T(8,128)S(1)}) custom-call(s32[16]{0:T(128)S(1)} %copy-done.9, bf16[16,512,128]{2,1,0:T(8,128)(2,1)} %cache.1, f32[16,1,512]{2,1,0:T(1,128)} %gate.1), custom_call_target="tpu_custom_call" | custom-call | tf_op jit(solution)/shard_map/pallas_call | solution.py:469
  34.8 0.0 copy-start.1
  34.8 0.0 copy-start.2
  34.8 8.3 %all-to-all-done.1.recv = bf16[32,9,4,128]{3,2,1,0:T(4,128)(2,1)S(1)} async-done(((bf16[32,9,4,128]{3,2,1,0:T(4,128)(2,1)}), bf16[32,9,4,128]{3,2,1,0:T(4,128)(2,1)S(1)}, u32[]{:S(2)}, u32[]{:S(2)}) %all-to-all-start.1) | async-done | bytes 294944 | tf_op jit(solution)/shard_map/all_to_all | solution.py:43
  43.2 1.5 %shard_map.148 = (bf16[32,9,4,128]{3,2,1,0:T(4,128)(2,1)S(1)}, f32[16,128]{1,0:T(8,128)S(1)}, f32[2,128]{1,0:T(2,128)S(1)}) custom-call(bf16[32,9,4,128]{3,2,1,0:T(4,128)(2,1)S(1)} %all-to-all-done.1.recv, bf16[4,256,512]{2,1,0:T(8,128)(2,1)S(1)} %get-tuple-element.21.keys, bf16[4,512,256]{2,1,0:T(8,128)(2,1)S(1)} %get-tuple-element.22.values, ...), custom_call_target="tpu_custom_call" | custom-call | tf_op jit(solution)/shard_map/pallas_call | solution.py:484
  44.7 15.2 %all_to_all.41.recv = bf16[32,9,4,128]{3,2,1,0:T(4,128)(2,1)S(1)} all-to-all(bf16[32,9,4,128]{3,2,1,0:T(4,128)(2,1)S(1)} %get-tuple-element.24), channel_id=1, replica_groups=mesh['kv_0'=8,'kv_1'=4,'tp'=16] {'kv_0','kv_1'}, dimensions={0} | all-to-all | bytes 589824 | tf_op jit(solution)/shard_map/all_to_all | solution.py:43
  59.9 0.6 shard_map.149
  60.5 13.8 %all_to_all.42.recv = bf16[16,16,128]{2,1,0:T(8,128)(2,1)S(1)} all-to-all(bf16[16,16,128]{2,1,0:T(8,128)(2,1)S(1)} %shard_map.149), channel_id=1, replica_groups=mesh['kv_0'=8,'kv_1'=4,'tp'=16] {'tp'}, dimensions={0} | all-to-all | bytes 131072 | tf_op jit(solution)/shard_map/all_to_all | solution.py:43
  74.3 0.4 shard_map.150
  74.7 12.3 %all_to_all.43.recv = bf16[32,3,2,128]{3,2,1,0:T(2,128)(2,1)S(1)} all-to-all(bf16[32,3,2,128]{3,2,1,0:T(2,128)(2,1)S(1)} %get-tuple-element.29), channel_id=1, replica_groups=mesh['kv_0'=8,'kv_1'=4,'tp'=16] {'kv_0','kv_1'}, dimensions={0} | all-to-all | bytes 98304 | tf_op jit(solution)/shard_map/all_to_all | solution.py:43
  87.0 0.2 shard_map.151
  87.2 11.7 %all_to_all.44.recv = bf16[32,4,128]{2,1,0:T(4,128)(2,1)S(1)} all-to-all(bf16[32,4,128]{2,1,0:T(4,128)(2,1)S(1)} %get-tuple-element.31), channel_id=1, replica_groups=mesh['kv_0'=8,'kv_1'=4,'tp'=16] {'kv_0','kv_1'}, dimensions={0} | all-to-all | bytes 65536 | tf_op jit(solution)/shard_map/all_to_all | solution.py:43
  98.8 0.0 copy-done.3
  98.8 0.2 shard_map.152
  99.0 12.9 %all_to_all.45.recv = bf16[16,16,128]{2,1,0:T(8,128)(2,1)S(1)} all-to-all(bf16[16,16,128]{2,1,0:T(8,128)(2,1)S(1)} %shard_map.152), channel_id=1, replica_groups=mesh['kv_0'=8,'kv_1'=4,'tp'=16] {'tp'}, dimensions={0} | all-to-all | bytes 131072 | tf_op jit(solution)/shard_map/all_to_all | solution.py:43
  111.9 0.2 shard_map.153
  112.1 11.6 %all_to_all.46.recv = f32[32,1,128]{2,1,0:T(1,128)S(1)} all-to-all(f32[32,1,128]{2,1,0:T(1,128)S(1)} %get-tuple-element.33), channel_id=1, replica_groups=mesh['kv_0'=8,'kv_1'=4,'tp'=16] {'kv_0','kv_1'}, dimensions={0} | all-to-all | bytes 32768 | tf_op jit(solution)/shard_map/all_to_all | solution.py:43
  123.7 0.8 shard_map.154
  (9 shorter events, 0.0 us)
Async XLA Ops:
  0.0 17.6 %copy-start = (bf16[256,128]{1,0:T(8,128)(2,1)S(1)}, bf16[256,128]{1,0:T(8,128)(2,1)}, u32[]{:S(2)}) copy-start(bf16[256,128]{1,0:T(8,128)(2,1)} %w_out.3) | copy-start | bytes 196612
  0.0 17.6 %copy-start.4 = (bf16[4096,16]{0,1:T(8,128)(2,1)S(1)}, bf16[4096,16]{0,1:T(8,128)(2,1)}, u32[]{:S(2)}) copy-start(bf16[4096,16]{0,1:T(8,128)(2,1)} %param.22) | copy-start | bytes 393220
  0.0 17.6 %copy-start.5 = (bf16[128,256]{1,0:T(8,128)(2,1)S(1)}, bf16[128,256]{1,0:T(8,128)(2,1)}, u32[]{:S(2)}) copy-start(bf16[128,256]{1,0:T(8,128)(2,1)} %w_query.1) | copy-start | bytes 196612
  0.0 17.6 %copy-start.6 = (bf16[128,64]{0,1:T(8,128)(2,1)S(1)}, bf16[128,64]{0,1:T(8,128)(2,1)}, u32[]{:S(2)}) copy-start(bf16[128,64]{0,1:T(8,128)(2,1)} %param.20) | copy-start | bytes 49156
  0.0 17.6 %copy-start.7 = (bf16[128,64]{0,1:T(8,128)(2,1)S(1)}, bf16[128,64]{0,1:T(8,128)(2,1)}, u32[]{:S(2)}) copy-start(bf16[128,64]{0,1:T(8,128)(2,1)} %param.21) | copy-start | bytes 49156
  0.0 17.6 %copy-start.8 = (f32[16]{0:T(128)S(1)}, f32[16]{0:T(128)}, u32[]{:S(2)}) copy-start(f32[16]{0:T(128)} %param.23) | copy-start | bytes 196
  0.0 30.8 %copy-start.9 = (s32[16]{0:T(128)S(1)}, s32[16]{0:T(128)}, u32[]{:S(2)}) copy-start(s32[16]{0:T(128)} %lengths.1) | copy-start | bytes 196
  18.8 24.4 %all-to-all-start.1 = ((bf16[32,9,4,128]{3,2,1,0:T(4,128)(2,1)}), bf16[32,9,4,128]{3,2,1,0:T(4,128)(2,1)S(1)}, u32[]{:S(2)}, u32[]{:S(2)}) async-start(bf16[32,9,4,128]{3,2,1,0:T(4,128)(2,1)} %get-tuple-element.20), calls=%async_computation.1 | async-start | bytes 589824 | tf_op jit(solution)/shard_map/all_to_all | solution.py:43
  34.8 39.5 %copy-start.1 = (bf16[128,704]{0,1:T(8,128)(2,1)S(1)}, bf16[128,704]{0,1:T(8,128)(2,1)}, u32[]{:S(2)}) copy-start(bf16[128,704]{0,1:T(8,128)(2,1)} %param.26) | copy-start | bytes 540676
  34.8 39.5 %copy-start.2 = (bf16[128,704]{0,1:T(8,128)(2,1)S(1)}, bf16[128,704]{0,1:T(8,128)(2,1)}, u32[]{:S(2)}) copy-start(bf16[128,704]{0,1:T(8,128)(2,1)} %param.27) | copy-start | bytes 540676
  43.2 55.6 %copy-start.3 = (bf16[704,128]{1,0:T(8,128)(2,1)S(1)}, bf16[704,128]{1,0:T(8,128)(2,1)}, u32[]{:S(2)}) copy-start(bf16[704,128]{1,0:T(8,128)(2,1)} %w_down.1) | copy-start | bytes 540676
  43.2 80.5 %copy-start.10 = (f32[8]{0:T(128)S(1)}, f32[8]{0:T(128)}, u32[]{:S(2)}) copy-start(f32[8]{0:T(128)} %param.29) | copy-start | bytes 100

commit v10 on v8

--- a/solution.py
+++ b/solution.py
@@ -8,11 +8,13 @@
 from jax.sharding import Mesh
 from jax.sharding import PartitionSpec as P
 
+
 D = 4096
 DH = 64
 LANES = 128
-KV = ("kv_0", "kv_1")
-KV_TP = ("kv_0", "kv_1", "tp")
+SPARE = 96
+KV = ("kv_0", "kv_1", "kv_2")
+KV_TP = ("kv_0", "kv_1", "kv_2", "tp")
 EPSILON = 1e-05
 EMPTY_SCORE = -1e30
 F32 = jnp.float32
@@ -44,7 +46,10 @@
 
 
 def kv_index():
-    return lax.axis_index("kv_0") * lax.axis_size("kv_1") + lax.axis_index("kv_1")
+    index = lax.axis_index(KV[0])
+    for axis in KV[1:]:
+        index = index * lax.axis_size(axis) + lax.axis_index(axis)
+    return index
 
 
 def iota(shape, dim):
@@ -193,7 +198,7 @@
             )
 
 
-def k_attend(recv, keys, values, gate, out, tok_out, sums_out, qs, os):
+def k_attend(recv, keys, values, gate, arrived, out, tok_out, sums_out, qs, os):
     rows = 4 * keys.shape[0]
     heads = 4
     scale = DH**-0.5
@@ -273,7 +278,6 @@
 def k_combine(recv, sums, w_out, out):
     devices = recv.shape[0]
     tiles = (recv.shape[1] - 1) // 2
-    rows = 4 * tiles
     heads = 4 * DH
     source = iota((LANES, 2 * heads), 0) % 32
     column = iota((LANES, 2 * heads), 1)
@@ -310,65 +314,65 @@
         out[k] = attn_part
 
 
-def k_expand(recv, x, tok, gain, w_gate, w_up, out, scaled_out, tile):
+def k_expand(recv, x, tok, gain, w_gate, w_up, out, scaled_out):
     rows = x.shape[0]
     centred = x[...] - tok[:, 0:1] / D + summed(recv, 0, rows)
     scaled = centred * gain[0:1, :]
     scaled_out[...] = scaled
-    squares = as_row(in_pieces(jnp.sum(centred * centred, axis=1, keepdims=True), 2))
+    squares = in_pieces(jnp.sum(centred * centred, axis=1, keepdims=True), 2)
     scaled = scaled.astype(BF16)
-    pieces = tile.shape[0] // (8 * rows)
-    tiles = 3 * pieces
-    columns = w_gate.shape[0]
+    parts = out.shape[0]
+    size = w_gate.shape[0] // parts
+    pad = jnp.zeros((rows, 3 * LANES - size), F32)
+    lane = iota((rows, LANES), 1)
     for k, weight in enumerate((w_gate, w_up)):
         part = across(scaled, weight[...], LAST)
-        pad = jnp.zeros((rows, tiles * LANES - columns), F32)
-        part = jnp.concatenate([part, pad], axis=1)
-        for t in range(tiles):
-            at = 8 * (t // 3) + 3 * k + t % 3
-            tile[pl.ds(at, rows, stride=8 * pieces), :] = part[:, t * LANES : (t + 1) * LANES]
-    for h in range(pieces):
-        tile[pl.ds(8 * h + 6, rows, stride=8 * pieces), :] = jnp.broadcast_to(
-            squares, (rows, LANES)
-        )
-        tile[pl.ds(8 * h + 7, rows, stride=8 * pieces), :] = jnp.zeros((rows, LANES), F32)
-    for k in range(out.shape[0]):
-        out[k] = tile[pl.ds(8 * k, 8), :].astype(BF16)
-
-
-def k_hidden(recv, scaled, out, mid_out):
+        for h in range(parts):
+            share = jnp.concatenate([part[:, h * size : (h + 1) * size], pad], axis=1)
+            for t in range(3):
+                block = share[:, t * LANES : (t + 1) * LANES]
+                if t == 2 and k == 0:
+                    for n, piece in enumerate(squares):
+                        block = jnp.where(lane == SPARE + n, piece, block)
+                out[h, pl.ds((3 * k + t) * rows, rows)] = block.astype(BF16)
+
+
+def k_gather(recv, out):
+    rows = recv.shape[1] // 6
+    lane = iota((rows, LANES), 1)
+    for t in range(6):
+        block = summed(recv, t * rows, rows)
+        if t == 2:
+            square = block[:, SPARE : SPARE + 1] + block[:, SPARE + 1 : SPARE + 2]
+            for n, piece in enumerate(in_pieces(square, 2)):
+                block = jnp.where(lane == SPARE + n, piece, block)
+        block = block.astype(BF16)
+        for k in range(out.shape[0]):
+            out[k, pl.ds(t * rows, rows)] = block
+
+
+def k_hidden(recv, scaled, w_own, w_other, out, mid_out):
     rows = scaled.shape[0]
-    total = summed(recv, 0, 8)
-    spread = as_column(total[6:7], rows, (0, 1)) / D
+    blocks = [summed(recv, t * rows, rows) for t in range(6)]
+    spread = (blocks[2][:, SPARE : SPARE + 1] + blocks[2][:, SPARE + 1 : SPARE + 2]) / D
     shrink = lax.rsqrt(spread + EPSILON)
     mid_out[...] = rounded(scaled[...] * shrink)
-    mine = iota((rows, 1), 0) == kv_index() // (out.shape[0] // rows)
-    own = jnp.sum(jnp.where(mine, shrink, 0.0), axis=0, keepdims=True)
-    total = total * own
-    up = pltpu.roll(total, 5, 0)
-    hidden = total / (1.0 + jnp.exp(-total)) * up
-    hidden = jnp.where(iota((8, LANES), 0) < 3, hidden, 0.0)[:4].astype(BF16)
-    for k in range(out.shape[0]):
-        out[k] = hidden
-
-
-def k_shrink(recv, w_down, out, tile):
-    rows = out.shape[1]
-    pieces = recv.shape[0] // rows
-    for k in range(recv.shape[0]):
-        tile[pl.ds(4 * k, 4), :] = recv[k].astype(F32)
-    part = jnp.zeros((rows, LANES), F32)
-    columns = w_down.shape[0]
-    for t in range(3 * pieces):
-        at = 4 * (t // 3) + t % 3
-        size = min(LANES, columns - t * LANES)
-        hidden = tile[pl.ds(at, rows, stride=4 * pieces), :][:, :size].astype(BF16)
-        part = part + jnp.dot(
-            hidden, w_down[pl.ds(t * LANES, size), :], preferred_element_type=F32
-        )
-    part = part.astype(BF16)
-    for k in range(out.shape[0]):
-        out[k] = part
+    side = lax.axis_index("kv_2")
+    size = w_own.shape[0] // 2
+    copies = out.shape[0] // 2
+    parts = [jnp.zeros((rows, LANES), F32)] * 2
+    for t in range(3):
+        gate = blocks[t] * shrink
+        up = blocks[3 + t] * shrink
+        width = min(LANES, size - t * LANES)
+        hidden = (gate / (1.0 + jnp.exp(-gate)) * up)[:, :width].astype(BF16)
+        at = pl.ds(pl.multiple_of(side * size + t * LANES, 16), width)
+        for n, weight in enumerate((w_own, w_other)):
+            parts[n] = parts[n] + jnp.dot(hidden, weight[at, :], preferred_element_type=F32)
+    for n, start in enumerate((side * copies, (1 - side) * copies)):
+        part = parts[n].astype(BF16)
+        for k in range(copies):
+            out[start + k] = part
 
 
 def k_sums(recv, mid, out, mix_out):
@@ -452,8 +456,9 @@
         forget_bias[None],
     )
     recv = exchanged(message, KV)
+    w_other = lax.ppermute(w_down, "kv_2", [(0, 1), (1, 0)])
     positions = kv_cache.shape[1]
-    keys, values, gate_sums = kernel(
+    prepare = kernel(
         k_prepare,
         [
             ((rows // 4, 4 * DH, positions), BF16),
@@ -467,30 +472,30 @@
             pltpu.SemaphoreType.DMA((rows,)),
             pltpu.SemaphoreType.DMA,
         ],
-    )(live_lengths, in_hbm(kv_cache), in_hbm(gate_sums))
-    message, tok, sums = kernel(
+    )
+    keys, values, gate_sums = prepare(live_lengths, in_hbm(kv_cache), in_hbm(gate_sums))
+    attend = kernel(
         k_attend,
         [((kv, rows // 2 + 1, 4, LANES), BF16), block, ((2, LANES), F32)],
-        [VMEM] * 4,
+        [VMEM] * 5,
         [pltpu.VMEM((4 * rows, LANES), F32), pltpu.VMEM((4 * rows, LANES), F32)],
-    )(recv, keys, values, gate_sums)
+    )
+    message, tok, sums = attend(recv, keys, values, gate_sums, w_other)
     (message,) = kernel(k_combine, [((tp, rows, width), BF16)], [VMEM] * 3)(
         exchanged(message, KV), sums, w_out
     )
+    pair = lax.axis_size("kv_2")
     message, scaled = kernel(
-        k_expand,
-        [((kv, 8, LANES), BF16), block],
-        [VMEM] * 6,
-        [pltpu.VMEM((8 * kv, LANES), F32)],
+        k_expand, [((pair, 6 * rows, LANES), BF16), block], [VMEM] * 6
     )(exchanged(message, "tp"), x, tok, gain, w_gate.T, w_up.T)
-    message, mid = kernel(k_hidden, [((kv, 4, LANES), BF16), block], [VMEM] * 2)(
-        exchanged(message, KV), scaled
-    )
-    (message,) = kernel(
-        k_shrink, [((tp, rows, width), BF16)], [VMEM] * 2, [pltpu.VMEM((4 * kv, LANES), F32)]
-    )(exchanged(message, KV), w_down)
+    (message,) = kernel(k_gather, [((kv // pair, 6 * rows, LANES), BF16)], [VMEM])(
+        exchanged(message, "kv_2")
+    )
+    message, mid = kernel(
+        k_hidden, [((pair * tp, rows, width), BF16), block], [VMEM] * 4
+    )(exchanged(message, ("kv_0", "kv_1")), scaled, w_down, w_other)
     message, mix = kernel(k_sums, [((kv, 1, LANES), F32), block], [VMEM] * 2)(
-        exchanged(message, "tp"), mid
+        exchanged(message, ("kv_2", "tp")), mid
     )
     (out,) = kernel(
         k_finish, [((own, rows), BF16)], [VMEM] * 3, [pltpu.VMEM((width, rows), F32)], last=True
@@ -499,7 +504,7 @@
 
 
 def solution(mesh):
-    split = Mesh(mesh.devices.reshape(8, 4, mesh.shape["tp"]), ("kv_0", "kv_1", "tp"))
+    split = Mesh(mesh.devices.reshape(8, 2, 2, mesh.shape["tp"]), KV_TP)
     placed = (
         P(None, KV_TP),
         P(),
@@ -517,6 +522,7 @@
         P("tp", KV),
         P(KV_TP),
     )
+
     return jax.shard_map(
         on_device, mesh=split, in_specs=placed, out_specs=P(None, KV_TP), check_vma=False
     )

time: 125 us -> 127 us (1.016)
  starting transfers between devices: 12 us -> 15.2 us
  waiting for transfers between devices: 8.35 us -> 5.19 us
  blocking collectives: 94.4 us -> 95.9 us
    all_to_all x1, waiting for transfers between devices: 8.35 us -> 2.42 us  [exchanged(): return lax.all_to_all(pieces, axis, 0, 0, tiled=True)]
    ppermute x0 -> x1, starting transfers between devices: none -> 3.14 us  [on_device(): w_other = lax.ppermute(w_down, 'kv_2', [(0, 1), (1, 0)])]
    ppermute x0 -> x1, waiting for transfers between devices: none -> 2.77 us  [on_device(): w_other = lax.ppermute(w_down, 'kv_2', [(0, 1), (1, 0)])]
    all_to_all x7, blocking collectives: 94.4 us -> 95.9 us  [exchanged(): return lax.all_to_all(pieces, axis, 0, 0, tiled=True)]
  transfers between devices with their start and end apart: 1 -> 2, of which waited for: 1 -> 2; matrix products, arithmetic and copies ran while one was open for 0% -> 0% of each run, Pallas kernels for 3% -> 3%
where the time goes in v10:
time: 127 us; the launch traced here: 126 us
  blocking collectives  95.9 us (76%)
  starting transfers between devices  15.2 us (12%)
  Pallas kernels  9.91 us (8%)
  waiting for transfers between devices  5.19 us (4%)
    all_to_all x7, blocking collectives, exchanged(): return lax.all_to_all(pieces, axis, 0, 0, tiled=True)  95.9 us
    all_to_all x1, starting transfers between devices, exchanged(): return lax.all_to_all(pieces, axis, 0, 0, tiled=True)  12 us
    pallas_call x1, Pallas kernels, on_device(): prepare(live_lengths, in_hbm(kv_cache), in_hbm(gate_sums))  3.92 us
    ppermute x1, starting transfers between devices, on_device(): w_other = lax.ppermute(w_down, 'kv_2', [(0, 1), (1, 0)])  3.14 us
    ppermute x1, waiting for transfers between devices, on_device(): w_other = lax.ppermute(w_down, 'kv_2', [(0, 1), (1, 0)])  2.77 us
  transfers between devices with their start and end apart: 2, of which 2 were waited for; matrix products, arithmetic and copies ran while one was open for 0% of the time, Pallas kernels for 3%

profile of v10, /device:TPU:1, one launch (start us, length us, event | category | flops | bytes accessed | tf_op | source)
XLA Modules:
  0.0 126.4 jit_solution(16146498916505500410)
XLA Ops:
  0.0 0.0 copy-start.6
  0.0 0.0 copy-start.7
  0.1 0.9 shard_map.145
  1.0 16.6 %all_to_all.40 = bf16[16,8,128]{2,1,0:T(8,128)(2,1)S(1)} all-to-all(bf16[16,8,128]{2,1,0:T(8,128)(2,1)S(1)} %shard_map.145), channel_id=1, replica_groups=mesh['kv_0'=8,'kv_1'=2,'kv_2'=2,'tp'=16] {'tp'}, dimensions={0} | all-to-all | bytes 65536 | tf_op jit(solution)/shard_map/all_to_all | solution.py:45
  17.6 0.0 copy-done.5
  17.6 0.0 copy-done.6
  17.6 0.0 copy-done.7
  17.6 0.0 copy-done.8
  17.7 1.1 shard_map.146
  18.8 12.0 %all-to-all-start.1 = ((bf16[32,9,4,128]{3,2,1,0:T(4,128)(2,1)}), bf16[32,9,4,128]{3,2,1,0:T(4,128)(2,1)S(1)}, u32[]{:S(2)}, u32[]{:S(2)}) async-start(bf16[32,9,4,128]{3,2,1,0:T(4,128)(2,1)} %get-tuple-element.20), calls=%async_computation.1 | async-start | bytes 589824 | tf_op jit(solution)/shard_map/all_to_all | solution.py:45
  30.8 3.1 %collective-permute-start = (bf16[704,128]{1,0:T(8,128)(2,1)S(1)}, bf16[704,128]{1,0:T(8,128)(2,1)S(1)}, u32[]{:S(2)}, u32[]{:S(2)}) collective-permute-start(bf16[704,128]{1,0:T(8,128)(2,1)S(1)} %copy-done.3), channel_id=1, source_target_pairs={{0,16},{16,0},{1,17},{17,1},{2,18},{18,2},{3,19},{19,3},{4,20},{20... | collective-permute-start | bytes 540680 | tf_op jit(solution)/shard_map/ppermute | solution.py:459
  34.0 0.0 copy-done.9
  34.0 3.9 %shard_map.147 = (bf16[4,256,512]{2,1,0:T(8,128)(2,1)S(1)}, bf16[4,512,256]{2,1,0:T(8,128)(2,1)S(1)}, f32[4,16,512]{2,1,0:T(8,128)S(1)}) custom-call(s32[16]{0:T(128)S(1)} %copy-done.9, bf16[16,512,128]{2,1,0:T(8,128)(2,1)} %cache.1, f32[16,1,512]{2,1,0:T(1,128)} %gate.1), custom_call_target="tpu_custom_call" | custom-call | tf_op jit(solution)/shard_map/pallas_call | solution.py:476
  37.9 0.0 copy-start.1
  37.9 0.0 copy-start.2
  38.0 2.8 %collective-permute-done.arrived.w_other = bf16[704,128]{1,0:T(8,128)(2,1)S(1)} collective-permute-done((bf16[704,128]{1,0:T(8,128)(2,1)S(1)}, bf16[704,128]{1,0:T(8,128)(2,1)S(1)}, u32[]{:S(2)}, u32[]{:S(2)}) %collective-permute-start) | collective-permute-done | bytes 180256 | tf_op jit(solution)/shard_map/ppermute | solution.py:459
  40.7 2.4 %all-to-all-done.1.recv = bf16[32,9,4,128]{3,2,1,0:T(4,128)(2,1)S(1)} async-done(((bf16[32,9,4,128]{3,2,1,0:T(4,128)(2,1)}), bf16[32,9,4,128]{3,2,1,0:T(4,128)(2,1)S(1)}, u32[]{:S(2)}, u32[]{:S(2)}) %all-to-all-start.1) | async-done | bytes 294944 | tf_op jit(solution)/shard_map/all_to_all | solution.py:45
  43.1 1.5 %shard_map.148 = (bf16[32,9,4,128]{3,2,1,0:T(4,128)(2,1)S(1)}, f32[16,128]{1,0:T(8,128)S(1)}, f32[2,128]{1,0:T(2,128)S(1)}) custom-call(bf16[32,9,4,128]{3,2,1,0:T(4,128)(2,1)S(1)} %all-to-all-done.1.recv, bf16[4,256,512]{2,1,0:T(8,128)(2,1)S(1)} %get-tuple-element.21.keys, bf16[4,512,256]{2,1,0:T(8,128)(2,1)S(1)} %get-tuple-element.22.values, ...), custom_call_target="tpu_custom_call" | custom-call | tf_op jit(solution)/shard_map/pallas_call | solution.py:483
  44.7 0.0 copy-start.10
  44.7 16.7 %all_to_all.41.recv = bf16[32,9,4,128]{3,2,1,0:T(4,128)(2,1)S(1)} all-to-all(bf16[32,9,4,128]{3,2,1,0:T(4,128)(2,1)S(1)} %get-tuple-element.24), channel_id=1, replica_groups=mesh['kv_0'=8,'kv_1'=2,'kv_2'=2,'tp'=16] {'kv_0','kv_1','kv_2'}, dimensions={0} | all-to-all | bytes 589824 | tf_op jit(solution)/shard_map/all_to_all | solution.py:45
  61.4 0.6 shard_map.149
  62.0 13.8 %all_to_all.42.recv = bf16[16,16,128]{2,1,0:T(8,128)(2,1)S(1)} all-to-all(bf16[16,16,128]{2,1,0:T(8,128)(2,1)S(1)} %shard_map.149), channel_id=1, replica_groups=mesh['kv_0'=8,'kv_1'=2,'kv_2'=2,'tp'=16] {'tp'}, dimensions={0} | all-to-all | bytes 131072 | tf_op jit(solution)/shard_map/all_to_all | solution.py:45
  75.8 0.0 copy-done.2
  75.8 0.3 shard_map.150
  76.1 5.3 %all_to_all.43.recv = bf16[2,96,128]{2,1,0:T(8,128)(2,1)S(1)} all-to-all(bf16[2,96,128]{2,1,0:T(8,128)(2,1)S(1)} %get-tuple-element.29), channel_id=1, replica_groups=mesh['kv_0'=8,'kv_1'=2,'kv_2'=2,'tp'=16] {'kv_2'}, dimensions={0} | all-to-all | bytes 98304 | tf_op jit(solution)/shard_map/all_to_all | solution.py:45
  81.4 0.2 shard_map.151
  81.6 17.0 %all_to_all.44.recv = bf16[16,96,128]{2,1,0:T(8,128)(2,1)S(1)} all-to-all(bf16[16,96,128]{2,1,0:T(8,128)(2,1)S(1)} %shard_map.151), channel_id=1, replica_groups=mesh['kv_0'=8,'kv_1'=2,'kv_2'=2,'tp'=16] {'kv_0','kv_1'}, dimensions={0} | all-to-all | bytes 786432 | tf_op jit(solution)/shard_map/all_to_all | solution.py:45
  98.6 0.3 shard_map.152
  98.9 14.8 %all_to_all.45.recv = bf16[32,16,128]{2,1,0:T(8,128)(2,1)S(1)} all-to-all(bf16[32,16,128]{2,1,0:T(8,128)(2,1)S(1)} %get-tuple-element.31), channel_id=1, replica_groups=mesh['kv_0'=8,'kv_1'=2,'kv_2'=2,'tp'=16] {'kv_2','tp'}, dimensions={0} | all-to-all | bytes 262144 | tf_op jit(solution)/shard_map/all_to_all | solution.py:45
  113.7 0.2 shard_map.153
  113.9 11.6 %all_to_all.46.recv = f32[32,1,128]{2,1,0:T(1,128)S(1)} all-to-all(f32[32,1,128]{2,1,0:T(1,128)S(1)} %get-tuple-element.33), channel_id=1, replica_groups=mesh['kv_0'=8,'kv_1'=2,'kv_2'=2,'tp'=16] {'kv_0','kv_1','kv_2'}, dimensions={0} | all-to-all | bytes 32768 | tf_op jit(solution)/shard_map/all_to_all | solution.py:45
  125.5 0.8 shard_map.154
  (11 shorter events, 0.0 us)
Async XLA Ops:
  0.0 17.6 %copy-start = (bf16[256,128]{1,0:T(8,128)(2,1)S(1)}, bf16[256,128]{1,0:T(8,128)(2,1)}, u32[]{:S(2)}) copy-start(bf16[256,128]{1,0:T(8,128)(2,1)} %w_out.3) | copy-start | bytes 196612
  0.0 17.6 %copy-start.4 = (bf16[4096,16]{0,1:T(8,128)(2,1)S(1)}, bf16[4096,16]{0,1:T(8,128)(2,1)}, u32[]{:S(2)}) copy-start(bf16[4096,16]{0,1:T(8,128)(2,1)} %param.22) | copy-start | bytes 393220
  0.0 17.6 %copy-start.5 = (bf16[128,256]{1,0:T(8,128)(2,1)S(1)}, bf16[128,256]{1,0:T(8,128)(2,1)}, u32[]{:S(2)}) copy-start(bf16[128,256]{1,0:T(8,128)(2,1)} %w_query.1) | copy-start | bytes 196612
  0.0 17.6 %copy-start.6 = (bf16[128,64]{0,1:T(8,128)(2,1)S(1)}, bf16[128,64]{0,1:T(8,128)(2,1)}, u32[]{:S(2)}) copy-start(bf16[128,64]{0,1:T(8,128)(2,1)} %param.20) | copy-start | bytes 49156
  0.0 17.6 %copy-start.7 = (bf16[128,64]{0,1:T(8,128)(2,1)S(1)}, bf16[128,64]{0,1:T(8,128)(2,1)}, u32[]{:S(2)}) copy-start(bf16[128,64]{0,1:T(8,128)(2,1)} %param.21) | copy-start | bytes 49156
  0.0 17.6 %copy-start.8 = (f32[16]{0:T(128)S(1)}, f32[16]{0:T(128)}, u32[]{:S(2)}) copy-start(f32[16]{0:T(128)} %param.23) | copy-start | bytes 196
  0.0 30.8 %copy-start.3 = (bf16[704,128]{1,0:T(8,128)(2,1)S(1)}, bf16[704,128]{1,0:T(8,128)(2,1)}, u32[]{:S(2)}) copy-start(bf16[704,128]{1,0:T(8,128)(2,1)} %w_own.1) | copy-start | bytes 540676
  0.0 33.9 %copy-start.9 = (s32[16]{0:T(128)S(1)}, s32[16]{0:T(128)}, u32[]{:S(2)}) copy-start(s32[16]{0:T(128)} %lengths.1) | copy-start | bytes 196
  18.8 24.4 %all-to-all-start.1 = ((bf16[32,9,4,128]{3,2,1,0:T(4,128)(2,1)}), bf16[32,9,4,128]{3,2,1,0:T(4,128)(2,1)S(1)}, u32[]{:S(2)}, u32[]{:S(2)}) async-start(bf16[32,9,4,128]{3,2,1,0:T(4,128)(2,1)} %get-tuple-element.20), calls=%async_computation.1 | async-start | bytes 589824 | tf_op jit(solution)/shard_map/all_to_all | solution.py:45
  30.8 9.9 %collective-permute-start = (bf16[704,128]{1,0:T(8,128)(2,1)S(1)}, bf16[704,128]{1,0:T(8,128)(2,1)S(1)}, u32[]{:S(2)}, u32[]{:S(2)}) collective-permute-start(bf16[704,128]{1,0:T(8,128)(2,1)S(1)} %copy-done.3), channel_id=1, source_target_pairs={{0,16},{16,0},{1,17},{17,1},{2,18},{18,2},{3,19},{19,3},{4,20},{20... | collective-permute-start | bytes 540680 | tf_op jit(solution)/shard_map/ppermute | solution.py:459
  37.9 37.9 %copy-start.1 = (bf16[128,704]{0,1:T(8,128)(2,1)S(1)}, bf16[128,704]{0,1:T(8,128)(2,1)}, u32[]{:S(2)}) copy-start(bf16[128,704]{0,1:T(8,128)(2,1)} %param.26) | copy-start | bytes 540676
  37.9 37.9 %copy-start.2 = (bf16[128,704]{0,1:T(8,128)(2,1)S(1)}, bf16[128,704]{0,1:T(8,128)(2,1)}, u32[]{:S(2)}) copy-start(bf16[128,704]{0,1:T(8,128)(2,1)} %param.27) | copy-start | bytes 540676
  44.7 80.9 %copy-start.10 = (f32[8]{0:T(128)S(1)}, f32[8]{0:T(128)}, u32[]{:S(2)}) copy-start(f32[8]{0:T(128)} %param.29) | copy-start | bytes 100

commit v11 on v8

--- a/solution.py
+++ b/solution.py
@@ -193,7 +193,7 @@
             )
 
 
-def k_attend(recv, keys, values, gate, out, tok_out, sums_out, qs, os):
+def k_attend(recv, keys, values, gate, out, tok_out, sums_out, qs, firsts, seconds):
     rows = 4 * keys.shape[0]
     heads = 4
     scale = DH**-0.5
@@ -233,6 +233,7 @@
     lane = iota((16, LANES), 1)
     spot = jnp.where(iota((16, LANES), 0) % 8 < heads, DH, 0)
     upper = iota((16, LANES), 0) < 8
+    straight = iota((16, LANES), 0) % 8 < heads
     for m in range(rows // 4):
         at = slice(16 * m, 16 * m + 16)
         query = qs[pl.ds(16 * m, 16), :] * scale
@@ -249,25 +250,29 @@
         value = jnp.where(upper, value[:, :LANES], value[:, LANES:])
         value = value + rounded(own_weight) * new_value
         spare = jnp.where(lane == spot, top, jnp.where(lane == spot + 1, total, value))
-        os[pl.ds(16 * m, 16), :] = spare
-    blocks = [os[pl.ds(h, rows, stride=heads), :] for h in range(heads)]
-    turned = [pltpu.roll(block, DH, 1) for block in blocks]
-    firsts = [jnp.where(even, block, turn) for block, turn in zip(blocks, turned)]
-    seconds = [jnp.where(even, turn, block) for block, turn in zip(blocks, turned)]
-    low_out = jnp.where(low, firsts[0], seconds[1]).astype(BF16)
-    high_out = jnp.where(low, firsts[2], seconds[3]).astype(BF16)
+        turned = pltpu.roll(spare, DH, 1)
+        firsts[pl.ds(16 * m, 16), :] = jnp.where(straight, spare, turned)
+        seconds[pl.ds(16 * m, 16), :] = jnp.where(straight, turned, spare)
+        for side in range(2):
+            at = 16 * m + 2 * side
+            left = firsts[pl.ds(at, 4, stride=heads), :]
+            right = seconds[pl.ds(at + 1, 4, stride=heads), :]
+            tile = jnp.where(low[:4], left, right).astype(BF16)
+            for k in range(out.shape[0]):
+                out[k, rows // 4 * side + m] = tile
+    blocks = [seconds[pl.ds(h, rows, stride=heads), :] for h in range(heads)]
     lane = iota((rows, LANES), 1)
     stats = jnp.zeros((rows, LANES), F32)
     for h in range(heads):
-        pieces = [*in_pieces(seconds[h][:, 0:1], 3), *in_pieces(seconds[h][:, 1:2], 2)]
+        pieces = [*in_pieces(blocks[h][:, 0:1], 3), *in_pieces(blocks[h][:, 1:2], 2)]
         for k, piece in enumerate(pieces):
             stats = jnp.where(lane == 8 * h + k, piece, stats)
     packed = stats[:4]
     for g in range(1, rows // 4):
         packed = packed + pltpu.roll(stats, 32 * g, 1)[4 * g : 4 * g + 4]
-    tiles = [*tiles_of(low_out), *tiles_of(high_out), packed.astype(BF16)]
-    for k in range(out.shape[0]):
-        put(out, k, tiles)
+    packed = packed.astype(BF16)
+    for k in range(out.shape[0]):
+        out[k, rows // 2] = packed
 
 
 def k_combine(recv, sums, w_out, out):
@@ -371,19 +376,22 @@
         out[k] = part
 
 
-def k_sums(recv, mid, out, mix_out):
+def k_sums(recv, mid, out, own_out, turned):
     rows, width = mid.shape
     mixture = mid[...] + summed(recv, 0, rows)
-    mix_out[...] = mixture
     centre = jnp.sum(mixture, axis=1, keepdims=True) / width
     square = jnp.sum((mixture - centre) ** 2, axis=1, keepdims=True)
     message = as_row([centre, square])
     for k in range(out.shape[0]):
         out[k] = message
-
-
-def k_finish(recv, mix, gain, out, turned):
-    rows, width = mix.shape
+    turned[...] = mixture.T
+    own = own_out.shape[0]
+    start = pl.multiple_of(lax.axis_index("tp") * own, own)
+    own_out[...] = turned[pl.ds(start, own), :]
+
+
+def k_finish(recv, mix, gain, out):
+    own, rows = mix.shape
     devices = recv.shape[0]
     total = recv[0]
     for k in range(1, devices):
@@ -392,15 +400,10 @@
     spread = (recv[0] - middle) ** 2
     for k in range(1, devices):
         spread = spread + (recv[k] - middle) ** 2
-    square = jnp.where(iota((1, LANES), 1) < rows, spread * width, total)
-    centre = as_column(middle, rows, (0,))
-    shrink = lax.rsqrt(as_column(square, rows, (0, 1)) / D + EPSILON)
-    own = out.shape[0]
-    scaled = ((mix[...] - centre) * shrink).T
-    at = pl.multiple_of(lax.axis_index("tp") * own, own)
-    turned[...] = scaled
-    gain_col = jnp.sum(jnp.where(diagonal(own, 0)[:, :own], gain[...], 0.0), axis=1, keepdims=True)
-    out[...] = (turned[pl.ds(at, own), :] * gain_col).astype(BF16)
+    spread = spread[:, :rows] * (D // devices) + total[:, rows : 2 * rows]
+    shrink = lax.rsqrt(spread / D + EPSILON)
+    column = jnp.sum(jnp.where(diagonal(own, 0)[:, :own], gain[...], 0.0), axis=1, keepdims=True)
+    out[...] = ((mix[...] - middle[:, :rows]) * shrink * column).astype(BF16)
 
 
 def on_device(
@@ -472,7 +475,7 @@
         k_attend,
         [((kv, rows // 2 + 1, 4, LANES), BF16), block, ((2, LANES), F32)],
         [VMEM] * 4,
-        [pltpu.VMEM((4 * rows, LANES), F32), pltpu.VMEM((4 * rows, LANES), F32)],
+        [pltpu.VMEM((4 * rows, LANES), F32)] * 3,
     )(recv, keys, values, gate_sums)
     (message,) = kernel(k_combine, [((tp, rows, width), BF16)], [VMEM] * 3)(
         exchanged(message, KV), sums, w_out
@@ -489,12 +492,15 @@
     (message,) = kernel(
         k_shrink, [((tp, rows, width), BF16)], [VMEM] * 2, [pltpu.VMEM((4 * kv, LANES), F32)]
     )(exchanged(message, KV), w_down)
-    message, mix = kernel(k_sums, [((kv, 1, LANES), F32), block], [VMEM] * 2)(
+    message, mix = kernel(
+        k_sums,
+        [((kv, 1, LANES), F32), ((own, rows), F32)],
+        [VMEM] * 2,
+        [pltpu.VMEM((width, rows), F32)],
+    )(
         exchanged(message, "tp"), mid
     )
-    (out,) = kernel(
-        k_finish, [((own, rows), BF16)], [VMEM] * 3, [pltpu.VMEM((width, rows), F32)], last=True
-    )(exchanged(message, KV), mix, second_gain[None])
+    (out,) = kernel(k_finish, [((own, rows), BF16)], [VMEM] * 3, last=True)(exchanged(message, KV), mix, second_gain[None])
     return out.T
 
 

time: 125 us -> 125 us (level)
  no operation moved by 1% of the time
where the time goes in v11:
time: 125 us; the launch traced here: 124 us
  blocking collectives  94.4 us (76%)
  starting transfers between devices  12 us (10%)
  Pallas kernels  9.51 us (8%)
  waiting for transfers between devices  8.35 us (7%)
    all_to_all x7, blocking collectives, exchanged(): return lax.all_to_all(pieces, axis, 0, 0, tiled=True)  94.4 us
    all_to_all x1, starting transfers between devices, exchanged(): return lax.all_to_all(pieces, axis, 0, 0, tiled=True)  12 us
    all_to_all x1, waiting for transfers between devices, exchanged(): return lax.all_to_all(pieces, axis, 0, 0, tiled=True)  8.35 us
    pallas_call x1, Pallas kernels, on_device(): kernel(k_prepare, [((rows // 4, 4 * DH, positions), BF16), ((rows // 4, p...  3.92 us
  transfers between devices with their start and end apart: 1, of which 1 were waited for; matrix products, arithmetic and copies ran while one was open for 0% of the time, Pallas kernels for 3%

profile of v11, /device:TPU:1, one launch (start us, length us, event | category | flops | bytes accessed | tf_op | source)
XLA Modules:
  0.0 124.4 jit_solution(11228510374828074728)
XLA Ops:
  0.0 0.0 copy-start.6
  0.0 0.0 copy-start.7
  0.0 0.0 copy-start.8
  0.0 0.0 copy-start.9
  0.0 0.9 shard_map.145
  0.9 16.7 %all_to_all.40 = bf16[16,8,128]{2,1,0:T(8,128)(2,1)S(1)} all-to-all(bf16[16,8,128]{2,1,0:T(8,128)(2,1)S(1)} %shard_map.145), channel_id=1, replica_groups=mesh['kv_0'=8,'kv_1'=4,'tp'=16] {'tp'}, dimensions={0} | all-to-all | bytes 65536 | tf_op jit(solution)/shard_map/all_to_all | solution.py:43
  17.6 0.0 copy-done
  17.6 0.0 copy-done.4
  17.6 0.0 copy-done.5
  17.6 0.0 copy-done.6
  17.6 0.0 copy-done.7
  17.6 0.0 copy-done.8
  17.6 1.1 shard_map.146
  18.8 12.0 %all-to-all-start.1 = ((bf16[32,9,4,128]{3,2,1,0:T(4,128)(2,1)}), bf16[32,9,4,128]{3,2,1,0:T(4,128)(2,1)S(1)}, u32[]{:S(2)}, u32[]{:S(2)}) async-start(bf16[32,9,4,128]{3,2,1,0:T(4,128)(2,1)} %get-tuple-element.20), calls=%async_computation.1 | async-start | bytes 589824 | tf_op jit(solution)/shard_map/all_to_all | solution.py:43
  30.8 3.9 %shard_map.147 = (bf16[4,256,512]{2,1,0:T(8,128)(2,1)S(1)}, bf16[4,512,256]{2,1,0:T(8,128)(2,1)S(1)}, f32[4,16,512]{2,1,0:T(8,128)S(1)}) custom-call(s32[16]{0:T(128)S(1)} %copy-done.9, bf16[16,512,128]{2,1,0:T(8,128)(2,1)} %cache.1, f32[16,1,512]{2,1,0:T(1,128)} %gate.1), custom_call_target="tpu_custom_call" | custom-call | tf_op jit(solution)/shard_map/pallas_call | solution.py:459
  34.7 0.0 copy-start.1
  34.7 0.0 copy-start.2
  34.7 8.3 %all-to-all-done.1.recv = bf16[32,9,4,128]{3,2,1,0:T(4,128)(2,1)S(1)} async-done(((bf16[32,9,4,128]{3,2,1,0:T(4,128)(2,1)}), bf16[32,9,4,128]{3,2,1,0:T(4,128)(2,1)S(1)}, u32[]{:S(2)}, u32[]{:S(2)}) %all-to-all-start.1) | async-done | bytes 294944 | tf_op jit(solution)/shard_map/all_to_all | solution.py:43
  43.1 1.5 %shard_map.148 = (bf16[32,9,4,128]{3,2,1,0:T(4,128)(2,1)S(1)}, f32[16,128]{1,0:T(8,128)S(1)}, f32[2,128]{1,0:T(2,128)S(1)}) custom-call(bf16[32,9,4,128]{3,2,1,0:T(4,128)(2,1)S(1)} %all-to-all-done.1.recv, bf16[4,256,512]{2,1,0:T(8,128)(2,1)S(1)} %get-tuple-element.21.keys, bf16[4,512,256]{2,1,0:T(8,128)(2,1)S(1)} %get-tuple-element.22.values, ...), custom_call_target="tpu_custom_call" | custom-call | tf_op jit(solution)/shard_map/pallas_call | solution.py:474
  44.6 15.2 %all_to_all.41.recv = bf16[32,9,4,128]{3,2,1,0:T(4,128)(2,1)S(1)} all-to-all(bf16[32,9,4,128]{3,2,1,0:T(4,128)(2,1)S(1)} %get-tuple-element.24), channel_id=1, replica_groups=mesh['kv_0'=8,'kv_1'=4,'tp'=16] {'kv_0','kv_1'}, dimensions={0} | all-to-all | bytes 589824 | tf_op jit(solution)/shard_map/all_to_all | solution.py:43
  59.8 0.6 shard_map.149
  60.4 13.8 %all_to_all.42.recv = bf16[16,16,128]{2,1,0:T(8,128)(2,1)S(1)} all-to-all(bf16[16,16,128]{2,1,0:T(8,128)(2,1)S(1)} %shard_map.149), channel_id=1, replica_groups=mesh['kv_0'=8,'kv_1'=4,'tp'=16] {'tp'}, dimensions={0} | all-to-all | bytes 131072 | tf_op jit(solution)/shard_map/all_to_all | solution.py:43
  74.2 0.3 shard_map.150
  74.6 12.3 %all_to_all.43.recv = bf16[32,8,128]{2,1,0:T(8,128)(2,1)S(1)} all-to-all(bf16[32,8,128]{2,1,0:T(8,128)(2,1)S(1)} %get-tuple-element.29), channel_id=1, replica_groups=mesh['kv_0'=8,'kv_1'=4,'tp'=16] {'kv_0','kv_1'}, dimensions={0} | all-to-all | bytes 131072 | tf_op jit(solution)/shard_map/all_to_all | solution.py:43
  86.9 0.2 shard_map.151
  87.0 11.8 %all_to_all.44.recv = bf16[32,4,128]{2,1,0:T(4,128)(2,1)S(1)} all-to-all(bf16[32,4,128]{2,1,0:T(4,128)(2,1)S(1)} %get-tuple-element.31), channel_id=1, replica_groups=mesh['kv_0'=8,'kv_1'=4,'tp'=16] {'kv_0','kv_1'}, dimensions={0} | all-to-all | bytes 65536 | tf_op jit(solution)/shard_map/all_to_all | solution.py:43
  98.8 0.0 copy-done.3
  98.8 0.2 shard_map.152
  99.0 13.0 %all_to_all.45.recv = bf16[16,16,128]{2,1,0:T(8,128)(2,1)S(1)} all-to-all(bf16[16,16,128]{2,1,0:T(8,128)(2,1)S(1)} %shard_map.152), channel_id=1, replica_groups=mesh['kv_0'=8,'kv_1'=4,'tp'=16] {'tp'}, dimensions={0} | all-to-all | bytes 131072 | tf_op jit(solution)/shard_map/all_to_all | solution.py:43
  112.0 0.2 shard_map.153
  112.1 11.6 %all_to_all.46.recv = f32[32,1,128]{2,1,0:T(1,128)S(1)} all-to-all(f32[32,1,128]{2,1,0:T(1,128)S(1)} %get-tuple-element.33), channel_id=1, replica_groups=mesh['kv_0'=8,'kv_1'=4,'tp'=16] {'kv_0','kv_1'}, dimensions={0} | all-to-all | bytes 32768 | tf_op jit(solution)/shard_map/all_to_all | solution.py:43
  123.7 0.7 shard_map.154
  (9 shorter events, 0.0 us)
Async XLA Ops:
  0.0 17.6 %copy-start = (bf16[256,128]{1,0:T(8,128)(2,1)S(1)}, bf16[256,128]{1,0:T(8,128)(2,1)}, u32[]{:S(2)}) copy-start(bf16[256,128]{1,0:T(8,128)(2,1)} %w_out.3) | copy-start | bytes 196612
  0.0 17.6 %copy-start.4 = (bf16[4096,16]{0,1:T(8,128)(2,1)S(1)}, bf16[4096,16]{0,1:T(8,128)(2,1)}, u32[]{:S(2)}) copy-start(bf16[4096,16]{0,1:T(8,128)(2,1)} %param.22) | copy-start | bytes 393220
  0.0 17.6 %copy-start.5 = (bf16[128,256]{1,0:T(8,128)(2,1)S(1)}, bf16[128,256]{1,0:T(8,128)(2,1)}, u32[]{:S(2)}) copy-start(bf16[128,256]{1,0:T(8,128)(2,1)} %w_query.1) | copy-start | bytes 196612
  0.0 17.6 %copy-start.6 = (bf16[128,64]{0,1:T(8,128)(2,1)S(1)}, bf16[128,64]{0,1:T(8,128)(2,1)}, u32[]{:S(2)}) copy-start(bf16[128,64]{0,1:T(8,128)(2,1)} %param.20) | copy-start | bytes 49156
  0.0 17.6 %copy-start.7 = (bf16[128,64]{0,1:T(8,128)(2,1)S(1)}, bf16[128,64]{0,1:T(8,128)(2,1)}, u32[]{:S(2)}) copy-start(bf16[128,64]{0,1:T(8,128)(2,1)} %param.21) | copy-start | bytes 49156
  0.0 17.6 %copy-start.8 = (f32[16]{0:T(128)S(1)}, f32[16]{0:T(128)}, u32[]{:S(2)}) copy-start(f32[16]{0:T(128)} %param.23) | copy-start | bytes 196
  0.0 30.7 %copy-start.9 = (s32[16]{0:T(128)S(1)}, s32[16]{0:T(128)}, u32[]{:S(2)}) copy-start(s32[16]{0:T(128)} %lengths.1) | copy-start | bytes 196
  18.8 24.3 %all-to-all-start.1 = ((bf16[32,9,4,128]{3,2,1,0:T(4,128)(2,1)}), bf16[32,9,4,128]{3,2,1,0:T(4,128)(2,1)S(1)}, u32[]{:S(2)}, u32[]{:S(2)}) async-start(bf16[32,9,4,128]{3,2,1,0:T(4,128)(2,1)} %get-tuple-element.20), calls=%async_computation.1 | async-start | bytes 589824 | tf_op jit(solution)/shard_map/all_to_all | solution.py:43
  34.7 39.5 %copy-start.1 = (bf16[128,704]{0,1:T(8,128)(2,1)S(1)}, bf16[128,704]{0,1:T(8,128)(2,1)}, u32[]{:S(2)}) copy-start(bf16[128,704]{0,1:T(8,128)(2,1)} %param.26) | copy-start | bytes 540676
  34.7 39.5 %copy-start.2 = (bf16[128,704]{0,1:T(8,128)(2,1)S(1)}, bf16[128,704]{0,1:T(8,128)(2,1)}, u32[]{:S(2)}) copy-start(bf16[128,704]{0,1:T(8,128)(2,1)} %param.27) | copy-start | bytes 540676
  43.1 55.7 %copy-start.3 = (bf16[704,128]{1,0:T(8,128)(2,1)S(1)}, bf16[704,128]{1,0:T(8,128)(2,1)}, u32[]{:S(2)}) copy-start(bf16[704,128]{1,0:T(8,128)(2,1)} %w_down.1) | copy-start | bytes 540676
  43.1 80.6 %copy-start.10 = (f32[8]{0:T(128)S(1)}, f32[8]{0:T(128)}, u32[]{:S(2)}) copy-start(f32[8]{0:T(128)} %param.29) | copy-start | bytes 100

commit v12 on v11

--- a/solution.py
+++ b/solution.py
@@ -193,7 +193,7 @@
             )
 
 
-def k_attend(recv, keys, values, gate, out, tok_out, sums_out, qs, firsts, seconds):
+def k_attend(recv, keys, values, gate, out, tok_out, sums_out, qs, firsts, seconds, stats):
     rows = 4 * keys.shape[0]
     heads = 4
     scale = DH**-0.5
@@ -234,6 +234,7 @@
     spot = jnp.where(iota((16, LANES), 0) % 8 < heads, DH, 0)
     upper = iota((16, LANES), 0) < 8
     straight = iota((16, LANES), 0) % 8 < heads
+    packed = jnp.zeros((4, LANES), F32)
     for m in range(rows // 4):
         at = slice(16 * m, 16 * m + 16)
         query = qs[pl.ds(16 * m, 16), :] * scale
@@ -252,7 +253,15 @@
         spare = jnp.where(lane == spot, top, jnp.where(lane == spot + 1, total, value))
         turned = pltpu.roll(spare, DH, 1)
         firsts[pl.ds(16 * m, 16), :] = jnp.where(straight, spare, turned)
-        seconds[pl.ds(16 * m, 16), :] = jnp.where(straight, turned, spare)
+        second = jnp.where(straight, turned, spare)
+        seconds[pl.ds(16 * m, 16), :] = second
+        pieces = in_pieces(second, 3)
+        stat = jnp.where(lane < 5, pltpu.roll(pieces[2], 4, 1), 0.0)
+        stat = jnp.where(lane < 4, pltpu.roll(pieces[1], 2, 1), stat)
+        stats[pl.ds(16 * m, 16), :] = jnp.where(lane < 2, pieces[0], stat)
+        for h in range(heads):
+            stat = stats[pl.ds(16 * m + h, 4, stride=heads), :]
+            packed = packed + pltpu.roll(stat, 32 * m + 8 * h, 1)
         for side in range(2):
             at = 16 * m + 2 * side
             left = firsts[pl.ds(at, 4, stride=heads), :]
@@ -260,16 +269,6 @@
             tile = jnp.where(low[:4], left, right).astype(BF16)
             for k in range(out.shape[0]):
                 out[k, rows // 4 * side + m] = tile
-    blocks = [seconds[pl.ds(h, rows, stride=heads), :] for h in range(heads)]
-    lane = iota((rows, LANES), 1)
-    stats = jnp.zeros((rows, LANES), F32)
-    for h in range(heads):
-        pieces = [*in_pieces(blocks[h][:, 0:1], 3), *in_pieces(blocks[h][:, 1:2], 2)]
-        for k, piece in enumerate(pieces):
-            stats = jnp.where(lane == 8 * h + k, piece, stats)
-    packed = stats[:4]
-    for g in range(1, rows // 4):
-        packed = packed + pltpu.roll(stats, 32 * g, 1)[4 * g : 4 * g + 4]
     packed = packed.astype(BF16)
     for k in range(out.shape[0]):
         out[k, rows // 2] = packed
@@ -280,31 +279,38 @@
     tiles = (recv.shape[1] - 1) // 2
     rows = 4 * tiles
     heads = 4 * DH
-    source = iota((LANES, 2 * heads), 0) % 32
-    column = iota((LANES, 2 * heads), 1)
-    first = 8 * ((column % heads) // DH)
-    is_top = column < heads
-    begin = jnp.where(is_top, first, first + 3)
-    end = jnp.where(is_top, first + 3, first + 5)
-    spread = jnp.where((source >= begin) & (source < end), 1.0, 0.0).astype(BF16)
+    source = iota((LANES, 2 * LANES), 0)
+    column = iota((LANES, 2 * LANES), 1)
+    place = source % 8
+    is_top = column < LANES
+    wanted = (place < 5) & (is_top == (place % 2 == 0))
+    wanted = wanted & (source // 8 == column % LANES // 8)
+    pick = jnp.where(wanted, 1.0, 0.0).astype(BF16)
     stats = recv[:, 2 * tiles].astype(F32)
-    stats = jnp.concatenate([stats, stats], axis=1)
-    group = iota(stats.shape, 2) // 32 - iota(stats.shape, 1) // 4
+    stats = jnp.concatenate([stats, stats], axis=1).astype(BF16).reshape(devices * 8, LANES)
+    stats = jnp.dot(stats, pick, preferred_element_type=F32).reshape(devices, 8, 2 * LANES)
+    tops = stats[:, :, :LANES]
+    totals = stats[:, :, LANES:]
+    scales = jnp.exp(tops - jnp.max(tops, axis=0, keepdims=True))
+    joint = jnp.sum(totals * scales, axis=0, keepdims=True)
+    shares = in_pieces(scales * (1.0 / joint), 2)
+    source = iota((2 * LANES, heads), 0) % LANES
+    column = iota((2 * LANES, heads), 1)
+    wanted = (source % 8 == 0) & (source % 32 // 8 == column // DH)
+    spread = jnp.where(wanted, 1.0, 0.0).astype(BF16)
+    group = iota(tops.shape, 2) // 32 - iota(tops.shape, 1) // 4
     blocks = []
     for half in range(2):
-        mine = jnp.where(group == 2 * half, stats, 0.0).astype(BF16).reshape(devices * 8, LANES)
-        wide = jnp.dot(mine, spread, preferred_element_type=F32).reshape(devices, 8, 2 * heads)
-        tops = wide[:, :, :heads]
-        totals = wide[:, :, heads:]
-        scales = jnp.exp(tops - jnp.max(tops, axis=0, keepdims=True))
-        total = jnp.sum(totals * scales, axis=0)
+        mine = [jnp.where(group == 2 * half, share, 0.0) for share in shares]
+        mine = jnp.concatenate(mine, axis=2).astype(BF16).reshape(devices * 8, 2 * LANES)
+        wide = jnp.dot(mine, spread, preferred_element_type=F32).reshape(devices, 8, heads)
         sides = []
         for side in range(2):
             at = tiles * side + 2 * half
             part = [recv[:, at + t].astype(F32) for t in range(2)]
             part = jnp.concatenate(part, axis=1)
-            sides.append(jnp.sum(part * scales[:, :, side * LANES : (side + 1) * LANES], axis=0))
-        blocks.append(jnp.concatenate(sides, axis=1) / total)
+            sides.append(jnp.sum(part * wide[:, :, side * LANES : (side + 1) * LANES], axis=0))
+        blocks.append(jnp.concatenate(sides, axis=1))
     attended = jnp.concatenate(blocks, axis=0).astype(BF16)
     wide = attended.astype(F32)
     mean = wide[:, :LANES] * sums[0:1, :] + wide[:, LANES:] * sums[1:2, :]
@@ -475,7 +481,7 @@
         k_attend,
         [((kv, rows // 2 + 1, 4, LANES), BF16), block, ((2, LANES), F32)],
         [VMEM] * 4,
-        [pltpu.VMEM((4 * rows, LANES), F32)] * 3,
+        [pltpu.VMEM((4 * rows, LANES), F32)] * 4,
     )(recv, keys, values, gate_sums)
     (message,) = kernel(k_combine, [((tp, rows, width), BF16)], [VMEM] * 3)(
         exchanged(message, KV), sums, w_out

time: 125 us -> 125 us (level)
  no operation moved by 1% of the time
where the time goes in v12:
time: 125 us; the launch traced here: 124 us
  blocking collectives  94.4 us (76%)
  starting transfers between devices  12 us (10%)
  Pallas kernels  9.49 us (8%)
  waiting for transfers between devices  8.35 us (7%)
    all_to_all x7, blocking collectives, exchanged(): return lax.all_to_all(pieces, axis, 0, 0, tiled=True)  94.4 us
    all_to_all x1, starting transfers between devices, exchanged(): return lax.all_to_all(pieces, axis, 0, 0, tiled=True)  12 us
    all_to_all x1, waiting for transfers between devices, exchanged(): return lax.all_to_all(pieces, axis, 0, 0, tiled=True)  8.35 us
    pallas_call x1, Pallas kernels, on_device(): kernel(k_prepare, [((rows // 4, 4 * DH, positions), BF16), ((rows // 4, p...  3.92 us
  transfers between devices with their start and end apart: 1, of which 1 were waited for; matrix products, arithmetic and copies ran while one was open for 0% of the time, Pallas kernels for 3%

profile of v12, /device:TPU:1, one launch (start us, length us, event | category | flops | bytes accessed | tf_op | source)
XLA Modules:
  0.0 124.4 jit_solution(14961522143610497643)
XLA Ops:
  0.0 0.0 copy-start.6
  0.0 0.0 copy-start.7
  0.0 0.0 copy-start.8
  0.0 0.0 copy-start.9
  0.0 0.9 shard_map.145
  0.9 16.7 %all_to_all.40 = bf16[16,8,128]{2,1,0:T(8,128)(2,1)S(1)} all-to-all(bf16[16,8,128]{2,1,0:T(8,128)(2,1)S(1)} %shard_map.145), channel_id=1, replica_groups=mesh['kv_0'=8,'kv_1'=4,'tp'=16] {'tp'}, dimensions={0} | all-to-all | bytes 65536 | tf_op jit(solution)/shard_map/all_to_all | solution.py:43
  17.6 0.0 copy-done
  17.6 0.0 copy-done.4
  17.6 0.0 copy-done.5
  17.6 0.0 copy-done.6
  17.6 0.0 copy-done.7
  17.6 1.1 shard_map.146
  18.8 12.0 %all-to-all-start.1 = ((bf16[32,9,4,128]{3,2,1,0:T(4,128)(2,1)}), bf16[32,9,4,128]{3,2,1,0:T(4,128)(2,1)S(1)}, u32[]{:S(2)}, u32[]{:S(2)}) async-start(bf16[32,9,4,128]{3,2,1,0:T(4,128)(2,1)} %get-tuple-element.20), calls=%async_computation.1 | async-start | bytes 589824 | tf_op jit(solution)/shard_map/all_to_all | solution.py:43
  30.8 3.9 %shard_map.147 = (bf16[4,256,512]{2,1,0:T(8,128)(2,1)S(1)}, bf16[4,512,256]{2,1,0:T(8,128)(2,1)S(1)}, f32[4,16,512]{2,1,0:T(8,128)S(1)}) custom-call(s32[16]{0:T(128)S(1)} %copy-done.9, bf16[16,512,128]{2,1,0:T(8,128)(2,1)} %cache.1, f32[16,1,512]{2,1,0:T(1,128)} %gate.1), custom_call_target="tpu_custom_call" | custom-call | tf_op jit(solution)/shard_map/pallas_call | solution.py:465
  34.7 0.0 copy-start.1
  34.7 0.0 copy-start.2
  34.7 8.3 %all-to-all-done.1.recv = bf16[32,9,4,128]{3,2,1,0:T(4,128)(2,1)S(1)} async-done(((bf16[32,9,4,128]{3,2,1,0:T(4,128)(2,1)}), bf16[32,9,4,128]{3,2,1,0:T(4,128)(2,1)S(1)}, u32[]{:S(2)}, u32[]{:S(2)}) %all-to-all-start.1) | async-done | bytes 294944 | tf_op jit(solution)/shard_map/all_to_all | solution.py:43
  43.1 1.5 %shard_map.148 = (bf16[32,9,4,128]{3,2,1,0:T(4,128)(2,1)S(1)}, f32[16,128]{1,0:T(8,128)S(1)}, f32[2,128]{1,0:T(2,128)S(1)}) custom-call(bf16[32,9,4,128]{3,2,1,0:T(4,128)(2,1)S(1)} %all-to-all-done.1.recv, bf16[4,256,512]{2,1,0:T(8,128)(2,1)S(1)} %get-tuple-element.21.keys, bf16[4,512,256]{2,1,0:T(8,128)(2,1)S(1)} %get-tuple-element.22.values, ...), custom_call_target="tpu_custom_call" | custom-call | tf_op jit(solution)/shard_map/pallas_call | solution.py:480
  44.6 15.2 %all_to_all.41.recv = bf16[32,9,4,128]{3,2,1,0:T(4,128)(2,1)S(1)} all-to-all(bf16[32,9,4,128]{3,2,1,0:T(4,128)(2,1)S(1)} %get-tuple-element.24), channel_id=1, replica_groups=mesh['kv_0'=8,'kv_1'=4,'tp'=16] {'kv_0','kv_1'}, dimensions={0} | all-to-all | bytes 589824 | tf_op jit(solution)/shard_map/all_to_all | solution.py:43
  59.8 0.6 shard_map.149
  60.4 13.8 %all_to_all.42.recv = bf16[16,16,128]{2,1,0:T(8,128)(2,1)S(1)} all-to-all(bf16[16,16,128]{2,1,0:T(8,128)(2,1)S(1)} %shard_map.149), channel_id=1, replica_groups=mesh['kv_0'=8,'kv_1'=4,'tp'=16] {'tp'}, dimensions={0} | all-to-all | bytes 131072 | tf_op jit(solution)/shard_map/all_to_all | solution.py:43
  74.2 0.0 copy-done.1
  74.2 0.3 shard_map.150
  74.5 12.3 %all_to_all.43.recv = bf16[32,8,128]{2,1,0:T(8,128)(2,1)S(1)} all-to-all(bf16[32,8,128]{2,1,0:T(8,128)(2,1)S(1)} %get-tuple-element.29), channel_id=1, replica_groups=mesh['kv_0'=8,'kv_1'=4,'tp'=16] {'kv_0','kv_1'}, dimensions={0} | all-to-all | bytes 131072 | tf_op jit(solution)/shard_map/all_to_all | solution.py:43
  86.9 0.2 shard_map.151
  87.0 11.8 %all_to_all.44.recv = bf16[32,4,128]{2,1,0:T(4,128)(2,1)S(1)} all-to-all(bf16[32,4,128]{2,1,0:T(4,128)(2,1)S(1)} %get-tuple-element.31), channel_id=1, replica_groups=mesh['kv_0'=8,'kv_1'=4,'tp'=16] {'kv_0','kv_1'}, dimensions={0} | all-to-all | bytes 65536 | tf_op jit(solution)/shard_map/all_to_all | solution.py:43
  98.8 0.2 shard_map.152
  99.0 13.0 %all_to_all.45.recv = bf16[16,16,128]{2,1,0:T(8,128)(2,1)S(1)} all-to-all(bf16[16,16,128]{2,1,0:T(8,128)(2,1)S(1)} %shard_map.152), channel_id=1, replica_groups=mesh['kv_0'=8,'kv_1'=4,'tp'=16] {'tp'}, dimensions={0} | all-to-all | bytes 131072 | tf_op jit(solution)/shard_map/all_to_all | solution.py:43
  111.9 0.2 shard_map.153
  112.1 11.6 %all_to_all.46.recv = f32[32,1,128]{2,1,0:T(1,128)S(1)} all-to-all(f32[32,1,128]{2,1,0:T(1,128)S(1)} %get-tuple-element.33), channel_id=1, replica_groups=mesh['kv_0'=8,'kv_1'=4,'tp'=16] {'kv_0','kv_1'}, dimensions={0} | all-to-all | bytes 32768 | tf_op jit(solution)/shard_map/all_to_all | solution.py:43
  123.7 0.0 copy-done.10
  123.7 0.7 shard_map.154
  (9 shorter events, 0.0 us)
Async XLA Ops:
  0.0 17.6 %copy-start = (bf16[256,128]{1,0:T(8,128)(2,1)S(1)}, bf16[256,128]{1,0:T(8,128)(2,1)}, u32[]{:S(2)}) copy-start(bf16[256,128]{1,0:T(8,128)(2,1)} %w_out.3) | copy-start | bytes 196612
  0.0 17.6 %copy-start.4 = (bf16[4096,16]{0,1:T(8,128)(2,1)S(1)}, bf16[4096,16]{0,1:T(8,128)(2,1)}, u32[]{:S(2)}) copy-start(bf16[4096,16]{0,1:T(8,128)(2,1)} %param.22) | copy-start | bytes 393220
  0.0 17.6 %copy-start.5 = (bf16[128,256]{1,0:T(8,128)(2,1)S(1)}, bf16[128,256]{1,0:T(8,128)(2,1)}, u32[]{:S(2)}) copy-start(bf16[128,256]{1,0:T(8,128)(2,1)} %w_query.1) | copy-start | bytes 196612
  0.0 17.6 %copy-start.6 = (bf16[128,64]{0,1:T(8,128)(2,1)S(1)}, bf16[128,64]{0,1:T(8,128)(2,1)}, u32[]{:S(2)}) copy-start(bf16[128,64]{0,1:T(8,128)(2,1)} %param.20) | copy-start | bytes 49156
  0.0 17.6 %copy-start.7 = (bf16[128,64]{0,1:T(8,128)(2,1)S(1)}, bf16[128,64]{0,1:T(8,128)(2,1)}, u32[]{:S(2)}) copy-start(bf16[128,64]{0,1:T(8,128)(2,1)} %param.21) | copy-start | bytes 49156
  0.0 17.6 %copy-start.8 = (f32[16]{0:T(128)S(1)}, f32[16]{0:T(128)}, u32[]{:S(2)}) copy-start(f32[16]{0:T(128)} %param.23) | copy-start | bytes 196
  0.0 30.7 %copy-start.9 = (s32[16]{0:T(128)S(1)}, s32[16]{0:T(128)}, u32[]{:S(2)}) copy-start(s32[16]{0:T(128)} %lengths.1) | copy-start | bytes 196
  18.8 24.3 %all-to-all-start.1 = ((bf16[32,9,4,128]{3,2,1,0:T(4,128)(2,1)}), bf16[32,9,4,128]{3,2,1,0:T(4,128)(2,1)S(1)}, u32[]{:S(2)}, u32[]{:S(2)}) async-start(bf16[32,9,4,128]{3,2,1,0:T(4,128)(2,1)} %get-tuple-element.20), calls=%async_computation.1 | async-start | bytes 589824 | tf_op jit(solution)/shard_map/all_to_all | solution.py:43
  34.7 39.5 %copy-start.1 = (bf16[128,704]{0,1:T(8,128)(2,1)S(1)}, bf16[128,704]{0,1:T(8,128)(2,1)}, u32[]{:S(2)}) copy-start(bf16[128,704]{0,1:T(8,128)(2,1)} %param.26) | copy-start | bytes 540676
  34.7 39.5 %copy-start.2 = (bf16[128,704]{0,1:T(8,128)(2,1)S(1)}, bf16[128,704]{0,1:T(8,128)(2,1)}, u32[]{:S(2)}) copy-start(bf16[128,704]{0,1:T(8,128)(2,1)} %param.27) | copy-start | bytes 540676
  43.1 55.7 %copy-start.3 = (bf16[704,128]{1,0:T(8,128)(2,1)S(1)}, bf16[704,128]{1,0:T(8,128)(2,1)}, u32[]{:S(2)}) copy-start(bf16[704,128]{1,0:T(8,128)(2,1)} %w_down.1) | copy-start | bytes 540676
  43.1 80.6 %copy-start.10 = (f32[8]{0:T(128)S(1)}, f32[8]{0:T(128)}, u32[]{:S(2)}) copy-start(f32[8]{0:T(128)} %param.29) | copy-start | bytes 100

commit v13 on v12

--- a/solution.py
+++ b/solution.py
@@ -23,15 +23,17 @@
 ANY = pl.BlockSpec(memory_space=pl.ANY)
 
 
-def kernel(body, outs, specs, scratch=(), last=False, flops=None):
+def kernel(body, outs, specs, scratch=(), last=False, first=False, flops=None):
     return pl.pallas_call(
         body,
         out_shape=[
-            jax.ShapeDtypeStruct(shape, dtype) if last else pltpu.VMEM(shape, dtype)
-            for shape, dtype in outs
+            jax.ShapeDtypeStruct(shape, dtype)
+            if last or (first and n == 0)
+            else pltpu.VMEM(shape, dtype)
+            for n, (shape, dtype) in enumerate(outs)
         ],
         in_specs=specs,
-        out_specs=[VMEM] * len(outs),
+        out_specs=[ANY if first and n == 0 else VMEM for n in range(len(outs))],
         scratch_shapes=scratch,
         cost_estimate=flops
         and pl.CostEstimate(flops=flops, bytes_accessed=flops // 100, transcendentals=0),
@@ -135,7 +137,7 @@
         out[k] = tile
 
 
-def k_project(recv, w_query, w_key, w_value, w_forget, w_out, bias, out, x_out, gain_out, new_rows):
+def k_project(recv, w_query, w_key, w_value, w_forget, w_out, bias, out, x_out, gain_out, new_rows, staged, sem):
     width = recv.shape[0]
     same = jnp.where(iota((width, width), 0) == iota((width, width), 1), 1.0, 0.0).astype(BF16)
     rows = new_rows.shape[0]
@@ -164,10 +166,19 @@
     tail = jnp.where(row == 2, sums[:, :LANES], tail)
     tail = jnp.where(row == 3, sums[:, LANES:], tail)
     tiles = tiles_of(query[:, :LANES].astype(BF16)) + tiles_of(query[:, LANES:].astype(BF16))
+    devices = staged.shape[0]
+    copies = []
     for b in range(rows):
         own_tail = jnp.where(row == 0, new_rows[pl.ds(b, 1), :], tail)[:4].astype(BF16)
-        for k in range(b, out.shape[0], rows):
-            put(out, k, [*tiles, own_tail])
+        for k in range(b, devices, rows):
+            put(staged, k, [*tiles, own_tail])
+        if b % 4 == 3:
+            for k in range(b - 3, devices, rows):
+                at = pl.ds(k, 4)
+                copies.append(pltpu.make_async_copy(staged.at[at], out.at[at], sem.at[k // 4]))
+                copies[-1].start()
+    for copy in copies:
+        copy.wait()
 
 
 def k_prepare(lengths, cache, gate, keys_o, values_o, gate_o, cache_v, gate_v, sem, gate_sem):
@@ -450,7 +461,12 @@
         k_project,
         [((kv, rows // 2 + 1, 4, LANES), BF16), block, ((8, LANES), F32)],
         [VMEM] * 7,
-        [pltpu.VMEM((rows, LANES), F32)],
+        [
+            pltpu.VMEM((rows, LANES), F32),
+            pltpu.VMEM((kv, rows // 2 + 1, 4, LANES), BF16),
+            pltpu.SemaphoreType.DMA((kv // 4,)),
+        ],
+        first=True,
     )(
         recv,
         w_query,

time: 125 us -> 125 us (level)
  no operation moved by 1% of the time
where the time goes in v13:
time: 125 us; the launch traced here: 124 us
  blocking collectives  94.4 us (76%)
  starting transfers between devices  12 us (10%)
  Pallas kernels  9.53 us (8%)
  waiting for transfers between devices  8.35 us (7%)
    all_to_all x7, blocking collectives, exchanged(): return lax.all_to_all(pieces, axis, 0, 0, tiled=True)  94.4 us
    all_to_all x1, starting transfers between devices, exchanged(): return lax.all_to_all(pieces, axis, 0, 0, tiled=True)  12 us
    all_to_all x1, waiting for transfers between devices, exchanged(): return lax.all_to_all(pieces, axis, 0, 0, tiled=True)  8.35 us
    pallas_call x1, Pallas kernels, on_device(): kernel(k_prepare, [((rows // 4, 4 * DH, positions), BF16), ((rows // 4, p...  3.92 us
  transfers between devices with their start and end apart: 1, of which 1 were waited for; matrix products, arithmetic and copies ran while one was open for 0% of the time, Pallas kernels for 3%

profile of v13, /device:TPU:1, one launch (start us, length us, event | category | flops | bytes accessed | tf_op | source)
XLA Modules:
  0.0 124.5 jit_solution(9897736057422372390)
XLA Ops:
  0.0 0.0 copy-start.6
  0.0 0.0 copy-start.7
  0.0 0.0 copy-start.8
  0.0 0.0 copy-start.9
  0.0 0.9 shard_map.145
  0.9 16.7 %all_to_all.40 = bf16[16,8,128]{2,1,0:T(8,128)(2,1)S(1)} all-to-all(bf16[16,8,128]{2,1,0:T(8,128)(2,1)S(1)} %shard_map.145), channel_id=1, replica_groups=mesh['kv_0'=8,'kv_1'=4,'tp'=16] {'tp'}, dimensions={0} | all-to-all | bytes 65536 | tf_op jit(solution)/shard_map/all_to_all | solution.py:45
  17.6 0.0 copy-done
  17.6 0.0 copy-done.4
  17.6 0.0 copy-done.5
  17.6 0.0 copy-done.6
  17.6 0.0 copy-done.7
  17.6 0.0 copy-done.8
  17.6 1.2 shard_map.146
  18.8 12.0 %all-to-all-start.1 = ((bf16[32,9,4,128]{3,2,1,0:T(4,128)(2,1)}), bf16[32,9,4,128]{3,2,1,0:T(4,128)(2,1)S(1)}, u32[]{:S(2)}, u32[]{:S(2)}) async-start(bf16[32,9,4,128]{3,2,1,0:T(4,128)(2,1)} %get-tuple-element.20), calls=%async_computation.1 | async-start | bytes 589824 | tf_op jit(solution)/shard_map/all_to_all | solution.py:45
  30.8 0.0 copy-done.9
  30.9 3.9 %shard_map.147 = (bf16[4,256,512]{2,1,0:T(8,128)(2,1)S(1)}, bf16[4,512,256]{2,1,0:T(8,128)(2,1)S(1)}, f32[4,16,512]{2,1,0:T(8,128)S(1)}) custom-call(s32[16]{0:T(128)S(1)} %copy-done.9, bf16[16,512,128]{2,1,0:T(8,128)(2,1)} %cache.1, f32[16,1,512]{2,1,0:T(1,128)} %gate.1), custom_call_target="tpu_custom_call" | custom-call | tf_op jit(solution)/shard_map/pallas_call | solution.py:481
  34.8 0.0 copy-start.1
  34.8 0.0 copy-start.2
  34.8 8.3 %all-to-all-done.1.recv = bf16[32,9,4,128]{3,2,1,0:T(4,128)(2,1)S(1)} async-done(((bf16[32,9,4,128]{3,2,1,0:T(4,128)(2,1)}), bf16[32,9,4,128]{3,2,1,0:T(4,128)(2,1)S(1)}, u32[]{:S(2)}, u32[]{:S(2)}) %all-to-all-start.1) | async-done | bytes 294944 | tf_op jit(solution)/shard_map/all_to_all | solution.py:45
  43.2 1.5 %shard_map.148 = (bf16[32,9,4,128]{3,2,1,0:T(4,128)(2,1)S(1)}, f32[16,128]{1,0:T(8,128)S(1)}, f32[2,128]{1,0:T(2,128)S(1)}) custom-call(bf16[32,9,4,128]{3,2,1,0:T(4,128)(2,1)S(1)} %all-to-all-done.1.recv, bf16[4,256,512]{2,1,0:T(8,128)(2,1)S(1)} %get-tuple-element.21.keys, bf16[4,512,256]{2,1,0:T(8,128)(2,1)S(1)} %get-tuple-element.22.values, ...), custom_call_target="tpu_custom_call" | custom-call | tf_op jit(solution)/shard_map/pallas_call | solution.py:496
  44.6 15.2 %all_to_all.41.recv = bf16[32,9,4,128]{3,2,1,0:T(4,128)(2,1)S(1)} all-to-all(bf16[32,9,4,128]{3,2,1,0:T(4,128)(2,1)S(1)} %get-tuple-element.24), channel_id=1, replica_groups=mesh['kv_0'=8,'kv_1'=4,'tp'=16] {'kv_0','kv_1'}, dimensions={0} | all-to-all | bytes 589824 | tf_op jit(solution)/shard_map/all_to_all | solution.py:45
  59.9 0.6 shard_map.149
  60.5 13.8 %all_to_all.42.recv = bf16[16,16,128]{2,1,0:T(8,128)(2,1)S(1)} all-to-all(bf16[16,16,128]{2,1,0:T(8,128)(2,1)S(1)} %shard_map.149), channel_id=1, replica_groups=mesh['kv_0'=8,'kv_1'=4,'tp'=16] {'tp'}, dimensions={0} | all-to-all | bytes 131072 | tf_op jit(solution)/shard_map/all_to_all | solution.py:45
  74.3 0.3 shard_map.150
  74.6 12.3 %all_to_all.43.recv = bf16[32,8,128]{2,1,0:T(8,128)(2,1)S(1)} all-to-all(bf16[32,8,128]{2,1,0:T(8,128)(2,1)S(1)} %get-tuple-element.29), channel_id=1, replica_groups=mesh['kv_0'=8,'kv_1'=4,'tp'=16] {'kv_0','kv_1'}, dimensions={0} | all-to-all | bytes 131072 | tf_op jit(solution)/shard_map/all_to_all | solution.py:45
  86.9 0.2 shard_map.151
  87.1 11.8 %all_to_all.44.recv = bf16[32,4,128]{2,1,0:T(4,128)(2,1)S(1)} all-to-all(bf16[32,4,128]{2,1,0:T(4,128)(2,1)S(1)} %get-tuple-element.31), channel_id=1, replica_groups=mesh['kv_0'=8,'kv_1'=4,'tp'=16] {'kv_0','kv_1'}, dimensions={0} | all-to-all | bytes 65536 | tf_op jit(solution)/shard_map/all_to_all | solution.py:45
  98.9 0.2 shard_map.152
  99.0 13.0 %all_to_all.45.recv = bf16[16,16,128]{2,1,0:T(8,128)(2,1)S(1)} all-to-all(bf16[16,16,128]{2,1,0:T(8,128)(2,1)S(1)} %shard_map.152), channel_id=1, replica_groups=mesh['kv_0'=8,'kv_1'=4,'tp'=16] {'tp'}, dimensions={0} | all-to-all | bytes 131072 | tf_op jit(solution)/shard_map/all_to_all | solution.py:45
  112.0 0.2 shard_map.153
  112.2 11.6 %all_to_all.46.recv = f32[32,1,128]{2,1,0:T(1,128)S(1)} all-to-all(f32[32,1,128]{2,1,0:T(1,128)S(1)} %get-tuple-element.33), channel_id=1, replica_groups=mesh['kv_0'=8,'kv_1'=4,'tp'=16] {'kv_0','kv_1'}, dimensions={0} | all-to-all | bytes 32768 | tf_op jit(solution)/shard_map/all_to_all | solution.py:45
  123.8 0.7 shard_map.154
  (9 shorter events, 0.0 us)
Async XLA Ops:
  0.0 17.6 %copy-start = (bf16[256,128]{1,0:T(8,128)(2,1)S(1)}, bf16[256,128]{1,0:T(8,128)(2,1)}, u32[]{:S(2)}) copy-start(bf16[256,128]{1,0:T(8,128)(2,1)} %w_out.3) | copy-start | bytes 196612
  0.0 17.6 %copy-start.4 = (bf16[4096,16]{0,1:T(8,128)(2,1)S(1)}, bf16[4096,16]{0,1:T(8,128)(2,1)}, u32[]{:S(2)}) copy-start(bf16[4096,16]{0,1:T(8,128)(2,1)} %param.22) | copy-start | bytes 393220
  0.0 17.6 %copy-start.5 = (bf16[128,256]{1,0:T(8,128)(2,1)S(1)}, bf16[128,256]{1,0:T(8,128)(2,1)}, u32[]{:S(2)}) copy-start(bf16[128,256]{1,0:T(8,128)(2,1)} %w_query.1) | copy-start | bytes 196612
  0.0 17.6 %copy-start.6 = (bf16[128,64]{0,1:T(8,128)(2,1)S(1)}, bf16[128,64]{0,1:T(8,128)(2,1)}, u32[]{:S(2)}) copy-start(bf16[128,64]{0,1:T(8,128)(2,1)} %param.20) | copy-start | bytes 49156
  0.0 17.6 %copy-start.7 = (bf16[128,64]{0,1:T(8,128)(2,1)S(1)}, bf16[128,64]{0,1:T(8,128)(2,1)}, u32[]{:S(2)}) copy-start(bf16[128,64]{0,1:T(8,128)(2,1)} %param.21) | copy-start | bytes 49156
  0.0 17.6 %copy-start.8 = (f32[16]{0:T(128)S(1)}, f32[16]{0:T(128)}, u32[]{:S(2)}) copy-start(f32[16]{0:T(128)} %param.23) | copy-start | bytes 196
  0.0 30.8 %copy-start.9 = (s32[16]{0:T(128)S(1)}, s32[16]{0:T(128)}, u32[]{:S(2)}) copy-start(s32[16]{0:T(128)} %lengths.1) | copy-start | bytes 196
  18.8 24.3 %all-to-all-start.1 = ((bf16[32,9,4,128]{3,2,1,0:T(4,128)(2,1)}), bf16[32,9,4,128]{3,2,1,0:T(4,128)(2,1)S(1)}, u32[]{:S(2)}, u32[]{:S(2)}) async-start(bf16[32,9,4,128]{3,2,1,0:T(4,128)(2,1)} %get-tuple-element.20), calls=%async_computation.1 | async-start | bytes 589824 | tf_op jit(solution)/shard_map/all_to_all | solution.py:45
  34.8 39.5 %copy-start.1 = (bf16[128,704]{0,1:T(8,128)(2,1)S(1)}, bf16[128,704]{0,1:T(8,128)(2,1)}, u32[]{:S(2)}) copy-start(bf16[128,704]{0,1:T(8,128)(2,1)} %param.26) | copy-start | bytes 540676
  34.8 39.5 %copy-start.2 = (bf16[128,704]{0,1:T(8,128)(2,1)S(1)}, bf16[128,704]{0,1:T(8,128)(2,1)}, u32[]{:S(2)}) copy-start(bf16[128,704]{0,1:T(8,128)(2,1)} %param.27) | copy-start | bytes 540676
  43.2 55.7 %copy-start.3 = (bf16[704,128]{1,0:T(8,128)(2,1)S(1)}, bf16[704,128]{1,0:T(8,128)(2,1)}, u32[]{:S(2)}) copy-start(bf16[704,128]{1,0:T(8,128)(2,1)} %w_down.1) | copy-start | bytes 540676
  43.2 80.6 %copy-start.10 = (f32[8]{0:T(128)S(1)}, f32[8]{0:T(128)}, u32[]{:S(2)}) copy-start(f32[8]{0:T(128)} %param.29) | copy-start | bytes 100

commit v14 on v12

--- a/solution.py
+++ b/solution.py
@@ -170,13 +170,37 @@
             put(out, k, [*tiles, own_tail])
 
 
-def k_prepare(lengths, cache, gate, keys_o, values_o, gate_o, cache_v, gate_v, sem, gate_sem):
+def k_prepare(
+    lengths,
+    cache,
+    gate,
+    keys_o,
+    values_o,
+    gate_o,
+    pick_o,
+    spread_o,
+    cache_v,
+    gate_v,
+    sem,
+    gate_sem,
+):
     rows, positions = cache.shape[:2]
     copies = [pltpu.make_async_copy(cache.at[b], cache_v.at[b], sem.at[b]) for b in range(rows)]
     gates = pltpu.make_async_copy(gate, gate_v, gate_sem)
     gates.start()
     for copy in copies:
         copy.start()
+    source = iota((LANES, 2 * LANES), 0)
+    column = iota((LANES, 2 * LANES), 1)
+    place = source % 8
+    is_top = column < LANES
+    wanted = (place < 5) & (is_top == (place % 2 == 0))
+    wanted = wanted & (source // 8 == column % LANES // 8)
+    pick_o[...] = jnp.where(wanted, 1.0, 0.0).astype(BF16)
+    source = iota((2 * LANES, 4 * DH), 0) % LANES
+    column = iota((2 * LANES, 4 * DH), 1)
+    wanted = (source % 8 == 0) & (source % 32 // 8 == column // DH)
+    spread_o[...] = jnp.where(wanted, 1.0, 0.0).astype(BF16)
     gates.wait()
     place = kv_index() * positions + iota((8, positions), 1)
     first = iota((8, positions), 0) < 4
@@ -274,36 +298,25 @@
         out[k, rows // 2] = packed
 
 
-def k_combine(recv, sums, w_out, out):
+def k_combine(recv, sums, w_out, pick, spread, out):
     devices = recv.shape[0]
     tiles = (recv.shape[1] - 1) // 2
     rows = 4 * tiles
     heads = 4 * DH
-    source = iota((LANES, 2 * LANES), 0)
-    column = iota((LANES, 2 * LANES), 1)
-    place = source % 8
-    is_top = column < LANES
-    wanted = (place < 5) & (is_top == (place % 2 == 0))
-    wanted = wanted & (source // 8 == column % LANES // 8)
-    pick = jnp.where(wanted, 1.0, 0.0).astype(BF16)
     stats = recv[:, 2 * tiles].astype(F32)
     stats = jnp.concatenate([stats, stats], axis=1).astype(BF16).reshape(devices * 8, LANES)
-    stats = jnp.dot(stats, pick, preferred_element_type=F32).reshape(devices, 8, 2 * LANES)
+    stats = jnp.dot(stats, pick[...], preferred_element_type=F32).reshape(devices, 8, 2 * LANES)
     tops = stats[:, :, :LANES]
     totals = stats[:, :, LANES:]
     scales = jnp.exp(tops - jnp.max(tops, axis=0, keepdims=True))
     joint = jnp.sum(totals * scales, axis=0, keepdims=True)
     shares = in_pieces(scales * (1.0 / joint), 2)
-    source = iota((2 * LANES, heads), 0) % LANES
-    column = iota((2 * LANES, heads), 1)
-    wanted = (source % 8 == 0) & (source % 32 // 8 == column // DH)
-    spread = jnp.where(wanted, 1.0, 0.0).astype(BF16)
     group = iota(tops.shape, 2) // 32 - iota(tops.shape, 1) // 4
     blocks = []
     for half in range(2):
         mine = [jnp.where(group == 2 * half, share, 0.0) for share in shares]
         mine = jnp.concatenate(mine, axis=2).astype(BF16).reshape(devices * 8, 2 * LANES)
-        wide = jnp.dot(mine, spread, preferred_element_type=F32).reshape(devices, 8, heads)
+        wide = jnp.dot(mine, spread[...], preferred_element_type=F32).reshape(devices, 8, heads)
         sides = []
         for side in range(2):
             at = tiles * side + 2 * half
@@ -462,12 +475,14 @@
     )
     recv = exchanged(message, KV)
     positions = kv_cache.shape[1]
-    keys, values, gate_sums = kernel(
+    keys, values, gate_sums, pick, spread = kernel(
         k_prepare,
         [
             ((rows // 4, 4 * DH, positions), BF16),
             ((rows // 4, positions, 4 * DH), BF16),
             ((rows // 4, 16, positions), F32),
+            ((LANES, 2 * LANES), BF16),
+            ((2 * LANES, 4 * DH), BF16),
         ],
         [SMEM, ANY, ANY],
         [
@@ -483,8 +498,8 @@
         [VMEM] * 4,
         [pltpu.VMEM((4 * rows, LANES), F32)] * 4,
     )(recv, keys, values, gate_sums)
-    (message,) = kernel(k_combine, [((tp, rows, width), BF16)], [VMEM] * 3)(
-        exchanged(message, KV), sums, w_out
+    (message,) = kernel(k_combine, [((tp, rows, width), BF16)], [VMEM] * 5)(
+        exchanged(message, KV), sums, w_out, pick, spread
     )
     message, scaled = kernel(
         k_expand,

time: 125 us -> 125 us (level)
  no operation moved by 1% of the time
where the time goes in v14:
time: 125 us; the launch traced here: 124 us
  blocking collectives  94.4 us (76%)
  starting transfers between devices  12 us (10%)
  Pallas kernels  9.46 us (8%)
  waiting for transfers between devices  8.35 us (7%)
    all_to_all x7, blocking collectives, exchanged(): return lax.all_to_all(pieces, axis, 0, 0, tiled=True)  94.4 us
    all_to_all x1, starting transfers between devices, exchanged(): return lax.all_to_all(pieces, axis, 0, 0, tiled=True)  12 us
    all_to_all x1, waiting for transfers between devices, exchanged(): return lax.all_to_all(pieces, axis, 0, 0, tiled=True)  8.35 us
    pallas_call x1, Pallas kernels, on_device(): kernel(k_prepare, [((rows // 4, 4 * DH, positions), BF16), ((rows // 4, p...  3.92 us
  transfers between devices with their start and end apart: 1, of which 1 were waited for; matrix products, arithmetic and copies ran while one was open for 0% of the time, Pallas kernels for 3%

profile of v14, /device:TPU:1, one launch (start us, length us, event | category | flops | bytes accessed | tf_op | source)
XLA Modules:
  0.0 124.4 jit_solution(4747518144545593816)
XLA Ops:
  0.0 0.0 copy-start.6
  0.0 0.0 copy-start.7
  0.0 0.0 copy-start.8
  0.0 0.0 copy-start.9
  0.0 0.9 shard_map.145
  0.9 16.7 %all_to_all.40 = bf16[16,8,128]{2,1,0:T(8,128)(2,1)S(1)} all-to-all(bf16[16,8,128]{2,1,0:T(8,128)(2,1)S(1)} %shard_map.145), channel_id=1, replica_groups=mesh['kv_0'=8,'kv_1'=4,'tp'=16] {'tp'}, dimensions={0} | all-to-all | bytes 65536 | tf_op jit(solution)/shard_map/all_to_all | solution.py:43
  17.6 0.0 copy-done
  17.6 0.0 copy-done.4
  17.6 0.0 copy-done.5
  17.6 0.0 copy-done.6
  17.6 0.0 copy-done.7
  17.6 0.0 copy-done.8
  17.6 1.1 shard_map.146
  18.8 12.0 %all-to-all-start.1 = ((bf16[32,9,4,128]{3,2,1,0:T(4,128)(2,1)}), bf16[32,9,4,128]{3,2,1,0:T(4,128)(2,1)S(1)}, u32[]{:S(2)}, u32[]{:S(2)}) async-start(bf16[32,9,4,128]{3,2,1,0:T(4,128)(2,1)} %get-tuple-element.22), calls=%async_computation.1 | async-start | bytes 589824 | tf_op jit(solution)/shard_map/all_to_all | solution.py:43
  30.8 3.9 %shard_map.147 = (bf16[4,256,512]{2,1,0:T(8,128)(2,1)S(1)}, bf16[4,512,256]{2,1,0:T(8,128)(2,1)S(1)}, f32[4,16,512]{2,1,0:T(8,128)S(1)}, bf16[128,256]{1,0:T(8,128)(2,1)S(1)}, bf16[256,256]{1,0:T(8,128)(2,1)S(1)}) custom-call(s32[16]{0:T(128)S(1)} %copy-done.9, bf16[16,512,128]{2,1,0:T(8,128)(2,1)} %cache.1, f32[16,1,512]{2,1,0:T(1,128)} %gate.1), custom_call_target="tpu_custom_call" | custom-call | tf_op jit(solution)/shard_map/pallas_call | solution.py:478
  34.7 0.0 copy-start.1
  34.7 0.0 copy-start.2
  34.7 8.3 %all-to-all-done.1.recv = bf16[32,9,4,128]{3,2,1,0:T(4,128)(2,1)S(1)} async-done(((bf16[32,9,4,128]{3,2,1,0:T(4,128)(2,1)}), bf16[32,9,4,128]{3,2,1,0:T(4,128)(2,1)S(1)}, u32[]{:S(2)}, u32[]{:S(2)}) %all-to-all-start.1) | async-done | bytes 294944 | tf_op jit(solution)/shard_map/all_to_all | solution.py:43
  43.1 1.5 %shard_map.148 = (bf16[32,9,4,128]{3,2,1,0:T(4,128)(2,1)S(1)}, f32[16,128]{1,0:T(8,128)S(1)}, f32[2,128]{1,0:T(2,128)S(1)}) custom-call(bf16[32,9,4,128]{3,2,1,0:T(4,128)(2,1)S(1)} %all-to-all-done.1.recv, bf16[4,256,512]{2,1,0:T(8,128)(2,1)S(1)} %get-tuple-element.23.keys, bf16[4,512,256]{2,1,0:T(8,128)(2,1)S(1)} %get-tuple-element.24.values, ...), custom_call_target="tpu_custom_call" | custom-call | tf_op jit(solution)/shard_map/pallas_call | solution.py:495
  44.6 15.2 %all_to_all.41.recv = bf16[32,9,4,128]{3,2,1,0:T(4,128)(2,1)S(1)} all-to-all(bf16[32,9,4,128]{3,2,1,0:T(4,128)(2,1)S(1)} %get-tuple-element.26), channel_id=1, replica_groups=mesh['kv_0'=8,'kv_1'=4,'tp'=16] {'kv_0','kv_1'}, dimensions={0} | all-to-all | bytes 589824 | tf_op jit(solution)/shard_map/all_to_all | solution.py:43
  59.8 0.6 shard_map.149
  60.4 13.8 %all_to_all.42.recv = bf16[16,16,128]{2,1,0:T(8,128)(2,1)S(1)} all-to-all(bf16[16,16,128]{2,1,0:T(8,128)(2,1)S(1)} %shard_map.149), channel_id=1, replica_groups=mesh['kv_0'=8,'kv_1'=4,'tp'=16] {'tp'}, dimensions={0} | all-to-all | bytes 131072 | tf_op jit(solution)/shard_map/all_to_all | solution.py:43
  74.2 0.3 shard_map.150
  74.5 12.3 %all_to_all.43.recv = bf16[32,8,128]{2,1,0:T(8,128)(2,1)S(1)} all-to-all(bf16[32,8,128]{2,1,0:T(8,128)(2,1)S(1)} %get-tuple-element.33), channel_id=1, replica_groups=mesh['kv_0'=8,'kv_1'=4,'tp'=16] {'kv_0','kv_1'}, dimensions={0} | all-to-all | bytes 131072 | tf_op jit(solution)/shard_map/all_to_all | solution.py:43
  86.8 0.2 shard_map.151
  87.0 11.8 %all_to_all.44.recv = bf16[32,4,128]{2,1,0:T(4,128)(2,1)S(1)} all-to-all(bf16[32,4,128]{2,1,0:T(4,128)(2,1)S(1)} %get-tuple-element.35), channel_id=1, replica_groups=mesh['kv_0'=8,'kv_1'=4,'tp'=16] {'kv_0','kv_1'}, dimensions={0} | all-to-all | bytes 65536 | tf_op jit(solution)/shard_map/all_to_all | solution.py:43
  98.8 0.2 shard_map.152
  98.9 13.0 %all_to_all.45.recv = bf16[16,16,128]{2,1,0:T(8,128)(2,1)S(1)} all-to-all(bf16[16,16,128]{2,1,0:T(8,128)(2,1)S(1)} %shard_map.152), channel_id=1, replica_groups=mesh['kv_0'=8,'kv_1'=4,'tp'=16] {'tp'}, dimensions={0} | all-to-all | bytes 131072 | tf_op jit(solution)/shard_map/all_to_all | solution.py:43
  111.9 0.2 shard_map.153
  112.1 11.6 %all_to_all.46.recv = f32[32,1,128]{2,1,0:T(1,128)S(1)} all-to-all(f32[32,1,128]{2,1,0:T(1,128)S(1)} %get-tuple-element.37), channel_id=1, replica_groups=mesh['kv_0'=8,'kv_1'=4,'tp'=16] {'kv_0','kv_1'}, dimensions={0} | all-to-all | bytes 32768 | tf_op jit(solution)/shard_map/all_to_all | solution.py:43
  123.7 0.0 copy-done.10
  123.7 0.7 shard_map.154
  (9 shorter events, 0.0 us)
Async XLA Ops:
  0.0 17.6 %copy-start = (bf16[256,128]{1,0:T(8,128)(2,1)S(1)}, bf16[256,128]{1,0:T(8,128)(2,1)}, u32[]{:S(2)}) copy-start(bf16[256,128]{1,0:T(8,128)(2,1)} %w_out.3) | copy-start | bytes 196612
  0.0 17.6 %copy-start.4 = (bf16[4096,16]{0,1:T(8,128)(2,1)S(1)}, bf16[4096,16]{0,1:T(8,128)(2,1)}, u32[]{:S(2)}) copy-start(bf16[4096,16]{0,1:T(8,128)(2,1)} %param.22) | copy-start | bytes 393220
  0.0 17.6 %copy-start.5 = (bf16[128,256]{1,0:T(8,128)(2,1)S(1)}, bf16[128,256]{1,0:T(8,128)(2,1)}, u32[]{:S(2)}) copy-start(bf16[128,256]{1,0:T(8,128)(2,1)} %w_query.1) | copy-start | bytes 196612
  0.0 17.6 %copy-start.6 = (bf16[128,64]{0,1:T(8,128)(2,1)S(1)}, bf16[128,64]{0,1:T(8,128)(2,1)}, u32[]{:S(2)}) copy-start(bf16[128,64]{0,1:T(8,128)(2,1)} %param.20) | copy-start | bytes 49156
  0.0 17.6 %copy-start.7 = (bf16[128,64]{0,1:T(8,128)(2,1)S(1)}, bf16[128,64]{0,1:T(8,128)(2,1)}, u32[]{:S(2)}) copy-start(bf16[128,64]{0,1:T(8,128)(2,1)} %param.21) | copy-start | bytes 49156
  0.0 17.6 %copy-start.8 = (f32[16]{0:T(128)S(1)}, f32[16]{0:T(128)}, u32[]{:S(2)}) copy-start(f32[16]{0:T(128)} %param.23) | copy-start | bytes 196
  0.0 30.7 %copy-start.9 = (s32[16]{0:T(128)S(1)}, s32[16]{0:T(128)}, u32[]{:S(2)}) copy-start(s32[16]{0:T(128)} %lengths.1) | copy-start | bytes 196
  18.8 24.3 %all-to-all-start.1 = ((bf16[32,9,4,128]{3,2,1,0:T(4,128)(2,1)}), bf16[32,9,4,128]{3,2,1,0:T(4,128)(2,1)S(1)}, u32[]{:S(2)}, u32[]{:S(2)}) async-start(bf16[32,9,4,128]{3,2,1,0:T(4,128)(2,1)} %get-tuple-element.22), calls=%async_computation.1 | async-start | bytes 589824 | tf_op jit(solution)/shard_map/all_to_all | solution.py:43
  34.7 39.5 %copy-start.1 = (bf16[128,704]{0,1:T(8,128)(2,1)S(1)}, bf16[128,704]{0,1:T(8,128)(2,1)}, u32[]{:S(2)}) copy-start(bf16[128,704]{0,1:T(8,128)(2,1)} %param.26) | copy-start | bytes 540676
  34.7 39.5 %copy-start.2 = (bf16[128,704]{0,1:T(8,128)(2,1)S(1)}, bf16[128,704]{0,1:T(8,128)(2,1)}, u32[]{:S(2)}) copy-start(bf16[128,704]{0,1:T(8,128)(2,1)} %param.27) | copy-start | bytes 540676
  43.1 55.7 %copy-start.3 = (bf16[704,128]{1,0:T(8,128)(2,1)S(1)}, bf16[704,128]{1,0:T(8,128)(2,1)}, u32[]{:S(2)}) copy-start(bf16[704,128]{1,0:T(8,128)(2,1)} %w_down.1) | copy-start | bytes 540676
  43.1 80.6 %copy-start.10 = (f32[8]{0:T(128)S(1)}, f32[8]{0:T(128)}, u32[]{:S(2)}) copy-start(f32[8]{0:T(128)} %param.29) | copy-start | bytes 100
